TPU v7x, 256 devices: a whole 4x4x8 slice. The times are simulated.
256 devices in a mesh: sp: 64 (over z, y, core), tp: 4 (over x).
Axes of the slice: x: 4, y: 4, z: 8, core: 2. Of those that a mesh axis runs over, the one named last changes fastest.
Arguments:
- queries: bfloat16 [8192, 1280], P('sp', 'tp'), may hold values from -4000 to 4000
- latents: bfloat16 [8192, 512], P('sp'), may hold values from -6 to 6
- shared_key: bfloat16 [8192, 64], P('sp'), may hold values from -4 to 4
- expand_weight: bfloat16 [512, 1536], P(None, 'tp'), may hold values from -0.25 to 0.25
- residual: bfloat16 [8192, 2048], P('sp'), may hold values from -3 to 3
- out_weight: bfloat16 [768, 2048], replicated, may hold values from -0.21875 to 0.21875
- norm_gain: bfloat16 [2048], replicated, may hold values from 0.099609375 to 1.8984375
- gate_weight: bfloat16 [2048, 3072], P('sp', 'tp'), may hold values from -0.125 to 0.125
- value_weight: bfloat16 [2048, 3072], P('sp', 'tp'), may hold values from -0.125 to 0.125
- conv_weight: bfloat16 [3, 3072], P(None, 'tp'), may hold values from -3.5 to 3.5
- down_weight: bfloat16 [3072, 2048], P('tp', 'sp'), may hold values from -0.109375 to 0.109375
Outputs:
- output: bfloat16 [8192, 2048], P(('sp', 'tp'))
All inputs are finite; a program needn't handle non-finite values.
Results may differ from a plain program's by a relative error of at most 0.018.
Values may be sent and summed in bfloat16 or wider, within the bound.
A program may use at most 128 MiB of HBM per device.

v0:
```python
import jax
import jax.numpy as jnp
from jax import lax
from jax.sharding import Mesh
from jax.sharding import PartitionSpec as P

NOPE_A = 128
VAL_A = 128
NOPE_B = 64
VAL_B = 64
ROPE = 64
SP = ("sp_0", "sp_1", "sp_2")
SP_TP = ("sp_0", "sp_1", "sp_2", "tp")


def in_one_piece(arrays, axis, dim, along):
    both = jnp.concatenate(arrays, axis=along)
    out, at, outs = (lax.all_gather(both, axis, axis=dim, tiled=True), 0, [])
    for a in arrays:
        outs.append(lax.slice_in_dim(out, at, at + a.shape[along], axis=along))
        at += a.shape[along]
    return tuple(outs)


def padded_2(block, sides, width):
    for axis, dim in sides:
        count = lax.axis_size(axis)
        forward = [(i, i + 1) for i in range(count - 1)]
        backward = [(target, source) for source, target in forward]
        low = lax.ppermute(
            lax.slice_in_dim(block, block.shape[dim] - width, None, axis=dim), axis, forward
        )
        high = lax.ppermute(lax.slice_in_dim(block, 0, width, axis=dim), axis, backward)
        block = jnp.concatenate([low, block, high], axis=dim)
    return block


def sent_to_all(x, axis):
    length = lax.axis_size(axis)
    return lax.all_to_all(jnp.broadcast_to(x[None], (length, *x.shape)), axis, 0, 0, tiled=True)


def joined_along(pieces, dim):
    lengths = list(pieces.shape[1:])
    lengths[dim] *= pieces.shape[0]
    return jnp.moveaxis(pieces, 0, dim).reshape(lengths)


def whole_of(x, axes, dim):
    far, near = axes
    leading = sent_to_all(x, far)
    pieces = jnp.swapaxes(sent_to_all(leading, near), 0, 1)
    return joined_along(pieces.reshape(-1, *x.shape), dim)


def in_blocks(x, dim, length):
    before, after = (x.shape[:dim], x.shape[dim + 1 :])
    return jnp.moveaxis(x.reshape(*before, length, -1, *after), dim, 0)


def sent_and_summed(x, axis, dim):
    pieces = in_blocks(x, dim, lax.axis_size(axis))
    arrived = lax.all_to_all(pieces, axis, split_axis=0, concat_axis=0, tiled=True)
    return arrived.astype(jnp.float32).sum(axis=0)


def tables(positions, width):
    half_width = width // 2
    frequency = 10000.0 ** (-jnp.arange(half_width, dtype=jnp.float32) / half_width)
    angles = positions.astype(jnp.float32)[:, None] * frequency[None, :]
    return (jnp.cos(angles), jnp.sin(angles))


def rotate(vectors, cos_table, sine_table):
    half_width = vectors.shape[-1] // 2
    first_half = vectors[:, :half_width].astype(jnp.float32)
    second_half = vectors[:, half_width:].astype(jnp.float32)
    turned = jnp.concatenate(
        [
            first_half * cos_table - second_half * sine_table,
            second_half * cos_table + first_half * sine_table,
        ],
        axis=1,
    )
    return turned.astype(jnp.bfloat16)


def normalize(stream, norm_gain):
    stream_f = stream.astype(jnp.float32)
    scaled = stream_f * lax.rsqrt(jnp.mean(stream_f * stream_f, axis=1, keepdims=True) + 1e-06)
    return (scaled * norm_gain.astype(jnp.float32)).astype(jnp.bfloat16)


def update(running, q_content, q_turned, k_content, k_turned, values, score_scale):
    row_max, row_sum, weighted = running
    scores = (
        jnp.einsum("qd,kd->qk", q_content, k_content, preferred_element_type=jnp.float32)
        + jnp.einsum("qd,kd->qk", q_turned, k_turned, preferred_element_type=jnp.float32)
    ) * score_scale
    new_max = jnp.maximum(row_max, jnp.max(scores, axis=1))
    weights = jnp.exp(scores - new_max[:, None])
    row_sum = jnp.sum(weights, axis=1)
    weighted = jnp.dot(weights.astype(jnp.bfloat16), values, preferred_element_type=jnp.float32)
    return (new_max, row_sum, weighted)


def body(
    queries,
    latents,
    shared_key,
    expand_weight,
    residual,
    out_weight,
    norm_gain,
    gate_weight,
    value_weight,
    conv_weight,
    down_weight,
):
    tok_rows = queries.shape[0]
    q_width = NOPE_A + NOPE_B + 2 * ROPE
    kv_width = NOPE_A + VAL_A + NOPE_B + VAL_B
    positions = lax.axis_index(SP) * tok_rows + jnp.arange(tok_rows, dtype=jnp.int32)
    cos_table, sine_table = tables(positions, ROPE)
    key_turned = rotate(shared_key, cos_table, sine_table)
    scale_wide = (NOPE_A + ROPE) ** (-0.5)
    scale_narrow = (NOPE_B + ROPE) ** (-0.5)
    initial = []
    pair_index = 0
    q_base = pair_index * q_width
    rotary_base = q_base + NOPE_A + NOPE_B
    wide_content = queries[:, q_base : q_base + NOPE_A]
    narrow_content = queries[:, q_base + NOPE_A : rotary_base]
    wide_turned = rotate(queries[:, rotary_base : rotary_base + ROPE], cos_table, sine_table)
    narrow_turned = rotate(
        queries[:, rotary_base + ROPE : rotary_base + 2 * ROPE], cos_table, sine_table
    )
    query_parts = [(wide_content, wide_turned, narrow_content, narrow_turned)]
    lowest = jnp.full((tok_rows,), -1e30, jnp.float32)
    empty_sum = jnp.zeros((tok_rows,), jnp.float32)
    initial += [
        lowest,
        empty_sum,
        jnp.zeros((tok_rows, VAL_A), jnp.float32),
        lowest,
        empty_sum,
        jnp.zeros((tok_rows, VAL_B), jnp.float32),
    ]
    initial = tuple(initial)
    expanded_own = jnp.dot(latents, expand_weight, preferred_element_type=jnp.float32).astype(
        jnp.bfloat16
    )
    pieces = in_one_piece((expanded_own, key_turned), SP, 0, 1)
    expanded = pieces[0]
    turned_keys = pieces[1]
    result = []
    pair_index = 0
    wide_content, wide_turned, narrow_content, narrow_turned = query_parts[pair_index]
    kv_base = pair_index * kv_width
    narrow_base = kv_base + NOPE_A + VAL_A
    wide_keys = expanded[:, kv_base : kv_base + NOPE_A]
    wide_values = expanded[:, kv_base + NOPE_A : narrow_base]
    narrow_keys = expanded[:, narrow_base : narrow_base + NOPE_B]
    narrow_values = expanded[:, narrow_base + NOPE_B : narrow_base + NOPE_B + VAL_B]
    absorb_offset = 6 * pair_index
    result += list(
        update(
            initial[absorb_offset : absorb_offset + 3],
            wide_content,
            wide_turned,
            wide_keys,
            turned_keys,
            wide_values,
            scale_wide,
        )
    )
    result += list(
        update(
            initial[absorb_offset + 3 : absorb_offset + 6],
            narrow_content,
            narrow_turned,
            narrow_keys,
            turned_keys,
            narrow_values,
            scale_narrow,
        )
    )
    running = tuple(result)
    outputs = []
    pair_index = 0
    for group_index in range(2):
        offset = 6 * pair_index + 3 * group_index
        outputs.append((running[offset + 2] / running[offset + 1][:, None]).astype(jnp.bfloat16))
    attended = jnp.concatenate(outputs, axis=1)
    share = tok_rows // lax.axis_size("tp")
    tp_index = lax.axis_index("tp")
    all_heads = lax.all_gather(attended, "tp", axis=1, tiled=True)
    projected = jnp.dot(all_heads, out_weight, preferred_element_type=jnp.float32)
    stream = (residual.astype(jnp.float32) + projected).astype(jnp.bfloat16)
    normed = normalize(stream, norm_gain)
    stream_own = lax.dynamic_slice_in_dim(stream, tp_index * share, share, 0)
    pieces = in_one_piece((gate_weight, value_weight), SP, 0, 1)
    gate_sum = jnp.dot(normed, pieces[0], preferred_element_type=jnp.float32)
    value_sum = jnp.dot(normed, pieces[1], preferred_element_type=jnp.float32)
    gate_pre = gate_sum.astype(jnp.bfloat16)
    value_pre = value_sum.astype(jnp.bfloat16)
    reach = conv_weight.shape[0] // 2
    padded = padded_2(gate_pre, ((SP, 0),), reach)
    mixed_gate = jnp.zeros(gate_pre.shape, jnp.float32)
    for tap in range(conv_weight.shape[0]):
        mixed_gate = mixed_gate + padded[tap : tap + tok_rows].astype(jnp.float32) * conv_weight[
            tap
        ].astype(jnp.float32)
    active = (jax.nn.silu(mixed_gate) * value_pre.astype(jnp.float32)).astype(jnp.bfloat16)
    partial_rows = jnp.dot(
        active,
        whole_of(down_weight, (("sp_0", "sp_1"), "sp_2"), 1),
        preferred_element_type=jnp.float32,
    )
    summed = sent_and_summed(partial_rows.astype(jnp.bfloat16), "tp", 0)
    return (stream_own.astype(jnp.float32) + summed).astype(jnp.bfloat16)


def solution(mesh):
    split = Mesh(mesh.devices.reshape(8, 4, 2, mesh.shape["tp"]), ("sp_0", "sp_1", "sp_2", "tp"))
    placed = (
        P(SP, "tp"),
        P(SP, None),
        P(SP, None),
        P(None, "tp"),
        P(SP, None),
        P(),
        P(),
        P(SP, "tp"),
        P(SP, "tp"),
        P(None, "tp"),
        P("tp", SP),
    )
    return jax.shard_map(
        body, mesh=split, in_specs=placed, out_specs=P(SP_TP, None), check_vma=False
    )
```

profile of v0, /device:TPU:1, one launch (start us, length us, event | category | flops | bytes accessed | tf_op | source)
XLA Modules:
  0.0 229.6 jit_solution(11036286875932649535)
XLA Ops:
  6.5 0.0 copy-start
  6.5 0.0 copy-start.3
  6.5 0.0 copy-start.5
  6.5 0.0 all-gather.3.cloned.1.call-start
  6.6 1.1 fusion.103
  7.7 0.1 copy.38
  7.8 0.1 copy.39
  7.9 1.3 convolution_convert_fusion.1
  9.2 0.7 pad_maximum_fusion.4
  10.0 0.0 all-gather.3.cloned.1.call-update
  10.0 0.0 all-gather.5.cloned.1.call-start
  10.0 1.5 pad_maximum_fusion.5
  11.5 0.0 all-gather.5.cloned.1.call-update
  11.6 2.1 broadcast_in_dim.7
  13.7 12.1 %all-to-all-start = ((bf16[32,768,32]{1,2,0:T(8,128)(2,1)}), bf16[32,768,32]{1,2,0:T(8,128)(2,1)}, u32[]{:S(2)}, u32[]{:S(2)}) async-start(bf16[32,768,32]{1,2,0:T(8,128)(2,1)} %broadcast_in_dim.7), calls=%async_computation | async-start | bytes 3145728 | tf_op jit(solution)/shard_map/all_to_all | solution.py:40
  25.8 0.0 copy-done.5
  25.9 78.5 %all-gather.3.cloned.1.call-done = bf16[8192,448]{1,0:T(8,128)(2,1)} async-done(((bf16[128,448]{1,0:T(8,128)(2,1)}), bf16[8192,448]{1,0:T(8,128)(2,1)}) %all-gather.3.cloned.1.call-update) | async-done | bytes 7340048 | tf_op jit(solution)/shard_map/all_gather | solution.py:18
  104.3 0.0 copy-done.3
  104.3 0.0 copy-start.1
  104.3 2.4 %convolution_bitcast_fusion.1 = f32[128,8192]{0,1:T(8,128)S(1)} fusion(bf16[8192,448]{1,0:T(8,128)(2,1)} %all-gather.3.cloned.1.call-done, bf16[128,320]{0,1:T(8,128)(2,1)S(1)} %copy-done.3), kind=kOutput, calls=%fused_computation.5 | convolution fusion | flops 268435456 | bytes 6324224 | tf_op jit(solution)/shard_map/qd,kd->qk/dot_general | solution.py:97
  106.8 1.6 copy-done.1
  108.4 1.2 fusion.123
  109.6 0.7 convolution_bitcast_fusion
  110.3 1.2 fusion.122
  111.5 1.1 fusion.2
  112.6 1.1 fusion.4
  113.8 1.9 fusion.43
  115.6 0.0 copy-start.2
  115.6 1.2 fusion.53
  116.9 10.2 %all_gather.10 = bf16[128,768]{0,1:T(8,128)(2,1)S(1)} all-gather(bf16[128,192]{0,1:T(8,128)(2,1)S(1)} %pad_maximum_fusion.6), channel_id=1, replica_groups=mesh['sp_0'=8,'sp_1'=4,'sp_2'=2,'tp'=4] {'tp'}, dimensions={1}, use_global_device_ids=true | all-gather | bytes 245760 | tf_op jit(solution)/shard_map/all_gather | solution.py:197
  127.0 0.0 copy-done
  127.0 0.0 copy-done.2
  127.0 0.0 copy-start.4
  127.0 1.4 fusion.58
  128.5 56.0 %all-gather.5.cloned.1.call-done = bf16[2048,1536]{1,0:T(8,128)(2,1)} async-done(((bf16[32,1536]{1,0:T(8,128)(2,1)}), bf16[2048,1536]{1,0:T(8,128)(2,1)}) %all-gather.5.cloned.1.call-update) | async-done | bytes 6291472 | tf_op jit(solution)/shard_map/all_gather | solution.py:18
  184.5 2.7 %fusion.23 = bf16[128,768]{1,0:T(8,128)(2,1)S(1)} fusion(bf16[2048,1536]{1,0:T(8,128)(2,1)} %all-gather.5.cloned.1.call-done, bf16[128,2048]{1,0:T(8,128)(2,1)} %get-tuple-element.23, f32[2048]{0:T(1024)S(1)} %convert_element_type.113, f32[128]{0:T(128)S(1)} %add_rsqrt_fusion), kind=kOutput, calls=%fused_computation.31 | convolution fusion | flops 403800064 | bytes 3875328 | tf_op jit(solution)/shard_map/dot_general | solution.py:203
  187.2 2.0 collective-permute-start
  189.2 2.3 %collective-permute-start.1 = (bf16[1,768]{1,0:T(2,128)(2,1)S(1)}, bf16[1,768]{1,0:T(2,128)(2,1)S(1)}, u32[]{:S(2)}, u32[]{:S(2)}) collective-permute-start(bf16[1,768]{1,0:T(2,128)(2,1)S(1)} %get-tuple-element.9), channel_id=1, source_target_pairs={{4,0},{8,4},{12,8},{16,12},{20,16},{24,20},{28,24},{32,28},{36,32}... | collective-permute-start | bytes 4616 | tf_op jit(solution)/shard_map/ppermute | solution.py:33
  191.5 0.0 copy-done.4
  191.6 0.0 all-to-all-done
  191.6 1.8 broadcast_in_dim.8
  193.4 5.9 %all_to_all.15 = bf16[2,32,768,32]{2,3,1,0:T(8,128)(2,1)S(1)} all-to-all(bf16[2,32,768,32]{2,3,1,0:T(8,128)(2,1)S(1)} %broadcast_in_dim.8), channel_id=1, replica_groups=mesh['sp_0'=8,'sp_1'=4,'sp_2'=2,'tp'=4] {'sp_2'}, dimensions={0} | all-to-all | bytes 6291456 | tf_op jit(solution)/shard_map/all_to_all | solution.py:40
  199.3 2.0 copy.42
  201.2 0.0 collective-permute-done
  201.2 0.0 collective-permute-done.1
  201.2 5.5 %convolution_convert_fusion = bf16[128,2048]{1,0:T(8,128)(2,1)} fusion(bf16[768,2048]{0,1:T(8,128)(2,1)} %bitcast.17, bf16[2048,1536]{1,0:T(8,128)(2,1)} %all-gather.5.cloned.1.call-done, bf16[128,768]{1,0:T(8,128)(2,1)S(1)} %fusion.23, bf16[1,768]{1,0:T(2,128)(2,1)S(1)} %collective-permute-done.1, bf16[1,768]{1,0:T(2,128)(2,1)S(1)} %collective-permute-done, ...), kind=kOutput, calls=%fused_computation.18 | convolution fusion | flops 808779776 | bytes 7557632 | tf_op jit(solution)/shard_map/dot_general | solution.py:215
  206.8 4.1 %all-to-all-start.2 = ((bf16[4,32,2048]{2,1,0:T(8,128)(2,1)}), bf16[4,32,2048]{2,1,0:T(8,128)(2,1)}, u32[]{:S(2)}, u32[]{:S(2)}) async-start(bf16[4,32,2048]{2,1,0:T(8,128)(2,1)} %bitcast.18), calls=%async_computation.2 | async-start | bytes 1048576 | tf_op jit(solution)/shard_map/all_to_all | solution.py:63
  210.9 9.1 %all-to-all-done.2 = bf16[4,32,2048]{2,1,0:T(8,128)(2,1)} async-done(((bf16[4,32,2048]{2,1,0:T(8,128)(2,1)}), bf16[4,32,2048]{2,1,0:T(8,128)(2,1)}, u32[]{:S(2)}, u32[]{:S(2)}) %all-to-all-start.2) | async-done | bytes 524320 | tf_op jit(solution)/shard_map/all_to_all | solution.py:63
  220.0 1.1 convert_reduce_fusion
  221.1 1.6 add_convert_fusion
  (9 shorter events, 0.1 us)
Async XLA Ops:
  6.5 120.5 %copy-start = (bf16[768,2048]{1,0:T(8,128)(2,1)S(1)}, bf16[768,2048]{1,0:T(8,128)(2,1)}, u32[]{:S(2)}) copy-start(bf16[768,2048]{1,0:T(8,128)(2,1)} %param.16) | copy-start | bytes 9437188
  6.5 97.8 %copy-start.3 = (bf16[128,320]{0,1:T(8,128)(2,1)S(1)}, bf16[128,320]{0,1:T(8,128)(2,1)}, u32[]{:S(2)}) copy-start(bf16[128,320]{0,1:T(8,128)(2,1)} %param.11) | copy-start | bytes 245764
  6.5 19.3 %copy-start.5 = (bf16[2048]{0:T(1024)(128)(2,1)S(1)}, bf16[2048]{0:T(1024)(128)(2,1)}, u32[]{:S(2)}) copy-start(bf16[2048]{0:T(1024)(128)(2,1)} %param.17) | copy-start | bytes 12292
  6.5 97.8 %all-gather.3.cloned.1.call-start = ((), (), s32[]{:S(2)}) async-start(), calls=%async_computation.3 | async-start | bytes 8519680 | tf_op jit(solution)/shard_map/all_gather | solution.py:18
  10.0 174.5 %all-gather.5.cloned.1.call-start = ((), (), s32[]{:S(2)}) async-start(), calls=%async_computation.4 | async-start | bytes 6389760 | tf_op jit(solution)/shard_map/all_gather | solution.py:18
  13.7 177.9 %all-to-all-start = ((bf16[32,768,32]{1,2,0:T(8,128)(2,1)}), bf16[32,768,32]{1,2,0:T(8,128)(2,1)}, u32[]{:S(2)}, u32[]{:S(2)}) async-start(bf16[32,768,32]{1,2,0:T(8,128)(2,1)} %broadcast_in_dim.7), calls=%async_computation | async-start | bytes 3145728 | tf_op jit(solution)/shard_map/all_to_all | solution.py:40
  104.3 4.0 %copy-start.1 = (bf16[8192,448]{1,0:T(8,128)(2,1)S(1)}, bf16[8192,448]{1,0:T(8,128)(2,1)}, u32[]{:S(2)}) copy-start(bf16[8192,448]{1,0:T(8,128)(2,1)} %all-gather.3.cloned.1.call-done) | copy-start | bytes 22020100
  115.6 11.4 %copy-start.2 = (bf16[128,2048]{1,0:T(8,128)(2,1)S(1)}, bf16[128,2048]{1,0:T(8,128)(2,1)}, u32[]{:S(2)}) copy-start(bf16[128,2048]{1,0:T(8,128)(2,1)} %param.15) | copy-start | bytes 1572868
  127.0 64.5 %copy-start.4 = (bf16[3,768]{1,0:T(4,128)(2,1)S(1)}, bf16[3,768]{1,0:T(4,128)(2,1)}, u32[]{:S(2)}) copy-start(bf16[3,768]{1,0:T(4,128)(2,1)} %param.20) | copy-start | bytes 13828
  187.2 14.1 %collective-permute-start = (bf16[1,768]{1,0:T(2,128)(2,1)S(1)}, bf16[1,768]{1,0:T(2,128)(2,1)S(1)}, u32[]{:S(2)}, u32[]{:S(2)}) collective-permute-start(bf16[1,768]{1,0:T(2,128)(2,1)S(1)} %get-tuple-element.8), channel_id=1, source_target_pairs={{0,4},{4,8},{8,12},{12,16},{16,20},{20,24},{24,28},{28,32},{32,36}... | collective-permute-start | bytes 4616 | tf_op jit(solution)/shard_map/ppermute | solution.py:30
  189.2 12.1 %collective-permute-start.1 = (bf16[1,768]{1,0:T(2,128)(2,1)S(1)}, bf16[1,768]{1,0:T(2,128)(2,1)S(1)}, u32[]{:S(2)}, u32[]{:S(2)}) collective-permute-start(bf16[1,768]{1,0:T(2,128)(2,1)S(1)} %get-tuple-element.9), channel_id=1, source_target_pairs={{4,0},{8,4},{12,8},{16,12},{20,16},{24,20},{28,24},{32,28},{36,32}... | collective-permute-start | bytes 4616 | tf_op jit(solution)/shard_map/ppermute | solution.py:33
  206.8 13.2 %all-to-all-start.2 = ((bf16[4,32,2048]{2,1,0:T(8,128)(2,1)}), bf16[4,32,2048]{2,1,0:T(8,128)(2,1)}, u32[]{:S(2)}, u32[]{:S(2)}) async-start(bf16[4,32,2048]{2,1,0:T(8,128)(2,1)} %bitcast.18), calls=%async_computation.2 | async-start | bytes 1048576 | tf_op jit(solution)/shard_map/all_to_all | solution.py:63
Sparse Core Ops, SparseCore 0:
  10.1 94.1 all-gather.2
  107.1 77.3 all-gather.4
where the time goes:
time: 233 us; the launch traced here: 230 us
  waiting for transfers between devices  144 us (62%)
  starting transfers between devices  20.6 us (9%)
  matrix products  19.6 us (8%)
  blocking collectives  16.1 us (7%)
  between operations  13.6 us (6%)
  other arithmetic  8.33 us (4%)
  local copies, waits for them, and re-layouts  7.75 us (3%)
    all_gather x2, waiting for transfers between devices, in_one_piece(): out, at, outs = (lax.all_gather(both, axis, axis=dim, tiled=True), 0, [])  134 us
    all_to_all x1, starting transfers between devices, sent_to_all(): lax.all_to_all(jnp.broadcast_to(x[None], (length, *x.shape)), axis, 0, 0,...  12.1 us
    all_gather x1, blocking collectives, body(): all_heads = lax.all_gather(attended, 'tp', axis=1, tiled=True)  10.2 us
    all_to_all x1, waiting for transfers between devices, sent_and_summed(): lax.all_to_all(pieces, axis, split_axis=0, concat_axis=0, tiled=True)  9.1 us
    all_to_all x1, blocking collectives, sent_to_all(): lax.all_to_all(jnp.broadcast_to(x[None], (length, *x.shape)), axis, 0, 0,...  5.9 us
    dot_general x1, matrix products, body(): jnp.dot(active, whole_of(down_weight, (('sp_0', 'sp_1'), 'sp_2'), 1), pre...  5.53 us
  transfers between devices with their start and end apart: 6, of which 3 were waited for; matrix products, arithmetic and copies ran while one was open for 10% of the time, Pallas kernels for 0%

commit v1 on v0

v1 whole, which is shorter than its diff:
```python
import functools

import jax
import jax.numpy as jnp
from jax import lax
from jax.experimental import pallas as pl
from jax.experimental.pallas import tpu as pltpu
from jax.sharding import Mesh
from jax.sharding import PartitionSpec as P

NOPE_A = 128
VAL_A = 128
NOPE_B = 64
VAL_B = 64
ROPE = 64
SP = ("sp_0", "sp_1", "sp_2")
SP_TP = ("sp_0", "sp_1", "sp_2", "tp")
NZ, NY, NX = 8, 4, 4
TOK = 128
D = 2048
FFD = 768
MESH = pl.DeviceIdType.MESH
LOG2E = 1.4426950408889634
F32 = jnp.float32
BF = jnp.bfloat16


def tables(positions, width):
    half_width = width // 2
    frequency = 10000.0 ** (-jnp.arange(half_width, dtype=jnp.float32) / half_width)
    angles = positions.astype(jnp.float32)[:, None] * frequency[None, :]
    return (jnp.cos(angles), jnp.sin(angles))


def rotate(vectors, cos_table, sine_table):
    half_width = vectors.shape[-1] // 2
    first_half = vectors[:, :half_width].astype(jnp.float32)
    second_half = vectors[:, half_width:].astype(jnp.float32)
    turned = jnp.concatenate(
        [
            first_half * cos_table - second_half * sine_table,
            second_half * cos_table + first_half * sine_table,
        ],
        axis=1,
    )
    return turned.astype(jnp.bfloat16)


def split3(v):
    hi = v.astype(BF).astype(F32)
    rest = v - hi
    mid = rest.astype(BF).astype(F32)
    return hi, mid, rest - mid


def kernel(
    q_own, kv_own, gv_own, dn_own, gain, conv_w, resid_hbm, ow_hbm,
    out_ref,
    kvb, qb, gv, dn, ow, resid, s_ref, macc, mrow, accw, accn,
    part, ob, att, stream, normed, gate, value, hp, hn, act, fp, fr,
    kvz_s, kvz_r, q_s, q_r, gvz_s, gvz_r, gvy_s, gvy_r, dny_s, dny_r, dnz_s, dnz_r,
    pk_s, pk_r, pg_s, pg_r, pd_s, pd_r, o_s, o_r, x_s, x_r, h_s, h_r, f_s, f_r, loc,
):
    z = lax.axis_index("sp_0")
    y = lax.axis_index("sp_1")
    c = lax.axis_index("sp_2")
    x = lax.axis_index("tp")
    other = 1 - c

    def zat(k):
        return lax.rem(z + (k + NZ), NZ)

    def yat(k):
        return lax.rem(y + (k + NY), NY)

    def xat(k):
        return lax.rem(x + (k + NX), NX)

    right_z, left_z = {"sp_0": zat(1)}, {"sp_0": zat(-1)}
    right_y, left_y = {"sp_1": yat(1)}, {"sp_1": yat(-1)}
    partner = {"sp_2": other}
    place = (z * NY + y) * 2 + c
    after = lax.rem(place + 1, 64)
    before = lax.rem(place + 63, 64)

    def device_of(i):
        return {"sp_0": i // 8, "sp_1": lax.rem(i // 2, 4), "sp_2": lax.rem(i, 2)}

    def send(src, dst, ssem, rsem, dev):
        pltpu.make_async_remote_copy(
            src_ref=src, dst_ref=dst, send_sem=ssem, recv_sem=rsem, device_id=dev, device_id_type=MESH
        ).start()

    def wait_recv(ref, sem):
        pltpu.make_async_remote_copy(
            src_ref=ref, dst_ref=ref, send_sem=sem, recv_sem=sem, device_id=partner, device_id_type=MESH
        ).wait_recv()

    def wait_send(ref, sem):
        pltpu.make_async_remote_copy(
            src_ref=ref, dst_ref=ref, send_sem=sem, recv_sem=sem, device_id=partner, device_id_type=MESH
        ).wait_send()

    load_ow = pltpu.make_async_copy(ow_hbm, ow, loc.at[0])
    load_ow.start()
    load_res = pltpu.make_async_copy(resid_hbm, resid, loc.at[1])
    load_res.start()

    barrier = pltpu.get_barrier_semaphore()
    greeted = [
        partner, right_z, left_z, right_y, left_y, {"sp_1": yat(2)},
        {"tp": xat(1)}, {"tp": xat(2)}, {"tp": xat(3)}, device_of(after), device_of(before),
    ]
    for dev in greeted:
        pl.semaphore_signal(barrier, inc=1, device_id=dev, device_id_type=MESH)
    pl.semaphore_wait(barrier, len(greeted))

    send(kv_own, kvb.at[z, c], kvz_s, kvz_r.at[0, 0], right_z)
    send(kv_own, kvb.at[z, c], kvz_s, kvz_r.at[1, 0], left_z)
    send(q_own, qb.at[y], q_s, q_r.at[0, 0], right_y)
    send(q_own, qb.at[y], q_s, q_r.at[1, 0], left_y)
    send(gv_own, gv.at[z, y, c], gvz_s, gvz_r.at[0, 0], right_z)
    send(gv_own, gv.at[z, y, c], gvz_s, gvz_r.at[1, 0], left_z)
    send(dn_own, dn.at[z, y, c], dny_s, dny_r.at[0, 0], right_y)
    send(dn_own, dn.at[z, y, c], dny_s, dny_r.at[1, 0], left_y)
    send(kv_own, kvb.at[z, c], pk_s, pk_r, partner)
    send(gv_own, gv.at[z, y, c], gvy_s, gvy_r.at[0, 0, 0], right_y)
    send(gv_own, gv.at[z, y, c], gvy_s, gvy_r.at[1, 0, 0], left_y)
    send(gv_own, gv.at[z, y, c], pg_s, pg_r, partner)
    kvb[z, c] = kv_own[...]
    qb[y] = q_own[...]
    gv[z, y, c] = gv_own[...]
    dn[z, y, c] = dn_own[...]

    offsets = [0, -1, 1, -2, 2, -3, 3, 4]

    def kvz(s):
        lo, hi = zat(-s), zat(s)
        if s < 4:
            wait_recv(kvb.at[lo, c], kvz_r.at[0, s - 1])
            if s < 3:
                send(kvb.at[lo, c], kvb.at[lo, c], kvz_s, kvz_r.at[0, s], right_z)
            else:
                send(kvb.at[lo, c, pl.ds(0, 64)], kvb.at[lo, c, pl.ds(0, 64)], kvz_s, kvz_r.at[0, s], right_z)
            wait_recv(kvb.at[hi, c], kvz_r.at[1, s - 1])
            if s < 3:
                send(kvb.at[hi, c], kvb.at[hi, c], kvz_s, kvz_r.at[1, s], left_z)
            else:
                send(kvb.at[hi, c, pl.ds(64, 64)], kvb.at[hi, c, pl.ds(64, 64)], kvz_s, kvz_r.at[1, s], left_z)
            send(kvb.at[lo, c], kvb.at[lo, c], pk_s, pk_r, partner)
            send(kvb.at[hi, c], kvb.at[hi, c], pk_s, pk_r, partner)
        else:
            wait_recv(kvb.at[lo, c, pl.ds(0, 64)], kvz_r.at[0, 3])
            wait_recv(kvb.at[lo, c, pl.ds(64, 64)], kvz_r.at[1, 3])
            send(kvb.at[lo, c], kvb.at[lo, c], pk_s, pk_r, partner)

    def q_relay(s):
        a, b, far = yat(-1), yat(1), yat(2)
        if s == 1:
            wait_recv(qb.at[a], q_r.at[0, 0])
            send(qb.at[a, pl.ds(0, 64)], qb.at[a, pl.ds(0, 64)], q_s, q_r.at[0, 1], right_y)
            wait_recv(qb.at[b], q_r.at[1, 0])
            send(qb.at[b, pl.ds(64, 64)], qb.at[b, pl.ds(64, 64)], q_s, q_r.at[1, 1], left_y)
        else:
            wait_recv(qb.at[far, pl.ds(0, 64)], q_r.at[0, 1])
            wait_recv(qb.at[far, pl.ds(64, 64)], q_r.at[1, 1])

    def gv_out(zz, j):
        block = gv.at[zz, y, c]
        send(block, block, gvy_s, gvy_r.at[0, 0, j], right_y)
        send(block, block, gvy_s, gvy_r.at[1, 0, j], left_y)
        send(block, block, pg_s, pg_r, partner)

    def gvz(s):
        lo, hi = zat(-s), zat(s)
        if s < 4:
            wait_recv(gv.at[lo, y, c], gvz_r.at[0, s - 1])
            src = gv.at[lo, y, c] if s < 3 else gv.at[lo, y, c, pl.ds(0, 32)]
            send(src, src, gvz_s, gvz_r.at[0, s], right_z)
            wait_recv(gv.at[hi, y, c], gvz_r.at[1, s - 1])
            src = gv.at[hi, y, c] if s < 3 else gv.at[hi, y, c, pl.ds(32, 32)]
            send(src, src, gvz_s, gvz_r.at[1, s], left_z)
            gv_out(lo, 2 * s - 1)
            gv_out(hi, 2 * s)
        else:
            wait_recv(gv.at[lo, y, c, pl.ds(0, 32)], gvz_r.at[0, 3])
            wait_recv(gv.at[lo, y, c, pl.ds(32, 32)], gvz_r.at[1, 3])
            gv_out(lo, 7)

    def gvy(s, j):
        zz = zat(offsets[j])
        a, b, far = yat(-1), yat(1), yat(2)
        if s == 1:
            wait_recv(gv.at[zz, a, c], gvy_r.at[0, 0, j])
            src = gv.at[zz, a, c, pl.ds(0, 32)]
            send(src, src, gvy_s, gvy_r.at[0, 1, j], right_y)
            wait_recv(gv.at[zz, b, c], gvy_r.at[1, 0, j])
            src = gv.at[zz, b, c, pl.ds(32, 32)]
            send(src, src, gvy_s, gvy_r.at[1, 1, j], left_y)
            send(gv.at[zz, a, c], gv.at[zz, a, c], pg_s, pg_r, partner)
            send(gv.at[zz, b, c], gv.at[zz, b, c], pg_s, pg_r, partner)
        else:
            wait_recv(gv.at[zz, far, c, pl.ds(0, 32)], gvy_r.at[0, 1, j])
            wait_recv(gv.at[zz, far, c, pl.ds(32, 32)], gvy_r.at[1, 1, j])
            send(gv.at[zz, far, c], gv.at[zz, far, c], pg_s, pg_r, partner)

    def dny(s):
        a, b, far = yat(-1), yat(1), yat(2)
        if s == 1:
            wait_recv(dn.at[z, a, c], dny_r.at[0, 0])
            src = dn.at[z, a, c, pl.ds(0, 16)]
            send(src, src, dny_s, dny_r.at[0, 1], right_y)
            wait_recv(dn.at[z, b, c], dny_r.at[1, 0])
            src = dn.at[z, b, c, pl.ds(16, 16)]
            send(src, src, dny_s, dny_r.at[1, 1], left_y)
        else:
            wait_recv(dn.at[z, far, c, pl.ds(0, 16)], dny_r.at[0, 1])
            wait_recv(dn.at[z, far, c, pl.ds(16, 16)], dny_r.at[1, 1])

    def dnz(s):
        lo, hi = zat(-s), zat(s)
        if s == 0:
            bundle = dn.at[z, :, c]
            send(bundle, bundle, dnz_s, dnz_r.at[0, 0], right_z)
            send(bundle, bundle, dnz_s, dnz_r.at[1, 0], left_z)
            send(bundle, bundle, pd_s, pd_r, partner)
        elif s < 4:
            wait_recv(dn.at[lo, :, c], dnz_r.at[0, s - 1])
            src = dn.at[lo, :, c] if s < 3 else dn.at[lo, pl.ds(0, 2), c]
            send(src, src, dnz_s, dnz_r.at[0, s], right_z)
            wait_recv(dn.at[hi, :, c], dnz_r.at[1, s - 1])
            src = dn.at[hi, :, c] if s < 3 else dn.at[hi, pl.ds(2, 2), c]
            send(src, src, dnz_s, dnz_r.at[1, s], left_z)
            send(dn.at[lo, :, c], dn.at[lo, :, c], pd_s, pd_r, partner)
            send(dn.at[hi, :, c], dn.at[hi, :, c], pd_s, pd_r, partner)
        else:
            wait_recv(dn.at[lo, pl.ds(0, 2), c], dnz_r.at[0, 3])
            wait_recv(dn.at[lo, pl.ds(2, 2), c], dnz_r.at[1, 3])
            send(dn.at[lo, :, c], dn.at[lo, :, c], pd_s, pd_r, partner)

    heads = (
        (0, 256, 0, 256, 256, 512, (NOPE_A + ROPE) ** (-0.5) * LOG2E, accw),
        (256, 384, 128, 256, 384, 512, (NOPE_B + ROPE) ** (-0.5) * LOG2E, accn),
    )

    def scores(head):
        q0, q1, k0, k1 = heads[head][:4]
        macc[...] = jnp.full((512, 128), -3e38, F32)

        def step(k, carry):
            qs = qb[:, :, q0:q1].reshape(512, q1 - q0)
            ks = kvb[k, :, :, k0:k1].reshape(256, k1 - k0)
            s = lax.dot_general(qs, ks, (((1,), (1,)), ((), ())), preferred_element_type=F32)
            s_ref[k] = s
            macc[...] = jnp.maximum(macc[...], jnp.maximum(s[:, :128], s[:, 128:]))
            return carry

        lax.fori_loop(0, NZ, step, 0)

    def weigh(head):
        v0, v1, factor, acc = heads[head][4:]
        m = jnp.max(macc[...], axis=1, keepdims=True)
        mrow[head] = jnp.broadcast_to(m, (512, 128))
        acc[...] = jnp.zeros(acc.shape, F32)

        def step(k, carry):
            mb = mrow[head]
            s = s_ref[k]
            p = jnp.exp2((s - jnp.concatenate([mb, mb], axis=1)) * factor).astype(BF)
            vs = kvb[k, :, :, v0:v1].reshape(256, v1 - v0)
            acc[...] += jnp.dot(p, vs, preferred_element_type=F32)
            return carry

        lax.fori_loop(0, NZ, step, 0)

    def pack():
        def step(b, carry):
            rows = pl.ds(pl.multiple_of(b * TOK, TOK), TOK)
            wide, narrow = accw[rows, :], accn[rows, :]
            lane = lax.broadcasted_iota(jnp.int32, (TOK, 128), 1)
            tile = narrow
            stats = (
                mrow[0, rows, :], mrow[1, rows, :],
                jnp.broadcast_to(wide[:, 192:193], (TOK, 128)), jnp.broadcast_to(narrow[:, 64:65], (TOK, 128)),
            )
            at = 64
            for stat in stats:
                for piece in split3(stat):
                    tile = jnp.where(lane == at, piece, tile)
                    at += 1
            tile = jnp.where(lane >= at, 0.0, tile)
            part[b, :, 0:128] = wide[:, 0:128].astype(BF)
            part[b, :, 128:256] = tile.astype(BF)
            return carry

        lax.fori_loop(0, NY, step, 0)

    def merge():
        ob[y] = part[y]

        def stat(g, at):
            t = ob[g, :, 128:256].astype(F32)
            return t[:, at : at + 1] + t[:, at + 1 : at + 2] + t[:, at + 2 : at + 3]

        for head in range(2):
            factor = heads[head][6]
            ms = [stat(g, 64 + 3 * head) for g in range(NY)]
            top = jnp.maximum(jnp.maximum(ms[0], ms[1]), jnp.maximum(ms[2], ms[3]))
            lanes = slice(0, 128) if head == 0 else slice(128, 256)
            total = jnp.zeros((TOK, 1), F32)
            value_sum = jnp.zeros((TOK, 128), F32)
            for g in range(NY):
                share = jnp.exp2((ms[g] - top) * factor)
                total = total + share * stat(g, 70 + 3 * head)
                value_sum = value_sum + share * ob[g, :, lanes].astype(F32)
            att[x, :, lanes] = (value_sum / total).astype(BF)

    kvz(1)
    q_relay(1)
    dny(1)
    gvz(1)
    gvy(1, 0)
    kvz(2)
    q_relay(2)
    dny(2)
    gvz(2)
    gvy(2, 0)
    gvy(1, 1)
    gvy(1, 2)
    kvz(3)
    gvz(3)
    dnz(0)
    kvz(4)
    gvz(4)
    wait_recv(kvb.at[:, other], pk_r)
    scores(0)
    gvy(2, 1)
    gvy(2, 2)
    gvy(1, 3)
    gvy(1, 4)
    weigh(0)
    gvy(2, 3)
    gvy(2, 4)
    gvy(1, 5)
    dnz(1)
    scores(1)
    gvy(1, 6)
    gvy(2, 5)
    weigh(1)
    pack()
    for o in (2, 1, 3):
        peer = yat(o)
        send(part.at[peer], ob.at[y], o_s, o_r.at[o - 1], {"sp_1": peer})
    gvy(1, 7)
    gvy(2, 6)
    dnz(2)
    for o in (2, 1, 3):
        wait_recv(ob.at[yat(-o)], o_r.at[o - 1])
    merge()
    for o in (2, 1, 3):
        send(att.at[x], att.at[x], x_s, x_r.at[o - 1], {"tp": xat(o)})
    gvy(2, 7)
    dnz(3)
    load_ow.wait()
    load_res.wait()
    for o in (2, 1, 3):
        wait_recv(att.at[xat(-o)], x_r.at[o - 1])

    def project(n, ss):
        cols = pl.ds(pl.multiple_of(n * 256, 256), 256)
        total = resid[:, cols].astype(F32)
        for h in range(NX):
            total = total + jnp.dot(
                att[h, :, 0:192], ow[pl.ds(h * 192, 192), cols], preferred_element_type=F32
            )
        rounded = total.astype(BF)
        stream[:, cols] = rounded
        wide = rounded.astype(F32)
        return ss + jnp.sum(wide * wide, axis=1, keepdims=True)

    ss = lax.fori_loop(0, 8, project, jnp.zeros((TOK, 1), F32))
    scale = lax.rsqrt(ss * (1.0 / D) + 1e-06)

    def norm(n, carry):
        cols = pl.ds(pl.multiple_of(n * 256, 256), 256)
        scaled = stream[:, cols].astype(F32) * scale
        normed[:, cols] = (scaled * gain[:, cols].astype(F32)).astype(BF)
        return carry

    lax.fori_loop(0, 8, norm, 0)
    dnz(4)
    wait_recv(gv.at[:, :, other], pg_r)

    def up(lo, dst):
        def step(n, carry):
            cols = pl.ds(pl.multiple_of(n * 256, 256), 256)
            w = gv[:, :, :, lo : lo + 32, cols].reshape(D, 256)
            dst[:, cols] = jnp.dot(normed[...], w, preferred_element_type=F32).astype(BF)
            return carry

        lax.fori_loop(0, 3, step, 0)

    up(0, gate)
    send(gate.at[pl.ds(112, 16)], hp, h_s.at[0], h_r.at[0], device_of(after))
    send(gate.at[pl.ds(0, 16)], hn, h_s.at[1], h_r.at[1], device_of(before))
    up(32, value)
    wait_recv(hp, h_r.at[0])
    wait_recv(hn, h_r.at[1])

    row = lax.broadcasted_iota(jnp.int32, (TOK, 256), 0)
    for n in range(3):
        cols = slice(n * 256, n * 256 + 256)
        g = gate[:, cols].astype(F32)
        first = jnp.where(place > 0, hp[:, cols].astype(F32)[15:16], 0.0)
        last = jnp.where(place < 63, hn[:, cols].astype(F32)[0:1], 0.0)
        low = jnp.where(row == 0, first, pltpu.roll(g, 1, 0))
        high = jnp.where(row == TOK - 1, last, pltpu.roll(g, TOK - 1, 0))
        cw = conv_w[:, cols].astype(F32)
        mixed = low * cw[0:1] + g * cw[1:2] + high * cw[2:3]
        silu = mixed / (1.0 + jnp.exp(-mixed))
        act[:, cols] = (silu * value[:, cols].astype(F32)).astype(BF)

    wait_recv(dn.at[:, :, other], pd_r)

    for half in range(2):

        def down(n, carry):
            w = dn[half * 4 + n].reshape(256, FFD)
            d = lax.dot_general(act[...], w, (((1,), (1,)), ((), ())), preferred_element_type=F32)
            cols = pl.ds(pl.multiple_of(n * 256, 256), 256)
            fp[half, :, :, cols] = d.astype(BF).reshape(NX, 32, 256)
            return carry

        lax.fori_loop(0, 4, down, 0)
        for o in (2, 1, 3):
            peer = xat(o)
            send(fp.at[half, peer], fr.at[half, x], f_s, f_r.at[half, o - 1], {"tp": peer})

    for half in range(2):
        cols = slice(half * 1024, half * 1024 + 1024)
        rows = pl.ds(pl.multiple_of(x * 32, 32), 32)
        total = stream[rows, cols].astype(F32) + fp[half, x].astype(F32)
        for o in (1, 3, 2):
            wait_recv(fr.at[half, xat(-o)], f_r.at[half, o - 1])
            total = total + fr[half, xat(-o)].astype(F32)
        out_ref[:, cols] = total.astype(BF)

    wait_send(kvb.at[pl.ds(0, 7), 0], kvz_s)
    wait_send(qb.at[pl.ds(0, 3)], q_s)
    wait_send(gv.at[pl.ds(0, 7), 0, 0], gvz_s)
    wait_send(gv.at[:, pl.ds(0, 3), 0], gvy_s)
    wait_send(dn.at[0, pl.ds(0, 3), 0], dny_s)
    wait_send(dn.at[pl.ds(0, 7), :, 0], dnz_s)
    wait_send(kvb.at[:, 0], pk_s)
    wait_send(gv.at[:, :, 0], pg_s)
    wait_send(dn.at[:, :, 0], pd_s)
    wait_send(part.at[pl.ds(0, 3)], o_s)
    wait_send(att.at[pl.ds(0, 3)], x_s)
    wait_send(hp, h_s.at[0])
    wait_send(hn, h_s.at[1])
    wait_send(fp.at[:, pl.ds(0, 3)], f_s)


def layer(q_own, kv_own, gv_own, dn_own, gain, conv_w, residual, out_weight):
    vmem = pl.BlockSpec(memory_space=pltpu.VMEM)
    hbm = pl.BlockSpec(memory_space=pltpu.HBM)
    dma = pltpu.SemaphoreType.DMA
    scratch = [
        pltpu.VMEM((NZ, 2, TOK, 512), BF),
        pltpu.VMEM((NY, TOK, 384), BF),
        pltpu.VMEM((NZ, NY, 2, 64, FFD), BF),
        pltpu.VMEM((NZ, NY, 2, 32, FFD), BF),
        pltpu.VMEM((768, D), BF),
        pltpu.VMEM((TOK, D), BF),
        pltpu.VMEM((NZ, 512, 256), F32),
        pltpu.VMEM((512, 128), F32),
        pltpu.VMEM((2, 512, 128), F32),
        pltpu.VMEM((512, 256), F32),
        pltpu.VMEM((512, 128), F32),
        pltpu.VMEM((NY, TOK, 256), BF),
        pltpu.VMEM((NY, TOK, 256), BF),
        pltpu.VMEM((NX, TOK, 256), BF),
        pltpu.VMEM((TOK, D), BF),
        pltpu.VMEM((TOK, D), BF),
        pltpu.VMEM((TOK, FFD), BF),
        pltpu.VMEM((TOK, FFD), BF),
        pltpu.VMEM((16, FFD), BF),
        pltpu.VMEM((16, FFD), BF),
        pltpu.VMEM((TOK, FFD), BF),
        pltpu.VMEM((2, NX, 32, 1024), BF),
        pltpu.VMEM((2, NX, 32, 1024), BF),
        dma, dma((2, 4)), dma, dma((2, 2)), dma, dma((2, 4)), dma, dma((2, 2, 8)),
        dma, dma((2, 2)), dma, dma((2, 4)),
        dma, dma, dma, dma, dma, dma, dma, dma((3,)), dma, dma((3,)), dma((2,)), dma((2,)),
        dma, dma((2, 3)), dma((2,)),
    ]
    return pl.pallas_call(
        kernel,
        out_shape=jax.ShapeDtypeStruct((32, D), BF),
        in_specs=[vmem] * 6 + [hbm] * 2,
        out_specs=vmem,
        scratch_shapes=scratch,
        compiler_params=pltpu.CompilerParams(collective_id=0, has_side_effects=True),
    )(q_own, kv_own, gv_own, dn_own, gain, conv_w, residual, out_weight)


def body(
    queries, latents, shared_key, expand_weight, residual, out_weight,
    norm_gain, gate_weight, value_weight, conv_weight, down_weight,
):
    rows = queries.shape[0]
    positions = lax.axis_index(SP) * rows + jnp.arange(rows, dtype=jnp.int32)
    cos_table, sine_table = tables(positions, ROPE)
    key_turned = rotate(shared_key, cos_table, sine_table)
    wide_turned = rotate(queries[:, 192:256], cos_table, sine_table)
    narrow_turned = rotate(queries[:, 256:320], cos_table, sine_table)
    pad = jnp.zeros((rows, 64), BF)
    q_own = jnp.concatenate([queries[:, 0:128], wide_turned, pad, narrow_turned, queries[:, 128:192]], axis=1)
    expanded = jnp.dot(latents, expand_weight, preferred_element_type=F32).astype(BF)
    kv_own = jnp.concatenate(
        [
            expanded[:, 0:128], key_turned, expanded[:, 256:320],
            expanded[:, 128:256], expanded[:, 320:384], jnp.ones((rows, 64), BF),
        ],
        axis=1,
    )
    gv_own = jnp.concatenate([gate_weight, value_weight], axis=0)
    dn_own = down_weight.T
    return layer(q_own, kv_own, gv_own, dn_own, norm_gain[None, :], conv_weight, residual, out_weight)


def solution(mesh):
    split = Mesh(mesh.devices.reshape(NZ, NY, 2, mesh.shape["tp"]), ("sp_0", "sp_1", "sp_2", "tp"))
    placed = (
        P(SP, "tp"),
        P(SP, None),
        P(SP, None),
        P(None, "tp"),
        P(SP, None),
        P(),
        P(),
        P(SP, "tp"),
        P(SP, "tp"),
        P(None, "tp"),
        P("tp", SP),
    )
    return jax.shard_map(
        body, mesh=split, in_specs=placed, out_specs=P(SP_TP, None), check_vma=False
    )
```

time: 233 us -> 83.8 us (0.36); the launches traced: 230 us -> 83.3 us
  waiting for transfers between devices: 144 us -> 0 us
  Pallas kernels: 0 us -> 71.8 us
  starting transfers between devices: 20.6 us -> 0 us
  matrix products: 19.6 us -> 1.13 us
  blocking collectives: 16.1 us -> 0 us
  between operations: 13.6 us -> 0.08 us
  other arithmetic: 8.33 us -> 2.61 us
    all_gather x2 -> x0, waiting for transfers between devices: 134 us -> none  [in_one_piece(): out, at, outs = (lax.all_gather(both, axis, axis=dim, tiled=True), 0, [])]
    pallas_call x0 -> x1, Pallas kernels: none -> 71.8 us  [layer(): pl.pallas_call(kernel, out_shape=jax.ShapeDtypeStruct((32, D), BF), in_sp...]
    dot_general x10 -> x1, matrix products: 19.6 us -> 1.13 us  [body(): jnp.dot(latents, expand_weight, preferred_element_type=F32).astype(BF)]
    all_to_all x2 -> x0, starting transfers between devices: 16.3 us -> none  [the longest x1 12.1 us: sent_to_all(): lax.all_to_all(jnp.broadcast_to(x[None], (length, *x.shape)), axis, 0, 0,...]
    all_gather x1 -> x0, blocking collectives: 10.2 us -> none  [body(): all_heads = lax.all_gather(attended, 'tp', axis=1, tiled=True)]
    all_to_all x2 -> x0, waiting for transfers between devices: 9.1 us -> none  [the longest x1 9.1 us: sent_and_summed(): lax.all_to_all(pieces, axis, split_axis=0, concat_axis=0, tiled=True)]
    all_to_all x1 -> x0, blocking collectives: 5.9 us -> none  [sent_to_all(): lax.all_to_all(jnp.broadcast_to(x[None], (length, *x.shape)), axis, 0, 0,...]
    ppermute x2 -> x0, starting transfers between devices: 4.32 us -> none  [the longest x1 2.33 us: padded_2(): lax.ppermute(lax.slice_in_dim(block, 0, width, axis=dim), axis, backward)]
  transfers between devices with their start and end apart: 6 -> 0, of which waited for: 3 -> 0; matrix products, arithmetic and copies ran while one was open for 10% -> 0% of each run, Pallas kernels for 0% -> 0%
where the time goes in v1:
time: 83.8 us; the launch traced here: 83.3 us
  Pallas kernels  71.8 us (86%)
  local copies, waits for them, and re-layouts  7.69 us (9%)
  other arithmetic  2.61 us (3%)
  matrix products  1.13 us (1%)
    pallas_call x1, Pallas kernels, layer(): pl.pallas_call(kernel, out_shape=jax.ShapeDtypeStruct((32, D), BF), in_sp...  71.8 us
    unnamed x10, local copies, waits for them, and re-layouts  2.4 us

profile of v1, /device:TPU:1, one launch (start us, length us, event | category | flops | bytes accessed | tf_op | source)
XLA Modules:
  0.0 83.3 jit_solution(16763265856676500580)
XLA Ops:
  0.0 0.0 copy-start
  0.0 1.3 %broadcast_in_dim.13.gain = bf16[1,2048]{1,0:T(2,128)(2,1)} reshape(bf16[2048]{0:T(1024)(128)(2,1)} %param.17) | data formatting | bytes 8192 | tf_op jit(solution)/shard_map/broadcast_in_dim | solution.py:529
  1.4 0.7 slice.47
  2.1 0.1 copy.33
  2.2 0.7 fusion.27
  2.9 0.1 copy.34
  3.1 0.1 copy.35
  3.2 0.8 slice.42
  3.9 0.1 copy.29
  4.1 0.8 fusion.26
  4.8 0.1 copy.31
  4.9 0.1 copy.32
  5.1 0.1 copy.30
  5.2 0.1 copy.21
  5.3 0.4 fusion.23
  5.7 0.8 concatenate.17.q_own
  6.4 0.0 copy-done
  6.5 1.1 %convolution_convert_fusion = bf16[128,384]{1,0:T(8,128)(2,1)S(1)} fusion(bf16[128,512]{1,0:T(8,128)(2,1)} %param.12, bf16[512,384]{1,0:T(8,128)(2,1)S(1)} %copy-done), kind=kOutput, calls=%fused_computation | convolution fusion | flops 50380800 | bytes 622592 | tf_op jit(solution)/shard_map/dot_general | solution.py:519
  7.6 0.1 fusion.24
  7.7 0.8 concatenate.18.kv_own
  8.5 1.5 %pad_maximum_fusion.gv_own = bf16[64,768]{1,0:T(8,128)(2,1)} fusion(bf16[32,768]{1,0:T(8,128)(2,1)} %param.19, bf16[32,768]{1,0:T(8,128)(2,1)} %param.18), kind=kLoop, calls=%fused_computation.1 | loop fusion | flops 196608 | bytes 196608 | tf_op jit(solution)/shard_map/concatenate | solution.py:527
  9.9 71.8 %shard_map.109 = bf16[32,2048]{1,0:T(8,128)(2,1)} custom-call(bf16[128,384]{1,0:T(8,128)(2,1)} %concatenate.17.q_own, bf16[128,512]{1,0:T(8,128)(2,1)} %concatenate.18.kv_own, bf16[64,768]{1,0:T(8,128)(2,1)} %pad_maximum_fusion.gv_own, bf16[32,768]{1,0:T(8,128)(2,1)} %bitcast.3, bf16[1,2048]{1,0:T(2,128)(2,1)} %broadcast_in_dim.13.gain, ...), custom_call_target="tpu_custom_call" | custom-call | tf_op jit(solution)/shard_map/pallas_call | solution.py:497
  81.8 1.6 %copy.37 = bf16[32,2048]{1,0:T(8,128)(2,1)} copy(bf16[32,2048]{1,0:T(8,128)(2,1)} %shard_map.109) | data formatting | bytes 262144
  (5 shorter events, 0.0 us)
Async XLA Ops:
  0.0 6.5 %copy-start = (bf16[512,384]{1,0:T(8,128)(2,1)S(1)}, bf16[512,384]{1,0:T(8,128)(2,1)}, u32[]{:S(2)}) copy-start(bf16[512,384]{1,0:T(8,128)(2,1)} %param.14) | copy-start | bytes 1179652

commit v2 on v1

--- a/solution.py
+++ b/solution.py
@@ -25,27 +25,6 @@
 BF = jnp.bfloat16
 
 
-def tables(positions, width):
-    half_width = width // 2
-    frequency = 10000.0 ** (-jnp.arange(half_width, dtype=jnp.float32) / half_width)
-    angles = positions.astype(jnp.float32)[:, None] * frequency[None, :]
-    return (jnp.cos(angles), jnp.sin(angles))
-
-
-def rotate(vectors, cos_table, sine_table):
-    half_width = vectors.shape[-1] // 2
-    first_half = vectors[:, :half_width].astype(jnp.float32)
-    second_half = vectors[:, half_width:].astype(jnp.float32)
-    turned = jnp.concatenate(
-        [
-            first_half * cos_table - second_half * sine_table,
-            second_half * cos_table + first_half * sine_table,
-        ],
-        axis=1,
-    )
-    return turned.astype(jnp.bfloat16)
-
-
 def split3(v):
     hi = v.astype(BF).astype(F32)
     rest = v - hi
@@ -54,9 +33,9 @@
 
 
 def kernel(
-    q_own, kv_own, gv_own, dn_own, gain, conv_w, resid_hbm, ow_hbm,
+    q_t, lat, key_t, ew, gate_own, value_own, dn_own, freq, gain, conv_w, resid_hbm, ow_hbm,
     out_ref,
-    kvb, qb, gv, dn, ow, resid, s_ref, macc, mrow, accw, accn,
+    kvb, qb, gv, dn, ow, resid, s_ref, p_ref, macc, mrow, accw, accn,
     part, ob, att, stream, normed, gate, value, hp, hn, act, fp, fr,
     kvz_s, kvz_r, q_s, q_r, gvz_s, gvz_r, gvy_s, gvy_r, dny_s, dny_r, dnz_s, dnz_r,
     pk_s, pk_r, pg_s, pg_r, pd_s, pd_r, o_s, o_r, x_s, x_r, h_s, h_r, f_s, f_r, loc,
@@ -106,6 +85,10 @@
     load_res = pltpu.make_async_copy(resid_hbm, resid, loc.at[1])
     load_res.start()
 
+    gv[z, y, c, 0:32] = gate_own[...]
+    gv[z, y, c, 32:64] = value_own[...]
+    dn[z, y, c] = dn_own[...]
+
     barrier = pltpu.get_barrier_semaphore()
     greeted = [
         partner, right_z, left_z, right_y, left_y, {"sp_1": yat(2)},
@@ -115,55 +98,87 @@
         pl.semaphore_signal(barrier, inc=1, device_id=dev, device_id_type=MESH)
     pl.semaphore_wait(barrier, len(greeted))
 
-    send(kv_own, kvb.at[z, c], kvz_s, kvz_r.at[0, 0], right_z)
-    send(kv_own, kvb.at[z, c], kvz_s, kvz_r.at[1, 0], left_z)
-    send(q_own, qb.at[y], q_s, q_r.at[0, 0], right_y)
-    send(q_own, qb.at[y], q_s, q_r.at[1, 0], left_y)
-    send(gv_own, gv.at[z, y, c], gvz_s, gvz_r.at[0, 0], right_z)
-    send(gv_own, gv.at[z, y, c], gvz_s, gvz_r.at[1, 0], left_z)
-    send(dn_own, dn.at[z, y, c], dny_s, dny_r.at[0, 0], right_y)
-    send(dn_own, dn.at[z, y, c], dny_s, dny_r.at[1, 0], left_y)
-    send(kv_own, kvb.at[z, c], pk_s, pk_r, partner)
-    send(gv_own, gv.at[z, y, c], gvy_s, gvy_r.at[0, 0, 0], right_y)
-    send(gv_own, gv.at[z, y, c], gvy_s, gvy_r.at[1, 0, 0], left_y)
-    send(gv_own, gv.at[z, y, c], pg_s, pg_r, partner)
-    kvb[z, c] = kv_own[...]
-    qb[y] = q_own[...]
-    gv[z, y, c] = gv_own[...]
-    dn[z, y, c] = dn_own[...]
+    own = gv.at[z, y, c]
+    send(own, own, gvz_s, gvz_r.at[0, 0], right_z)
+    send(own, own, gvz_s, gvz_r.at[1, 0], left_z)
+    send(dn.at[z, y, c], dn.at[z, y, c], dny_s, dny_r.at[0, 0], right_y)
+    send(dn.at[z, y, c], dn.at[z, y, c], dny_s, dny_r.at[1, 0], left_y)
+    send(own, own, gvy_s, gvy_r.at[0, 0, 0], right_y)
+    send(own, own, gvy_s, gvy_r.at[1, 0, 0], left_y)
+    send(own, own, pg_s, pg_r, partner)
+
+    position = (lax.broadcasted_iota(jnp.int32, (32, TOK), 1) + place * TOK).astype(F32)
+    angles = position * freq[...]
+    cosine, sine = jnp.cos(angles), jnp.sin(angles)
+
+    def turned(a, b):
+        a, b = a.astype(F32), b.astype(F32)
+        return [a * cosine - b * sine, b * cosine + a * sine]
+
+    def upright(pieces):
+        return jnp.transpose(jnp.concatenate(pieces, axis=0), (1, 0))
+
+    nothing = jnp.zeros((64, TOK), F32)
+    expanded = jnp.dot(lat[...], ew[...], preferred_element_type=F32)
+    key_rows = upright(turned(key_t[0:32, :], key_t[32:64, :]) + [nothing])
+    low_lane = lax.broadcasted_iota(jnp.int32, (TOK, 128), 1) < 64
+    swapped = pltpu.roll(expanded[:, 256:384], 64, 1)
+    kvb[0, 0, :, 0:128] = expanded[:, 0:128].astype(BF)
+    kvb[0, 0, :, 128:256] = jnp.where(low_lane, key_rows, swapped).astype(BF)
+    kvb[0, 0, :, 256:384] = expanded[:, 128:256].astype(BF)
+    kvb[0, 0, :, 384:512] = jnp.where(low_lane, swapped, 1.0).astype(BF)
+    qb[0, :, 0:128] = upright([q_t[0:128, :].astype(F32)]).astype(BF)
+    qb[0, :, 128:256] = upright(turned(q_t[192:224, :], q_t[224:256, :]) + [nothing]).astype(BF)
+    qb[0, :, 256:384] = upright(
+        turned(q_t[256:288, :], q_t[288:320, :]) + [q_t[128:192, :].astype(F32)]
+    ).astype(BF)
+
+    def rows_of(slot, h):
+        return kvb.at[slot, 0, pl.ds(64 * h, 64)]
+
+    def slot_of(s, ahead):
+        return 0 if s == 0 else 7 if s == 4 else 2 * s - 1 + ahead
+
+    def kv_out(s, h):
+        if s < 3 or h == 0:
+            send(rows_of(slot_of(s, 0), h), rows_of(slot_of(s + 1, 0), h), kvz_s, kvz_r.at[0, s, h], right_z)
+        if s < 3 or h == 1:
+            send(rows_of(slot_of(s, 1), h), rows_of(slot_of(s + 1, 1), h), kvz_s, kvz_r.at[1, s, h], left_z)
+
+    def kv_across(slot):
+        send(kvb.at[slot, 0], kvb.at[slot, 1], pk_s, pk_r.at[slot], partner)
+
+    def kvz(s, h):
+        if s < 4:
+            wait_recv(rows_of(slot_of(s, 0), h), kvz_r.at[0, s - 1, h])
+            wait_recv(rows_of(slot_of(s, 1), h), kvz_r.at[1, s - 1, h])
+            kv_out(s, h)
+            if h == 1:
+                kv_across(2 * s - 1)
+                kv_across(2 * s)
+        else:
+            wait_recv(rows_of(7, 0), kvz_r.at[0, 3, 0])
+            wait_recv(rows_of(7, 1), kvz_r.at[1, 3, 1])
+            kv_across(7)
+
+    def q_relay(s):
+        if s == 1:
+            wait_recv(qb.at[1], q_r.at[0, 0])
+            send(qb.at[1, pl.ds(0, 64)], qb.at[3, pl.ds(0, 64)], q_s, q_r.at[0, 1], right_y)
+            wait_recv(qb.at[2], q_r.at[1, 0])
+            send(qb.at[2, pl.ds(64, 64)], qb.at[3, pl.ds(64, 64)], q_s, q_r.at[1, 1], left_y)
+        else:
+            wait_recv(qb.at[3, pl.ds(0, 64)], q_r.at[0, 1])
+            wait_recv(qb.at[3, pl.ds(64, 64)], q_r.at[1, 1])
+
+    kv_out(0, 0)
+    kv_out(0, 1)
+    send(qb.at[0], qb.at[1], q_s, q_r.at[0, 0], right_y)
+    send(qb.at[0], qb.at[2], q_s, q_r.at[1, 0], left_y)
+    kv_across(0)
+    macc[...] = jnp.full((2, 512, 128), -3e38, F32)
 
     offsets = [0, -1, 1, -2, 2, -3, 3, 4]
-
-    def kvz(s):
-        lo, hi = zat(-s), zat(s)
-        if s < 4:
-            wait_recv(kvb.at[lo, c], kvz_r.at[0, s - 1])
-            if s < 3:
-                send(kvb.at[lo, c], kvb.at[lo, c], kvz_s, kvz_r.at[0, s], right_z)
-            else:
-                send(kvb.at[lo, c, pl.ds(0, 64)], kvb.at[lo, c, pl.ds(0, 64)], kvz_s, kvz_r.at[0, s], right_z)
-            wait_recv(kvb.at[hi, c], kvz_r.at[1, s - 1])
-            if s < 3:
-                send(kvb.at[hi, c], kvb.at[hi, c], kvz_s, kvz_r.at[1, s], left_z)
-            else:
-                send(kvb.at[hi, c, pl.ds(64, 64)], kvb.at[hi, c, pl.ds(64, 64)], kvz_s, kvz_r.at[1, s], left_z)
-            send(kvb.at[lo, c], kvb.at[lo, c], pk_s, pk_r, partner)
-            send(kvb.at[hi, c], kvb.at[hi, c], pk_s, pk_r, partner)
-        else:
-            wait_recv(kvb.at[lo, c, pl.ds(0, 64)], kvz_r.at[0, 3])
-            wait_recv(kvb.at[lo, c, pl.ds(64, 64)], kvz_r.at[1, 3])
-            send(kvb.at[lo, c], kvb.at[lo, c], pk_s, pk_r, partner)
-
-    def q_relay(s):
-        a, b, far = yat(-1), yat(1), yat(2)
-        if s == 1:
-            wait_recv(qb.at[a], q_r.at[0, 0])
-            send(qb.at[a, pl.ds(0, 64)], qb.at[a, pl.ds(0, 64)], q_s, q_r.at[0, 1], right_y)
-            wait_recv(qb.at[b], q_r.at[1, 0])
-            send(qb.at[b, pl.ds(64, 64)], qb.at[b, pl.ds(64, 64)], q_s, q_r.at[1, 1], left_y)
-        else:
-            wait_recv(qb.at[far, pl.ds(0, 64)], q_r.at[0, 1])
-            wait_recv(qb.at[far, pl.ds(64, 64)], q_r.at[1, 1])
 
     def gv_out(zz, j):
         block = gv.at[zz, y, c]
@@ -217,61 +232,54 @@
             wait_recv(dn.at[z, far, c, pl.ds(0, 16)], dny_r.at[0, 1])
             wait_recv(dn.at[z, far, c, pl.ds(16, 16)], dny_r.at[1, 1])
 
-    def dnz(s):
+    def dnz(s, r):
+        yy = yat((0, -1, 1, 2)[r])
         lo, hi = zat(-s), zat(s)
         if s == 0:
-            bundle = dn.at[z, :, c]
-            send(bundle, bundle, dnz_s, dnz_r.at[0, 0], right_z)
-            send(bundle, bundle, dnz_s, dnz_r.at[1, 0], left_z)
-            send(bundle, bundle, pd_s, pd_r, partner)
+            block = dn.at[z, yy, c]
+            send(block, block, dnz_s, dnz_r.at[0, 0, r], right_z)
+            send(block, block, dnz_s, dnz_r.at[1, 0, r], left_z)
         elif s < 4:
-            wait_recv(dn.at[lo, :, c], dnz_r.at[0, s - 1])
-            src = dn.at[lo, :, c] if s < 3 else dn.at[lo, pl.ds(0, 2), c]
-            send(src, src, dnz_s, dnz_r.at[0, s], right_z)
-            wait_recv(dn.at[hi, :, c], dnz_r.at[1, s - 1])
-            src = dn.at[hi, :, c] if s < 3 else dn.at[hi, pl.ds(2, 2), c]
-            send(src, src, dnz_s, dnz_r.at[1, s], left_z)
+            wait_recv(dn.at[lo, yy, c], dnz_r.at[0, s - 1, r])
+            src = dn.at[lo, yy, c] if s < 3 else dn.at[lo, yy, c, pl.ds(0, 16)]
+            send(src, src, dnz_s, dnz_r.at[0, s, r], right_z)
+            wait_recv(dn.at[hi, yy, c], dnz_r.at[1, s - 1, r])
+            src = dn.at[hi, yy, c] if s < 3 else dn.at[hi, yy, c, pl.ds(16, 16)]
+            send(src, src, dnz_s, dnz_r.at[1, s, r], left_z)
+        else:
+            wait_recv(dn.at[lo, yy, c, pl.ds(0, 16)], dnz_r.at[0, 3, r])
+            wait_recv(dn.at[lo, yy, c, pl.ds(16, 16)], dnz_r.at[1, 3, r])
+        if r == 3:
             send(dn.at[lo, :, c], dn.at[lo, :, c], pd_s, pd_r, partner)
-            send(dn.at[hi, :, c], dn.at[hi, :, c], pd_s, pd_r, partner)
-        else:
-            wait_recv(dn.at[lo, pl.ds(0, 2), c], dnz_r.at[0, 3])
-            wait_recv(dn.at[lo, pl.ds(2, 2), c], dnz_r.at[1, 3])
-            send(dn.at[lo, :, c], dn.at[lo, :, c], pd_s, pd_r, partner)
+            if 0 < s < 4:
+                send(dn.at[hi, :, c], dn.at[hi, :, c], pd_s, pd_r, partner)
 
     heads = (
         (0, 256, 0, 256, 256, 512, (NOPE_A + ROPE) ** (-0.5) * LOG2E, accw),
         (256, 384, 128, 256, 384, 512, (NOPE_B + ROPE) ** (-0.5) * LOG2E, accn),
     )
 
-    def scores(head):
-        q0, q1, k0, k1 = heads[head][:4]
-        macc[...] = jnp.full((512, 128), -3e38, F32)
-
-        def step(k, carry):
+    def scores(j):
+        wait_recv(kvb.at[j, 1], pk_r.at[j])
+        for head in range(2):
+            q0, q1, k0, k1 = heads[head][:4]
             qs = qb[:, :, q0:q1].reshape(512, q1 - q0)
-            ks = kvb[k, :, :, k0:k1].reshape(256, k1 - k0)
+            ks = kvb[j, :, :, k0:k1].reshape(256, k1 - k0)
             s = lax.dot_general(qs, ks, (((1,), (1,)), ((), ())), preferred_element_type=F32)
-            s_ref[k] = s
-            macc[...] = jnp.maximum(macc[...], jnp.maximum(s[:, :128], s[:, 128:]))
-            return carry
-
-        lax.fori_loop(0, NZ, step, 0)
+            s_ref[head, j] = s
+            macc[head] = jnp.maximum(macc[head], jnp.maximum(s[:, :128], s[:, 128:]))
 
     def weigh(head):
         v0, v1, factor, acc = heads[head][4:]
-        m = jnp.max(macc[...], axis=1, keepdims=True)
-        mrow[head] = jnp.broadcast_to(m, (512, 128))
-        acc[...] = jnp.zeros(acc.shape, F32)
-
-        def step(k, carry):
-            mb = mrow[head]
-            s = s_ref[k]
-            p = jnp.exp2((s - jnp.concatenate([mb, mb], axis=1)) * factor).astype(BF)
-            vs = kvb[k, :, :, v0:v1].reshape(256, v1 - v0)
-            acc[...] += jnp.dot(p, vs, preferred_element_type=F32)
-            return carry
-
-        lax.fori_loop(0, NZ, step, 0)
+        m = jnp.broadcast_to(jnp.max(macc[head], axis=1, keepdims=True), (512, 128))
+        mrow[head] = m
+        for j in range(NZ):
+            for half in range(2):
+                s = s_ref[head, j, :, half * 128 : half * 128 + 128]
+                at = j * 256 + half * 128
+                p_ref[head, :, at : at + 128] = jnp.exp2((s - m) * factor).astype(BF)
+        vs = kvb[:, :, :, v0:v1].reshape(2048, v1 - v0)
+        acc[...] = jnp.dot(p_ref[head], vs, preferred_element_type=F32)
 
     def pack():
         def step(b, carry):
@@ -296,7 +304,7 @@
         lax.fori_loop(0, NY, step, 0)
 
     def merge():
-        ob[y] = part[y]
+        ob[0] = part[0]
 
         def stat(g, at):
             t = ob[g, :, 128:256].astype(F32)
@@ -315,52 +323,84 @@
                 value_sum = value_sum + share * ob[g, :, lanes].astype(F32)
             att[x, :, lanes] = (value_sum / total).astype(BF)
 
-    kvz(1)
+    def part_out():
+        send(part.at[3], ob.at[3], o_s, o_r.at[2], {"sp_1": yat(2)})
+        send(part.at[1], ob.at[2], o_s, o_r.at[1], left_y)
+        send(part.at[2], ob.at[1], o_s, o_r.at[0], right_y)
+
+    def part_in():
+        for o in (1, 2, 3):
+            wait_recv(ob.at[o], o_r.at[o - 1])
+
+    def att_out():
+        for o in (2, 1, 3):
+            send(att.at[x], att.at[x], x_s, x_r.at[o - 1], {"tp": xat(o)})
+
+    dny(1)
+    gvy(1, 0)
+    gvz(1)
+    kvz(1, 0)
     q_relay(1)
-    dny(1)
-    gvz(1)
-    gvy(1, 0)
-    kvz(2)
+    dny(2)
+    kvz(1, 1)
+    gvy(2, 0)
+    gvz(2)
+    gvy(1, 1)
+    kvz(2, 0)
+    kvz(2, 1)
+    gvy(1, 2)
     q_relay(2)
-    dny(2)
-    gvz(2)
-    gvy(2, 0)
-    gvy(1, 1)
-    gvy(1, 2)
-    kvz(3)
+    scores(0)
+    scores(1)
+    scores(2)
     gvz(3)
-    dnz(0)
-    kvz(4)
+    scores(3)
+    scores(4)
+    gvy(1, 3)
+    kvz(3, 0)
+    kvz(3, 1)
+    dnz(0, 0)
+    dnz(0, 1)
+    dnz(0, 2)
+    gvy(1, 4)
+    dnz(0, 3)
     gvz(4)
-    wait_recv(kvb.at[:, other], pk_r)
-    scores(0)
     gvy(2, 1)
+    scores(5)
+    scores(6)
     gvy(2, 2)
-    gvy(1, 3)
-    gvy(1, 4)
+    kvz(4, 0)
+    gvy(1, 5)
+    dnz(1, 0)
+    scores(7)
     weigh(0)
+    gvy(1, 6)
     gvy(2, 3)
-    gvy(2, 4)
-    gvy(1, 5)
-    dnz(1)
-    scores(1)
-    gvy(1, 6)
-    gvy(2, 5)
+    dnz(1, 1)
+    dnz(1, 2)
+    dnz(1, 3)
     weigh(1)
     pack()
-    for o in (2, 1, 3):
-        peer = yat(o)
-        send(part.at[peer], ob.at[y], o_s, o_r.at[o - 1], {"sp_1": peer})
+    part_out()
+    gvy(2, 4)
+    dnz(2, 0)
     gvy(1, 7)
+    dnz(2, 1)
+    gvy(2, 5)
+    dnz(2, 2)
     gvy(2, 6)
-    dnz(2)
-    for o in (2, 1, 3):
-        wait_recv(ob.at[yat(-o)], o_r.at[o - 1])
+    dnz(2, 3)
+    dnz(3, 0)
+    part_in()
     merge()
-    for o in (2, 1, 3):
-        send(att.at[x], att.at[x], x_s, x_r.at[o - 1], {"tp": xat(o)})
+    att_out()
+    dnz(3, 1)
     gvy(2, 7)
-    dnz(3)
+    dnz(3, 2)
+    dnz(3, 3)
+    dnz(4, 0)
+    dnz(4, 1)
+    dnz(4, 2)
     load_ow.wait()
     load_res.wait()
     for o in (2, 1, 3):
@@ -388,7 +428,7 @@
         return carry
 
     lax.fori_loop(0, 8, norm, 0)
-    dnz(4)
+    dnz(4, 3)
     wait_recv(gv.at[:, :, other], pg_r)
 
     def up(lo, dst):
@@ -461,7 +501,7 @@
     wait_send(fp.at[:, pl.ds(0, 3)], f_s)
 
 
-def layer(q_own, kv_own, gv_own, dn_own, gain, conv_w, residual, out_weight):
+def layer(*operands):
     vmem = pl.BlockSpec(memory_space=pltpu.VMEM)
     hbm = pl.BlockSpec(memory_space=pltpu.HBM)
     dma = pltpu.SemaphoreType.DMA
@@ -472,8 +512,9 @@
         pltpu.VMEM((NZ, NY, 2, 32, FFD), BF),
         pltpu.VMEM((768, D), BF),
         pltpu.VMEM((TOK, D), BF),
-        pltpu.VMEM((NZ, 512, 256), F32),
-        pltpu.VMEM((512, 128), F32),
+        pltpu.VMEM((2, NZ, 512, 256), F32),
+        pltpu.VMEM((2, 512, 2048), BF),
+        pltpu.VMEM((2, 512, 128), F32),
         pltpu.VMEM((2, 512, 128), F32),
         pltpu.VMEM((512, 256), F32),
         pltpu.VMEM((512, 128), F32),
@@ -489,44 +530,31 @@
         pltpu.VMEM((TOK, FFD), BF),
         pltpu.VMEM((2, NX, 32, 1024), BF),
         pltpu.VMEM((2, NX, 32, 1024), BF),
-        dma, dma((2, 4)), dma, dma((2, 2)), dma, dma((2, 4)), dma, dma((2, 2, 8)),
-        dma, dma((2, 2)), dma, dma((2, 4)),
-        dma, dma, dma, dma, dma, dma, dma, dma((3,)), dma, dma((3,)), dma((2,)), dma((2,)),
+        dma, dma((2, 4, 2)), dma, dma((2, 2)), dma, dma((2, 4)), dma, dma((2, 2, 8)),
+        dma, dma((2, 2)), dma, dma((2, 4, 4)),
+        dma, dma((8,)), dma, dma, dma, dma, dma, dma((3,)), dma, dma((3,)), dma((2,)), dma((2,)),
         dma, dma((2, 3)), dma((2,)),
     ]
     return pl.pallas_call(
         kernel,
         out_shape=jax.ShapeDtypeStruct((32, D), BF),
-        in_specs=[vmem] * 6 + [hbm] * 2,
+        in_specs=[vmem] * 10 + [hbm] * 2,
         out_specs=vmem,
         scratch_shapes=scratch,
         compiler_params=pltpu.CompilerParams(collective_id=0, has_side_effects=True),
-    )(q_own, kv_own, gv_own, dn_own, gain, conv_w, residual, out_weight)
+    )(*operands)
 
 
 def body(
     queries, latents, shared_key, expand_weight, residual, out_weight,
     norm_gain, gate_weight, value_weight, conv_weight, down_weight,
 ):
-    rows = queries.shape[0]
-    positions = lax.axis_index(SP) * rows + jnp.arange(rows, dtype=jnp.int32)
-    cos_table, sine_table = tables(positions, ROPE)
-    key_turned = rotate(shared_key, cos_table, sine_table)
-    wide_turned = rotate(queries[:, 192:256], cos_table, sine_table)
-    narrow_turned = rotate(queries[:, 256:320], cos_table, sine_table)
-    pad = jnp.zeros((rows, 64), BF)
-    q_own = jnp.concatenate([queries[:, 0:128], wide_turned, pad, narrow_turned, queries[:, 128:192]], axis=1)
-    expanded = jnp.dot(latents, expand_weight, preferred_element_type=F32).astype(BF)
-    kv_own = jnp.concatenate(
-        [
-            expanded[:, 0:128], key_turned, expanded[:, 256:320],
-            expanded[:, 128:256], expanded[:, 320:384], jnp.ones((rows, 64), BF),
-        ],
-        axis=1,
+    frequency = 10000.0 ** (-jnp.arange(ROPE // 2, dtype=F32) / (ROPE // 2))
+    return layer(
+        queries.T, latents, shared_key.T, expand_weight, gate_weight, value_weight, down_weight.T,
+        jnp.broadcast_to(frequency[:, None], (ROPE // 2, TOK)), norm_gain[None, :], conv_weight,
+        residual, out_weight,
     )
-    gv_own = jnp.concatenate([gate_weight, value_weight], axis=0)
-    dn_own = down_weight.T
-    return layer(q_own, kv_own, gv_own, dn_own, norm_gain[None, :], conv_weight, residual, out_weight)
 
 
 def solution(mesh):

time: 83.8 us -> 70.7 us (0.84)
  Pallas kernels: 71.8 us -> 67 us
  local copies, waits for them, and re-layouts: 7.69 us -> 3.53 us
  other arithmetic: 2.61 us -> 0.01 us
  matrix products: 1.13 us -> 0 us
    pallas_call x1, Pallas kernels: 71.8 us -> 67 us  [layer(): pl.pallas_call(kernel, out_shape=jax.ShapeDtypeStruct((32, D), BF), in_sp...]
    slice x5 -> x0, local copies, waits for them, and re-layouts: 2.3 us -> none  [the longest x1 0.77 us: body(): queries[:, 0:128]]
    concatenate x2 -> x0, local copies, waits for them, and re-layouts: 1.54 us -> none  [the longest x1 0.78 us: body(): jnp.concatenate([expanded[:, 0:128], key_turned, expanded[:, 256:320], ex...]
    concatenate x1 -> x0, other arithmetic: 1.46 us -> none  [body(): gv_own = jnp.concatenate([gate_weight, value_weight], axis=0)]
    dot_general x1 -> x0, matrix products: 1.13 us -> none  [body(): jnp.dot(latents, expand_weight, preferred_element_type=F32).astype(BF)]
    unnamed x10 -> x1, local copies, waits for them, and re-layouts: 2.4 us -> 1.57 us
where the time goes in v2:
time: 70.7 us; the launch traced here: 70.6 us
  Pallas kernels  67 us (95%)
  local copies, waits for them, and re-layouts  3.53 us (5%)
    pallas_call x1, Pallas kernels, layer(): pl.pallas_call(kernel, out_shape=jax.ShapeDtypeStruct((32, D), BF), in_sp...  67 us
    unnamed x1, local copies, waits for them, and re-layouts  1.57 us

profile of v2, /device:TPU:1, one launch (start us, length us, event | category | flops | bytes accessed | tf_op | source)
XLA Modules:
  0.0 70.6 jit_solution(7706302704669802189)
XLA Ops:
  0.0 1.3 %broadcast_in_dim.10.gain = bf16[1,2048]{1,0:T(2,128)(2,1)} reshape(bf16[2048]{0:T(1024)(128)(2,1)} %param.17) | data formatting | bytes 8192 | tf_op jit(solution)/shard_map/broadcast_in_dim | solution.py:555
  1.3 0.7 broadcast_in_dim.4.freq
  2.0 67.0 %shard_map.109 = bf16[32,2048]{1,0:T(8,128)(2,1)} custom-call(bf16[320,128]{1,0:T(8,128)(2,1)} %bitcast.3, bf16[128,512]{1,0:T(8,128)(2,1)} %lat.1, bf16[64,128]{1,0:T(8,128)(2,1)} %bitcast.5, bf16[512,384]{1,0:T(8,128)(2,1)} %ew.1, bf16[32,768]{1,0:T(8,128)(2,1)} %gate_own.1, bf16[32,768]{1,0:T(8,128)(2,1)} %value_own.1, bf16[32,768]{1,0:T(8,128)(2,1)} %bitcast.4, ...), custom_call_target="tpu_custom_call" | custom-call | tf_op jit(solution)/shard_map/pallas_call | solution.py:538
  69.0 1.6 %copy.13 = bf16[32,2048]{1,0:T(8,128)(2,1)} copy(bf16[32,2048]{1,0:T(8,128)(2,1)} %shard_map.109) | data formatting | bytes 262144
  (1 shorter events, 0.0 us)

commit v3 on v2

--- a/solution.py
+++ b/solution.py
@@ -2,6 +2,7 @@
 
 import jax
 import jax.numpy as jnp
+import numpy as np
 from jax import lax
 from jax.experimental import pallas as pl
 from jax.experimental.pallas import tpu as pltpu
@@ -33,9 +34,9 @@
 
 
 def kernel(
-    q_t, lat, key_t, ew, gate_own, value_own, dn_own, freq, gain, conv_w, resid_hbm, ow_hbm,
+    gain, conv_w, q_hbm, lat_hbm, key_hbm, ew_hbm, gate_hbm, value_hbm, dn_hbm, freq_hbm, resid_hbm, ow_hbm,
     out_ref,
-    kvb, qb, gv, dn, ow, resid, s_ref, p_ref, macc, mrow, accw, accn,
+    q_t, lat, key_t, ew, freq, kvb, qb, gv, dn, ow, resid, s_ref, p_ref, macc, mrow, accw, accn,
     part, ob, att, stream, normed, gate, value, hp, hn, act, fp, fr,
     kvz_s, kvz_r, q_s, q_r, gvz_s, gvz_r, gvy_s, gvy_r, dny_s, dny_r, dnz_s, dnz_r,
     pk_s, pk_r, pg_s, pg_r, pd_s, pd_r, o_s, o_r, x_s, x_r, h_s, h_r, f_s, f_r, loc,
@@ -80,15 +81,6 @@
             src_ref=ref, dst_ref=ref, send_sem=sem, recv_sem=sem, device_id=partner, device_id_type=MESH
         ).wait_send()
 
-    load_ow = pltpu.make_async_copy(ow_hbm, ow, loc.at[0])
-    load_ow.start()
-    load_res = pltpu.make_async_copy(resid_hbm, resid, loc.at[1])
-    load_res.start()
-
-    gv[z, y, c, 0:32] = gate_own[...]
-    gv[z, y, c, 32:64] = value_own[...]
-    dn[z, y, c] = dn_own[...]
-
     barrier = pltpu.get_barrier_semaphore()
     greeted = [
         partner, right_z, left_z, right_y, left_y, {"sp_1": yat(2)},
@@ -96,16 +88,25 @@
     ]
     for dev in greeted:
         pl.semaphore_signal(barrier, inc=1, device_id=dev, device_id_type=MESH)
+
+    def load(src, dst, i):
+        copy = pltpu.make_async_copy(src, dst, loc.at[i])
+        copy.start()
+        return copy
+
+    first_loads = [
+        load(lat_hbm, lat, 0), load(ew_hbm, ew, 1), load(key_hbm, key_t, 2), load(freq_hbm, freq, 3),
+        load(q_hbm, q_t, 4),
+    ]
+    weight_loads = [
+        load(gate_hbm, gv.at[z, y, c, pl.ds(0, 32)], 5), load(value_hbm, gv.at[z, y, c, pl.ds(32, 32)], 6),
+        load(dn_hbm, dn.at[z, y, c], 7),
+    ]
+    load_res = load(resid_hbm, resid, 8)
+    load_ow = load(ow_hbm, ow, 9)
     pl.semaphore_wait(barrier, len(greeted))
-
-    own = gv.at[z, y, c]
-    send(own, own, gvz_s, gvz_r.at[0, 0], right_z)
-    send(own, own, gvz_s, gvz_r.at[1, 0], left_z)
-    send(dn.at[z, y, c], dn.at[z, y, c], dny_s, dny_r.at[0, 0], right_y)
-    send(dn.at[z, y, c], dn.at[z, y, c], dny_s, dny_r.at[1, 0], left_y)
-    send(own, own, gvy_s, gvy_r.at[0, 0, 0], right_y)
-    send(own, own, gvy_s, gvy_r.at[1, 0, 0], left_y)
-    send(own, own, pg_s, pg_r, partner)
+    for copy in first_loads:
+        copy.wait()
 
     position = (lax.broadcasted_iota(jnp.int32, (32, TOK), 1) + place * TOK).astype(F32)
     angles = position * freq[...]
@@ -177,6 +178,25 @@
     send(qb.at[0], qb.at[2], q_s, q_r.at[1, 0], left_y)
     kv_across(0)
     macc[...] = jnp.full((2, 512, 128), -3e38, F32)
+
+    def gvz_own():
+        own = gv.at[z, y, c]
+        send(own, own, gvz_s, gvz_r.at[0, 0], right_z)
+        send(own, own, gvz_s, gvz_r.at[1, 0], left_z)
+
+    def dny_own():
+        own = dn.at[z, y, c]
+        send(own, own, dny_s, dny_r.at[0, 0], right_y)
+        send(own, own, dny_s, dny_r.at[1, 0], left_y)
+
+    def gvy_own():
+        own = gv.at[z, y, c]
+        send(own, own, gvy_s, gvy_r.at[0, 0, 0], right_y)
+        send(own, own, gvy_s, gvy_r.at[1, 0, 0], left_y)
+        send(own, own, pg_s, pg_r, partner)
+
+    for copy in weight_loads:
+        copy.wait()
 
     offsets = [0, -1, 1, -2, 2, -3, 3, 4]
 
@@ -336,109 +356,102 @@
         for o in (2, 1, 3):
             send(att.at[x], att.at[x], x_s, x_r.at[o - 1], {"tp": xat(o)})
 
+    gvz_own()
+    dny_own()
+    gvy_own()
+    q_relay(1)
+    kvz(1, 0)
     dny(1)
+    kvz(1, 1)
     gvy(1, 0)
     gvz(1)
-    kvz(1, 0)
-    q_relay(1)
-    dny(2)
-    kvz(1, 1)
-    gvy(2, 0)
-    gvz(2)
-    gvy(1, 1)
-    kvz(2, 0)
-    kvz(2, 1)
-    gvy(1, 2)
     q_relay(2)
     scores(0)
     scores(1)
+    dny(2)
     scores(2)
-    gvz(3)
+    kvz(2, 0)
+    gvy(2, 0)
+    kvz(2, 1)
+    gvy(1, 1)
     scores(3)
     scores(4)
-    gvy(1, 3)
+    gvz(2)
     kvz(3, 0)
+    gvy(2, 1)
     kvz(3, 1)
+    dnz(0, 1)
     dnz(0, 0)
-    dnz(0, 1)
+    gvy(1, 2)
     dnz(0, 2)
-    gvy(1, 4)
-    dnz(0, 3)
-    gvz(4)
-    gvy(2, 1)
     scores(5)
     scores(6)
+    gvz(3)
+    kvz(4, 0)
+    gvy(1, 3)
+    dnz(0, 3)
     gvy(2, 2)
-    kvz(4, 0)
-    gvy(1, 5)
-    dnz(1, 0)
+    dnz(1, 1)
     scores(7)
     weigh(0)
-    gvy(1, 6)
-    gvy(2, 3)
-    dnz(1, 1)
-    dnz(1, 2)
-    dnz(1, 3)
     weigh(1)
     pack()
     part_out()
-    gvy(2, 4)
-    dnz(2, 0)
-    gvy(1, 7)
+    dnz(1, 2)
+    dnz(1, 0)
+    gvz(4)
+    gvy(1, 4)
+    gvy(1, 5)
+    gvy(1, 6)
+    dnz(1, 3)
+    gvy(2, 3)
     dnz(2, 1)
-    gvy(2, 5)
     dnz(2, 2)
-    gvy(2, 6)
-    dnz(2, 3)
-    dnz(3, 0)
     part_in()
     merge()
     att_out()
+    dnz(2, 0)
+    dnz(2, 3)
+    gvy(1, 7)
     dnz(3, 1)
-    gvy(2, 7)
+    gvy(2, 4)
     dnz(3, 2)
-    dnz(3, 3)
-    dnz(4, 0)
-    dnz(4, 1)
-    dnz(4, 2)
+    gvy(2, 5)
+    dnz(3, 0)
     load_ow.wait()
     load_res.wait()
     for o in (2, 1, 3):
         wait_recv(att.at[xat(-o)], x_r.at[o - 1])
 
-    def project(n, ss):
-        cols = pl.ds(pl.multiple_of(n * 256, 256), 256)
+    ss = jnp.zeros((TOK, 1), F32)
+    for n in range(8):
+        cols = slice(n * 256, n * 256 + 256)
         total = resid[:, cols].astype(F32)
         for h in range(NX):
-            total = total + jnp.dot(
-                att[h, :, 0:192], ow[pl.ds(h * 192, 192), cols], preferred_element_type=F32
-            )
+            total = total + jnp.dot(att[h, :, 0:192], ow[h * 192 : h * 192 + 192, cols], preferred_element_type=F32)
         rounded = total.astype(BF)
         stream[:, cols] = rounded
         wide = rounded.astype(F32)
-        return ss + jnp.sum(wide * wide, axis=1, keepdims=True)
-
-    ss = lax.fori_loop(0, 8, project, jnp.zeros((TOK, 1), F32))
+        ss = ss + jnp.sum(wide * wide, axis=1, keepdims=True)
     scale = lax.rsqrt(ss * (1.0 / D) + 1e-06)
-
-    def norm(n, carry):
-        cols = pl.ds(pl.multiple_of(n * 256, 256), 256)
+    for n in range(8):
+        cols = slice(n * 256, n * 256 + 256)
         scaled = stream[:, cols].astype(F32) * scale
-        normed[:, cols] = (scaled * gain[:, cols].astype(F32)).astype(BF)
-        return carry
-
-    lax.fori_loop(0, 8, norm, 0)
+        normed[:, cols] = (scaled * gain[cols].astype(F32).reshape(1, 256)).astype(BF)
+    gvy(2, 6)
+    dnz(3, 3)
+    gvy(2, 7)
+    dnz(4, 1)
+    dnz(4, 2)
+    dnz(4, 0)
     dnz(4, 3)
     wait_recv(gv.at[:, :, other], pg_r)
 
     def up(lo, dst):
-        def step(n, carry):
-            cols = pl.ds(pl.multiple_of(n * 256, 256), 256)
+        for n in range(3):
+            cols = slice(n * 256, n * 256 + 256)
             w = gv[:, :, :, lo : lo + 32, cols].reshape(D, 256)
             dst[:, cols] = jnp.dot(normed[...], w, preferred_element_type=F32).astype(BF)
-            return carry
-
-        lax.fori_loop(0, 3, step, 0)
 
     up(0, gate)
     send(gate.at[pl.ds(112, 16)], hp, h_s.at[0], h_r.at[0], device_of(after))
@@ -462,27 +475,21 @@
 
     wait_recv(dn.at[:, :, other], pd_r)
 
-    for half in range(2):
-
-        def down(n, carry):
-            w = dn[half * 4 + n].reshape(256, FFD)
-            d = lax.dot_general(act[...], w, (((1,), (1,)), ((), ())), preferred_element_type=F32)
-            cols = pl.ds(pl.multiple_of(n * 256, 256), 256)
-            fp[half, :, :, cols] = d.astype(BF).reshape(NX, 32, 256)
-            return carry
-
-        lax.fori_loop(0, 4, down, 0)
+    for n in range(NZ):
+        w = dn[n].reshape(256, FFD)
+        d = lax.dot_general(act[...], w, (((1,), (1,)), ((), ())), preferred_element_type=F32)
+        fp[n] = d.astype(BF).reshape(NX, 32, 256)
         for o in (2, 1, 3):
             peer = xat(o)
-            send(fp.at[half, peer], fr.at[half, x], f_s, f_r.at[half, o - 1], {"tp": peer})
-
-    for half in range(2):
-        cols = slice(half * 1024, half * 1024 + 1024)
-        rows = pl.ds(pl.multiple_of(x * 32, 32), 32)
-        total = stream[rows, cols].astype(F32) + fp[half, x].astype(F32)
+            send(fp.at[n, peer], fr.at[n, x], f_s, f_r.at[n, o - 1], {"tp": peer})
+
+    rows = pl.ds(pl.multiple_of(x * 32, 32), 32)
+    for n in range(NZ):
+        cols = slice(n * 256, n * 256 + 256)
+        total = stream[rows, cols].astype(F32) + fp[n, x].astype(F32)
         for o in (1, 3, 2):
-            wait_recv(fr.at[half, xat(-o)], f_r.at[half, o - 1])
-            total = total + fr[half, xat(-o)].astype(F32)
+            wait_recv(fr.at[n, xat(-o)], f_r.at[n, o - 1])
+            total = total + fr[n, xat(-o)].astype(F32)
         out_ref[:, cols] = total.astype(BF)
 
     wait_send(kvb.at[pl.ds(0, 7), 0], kvz_s)
@@ -506,6 +513,11 @@
     hbm = pl.BlockSpec(memory_space=pltpu.HBM)
     dma = pltpu.SemaphoreType.DMA
     scratch = [
+        pltpu.VMEM((320, TOK), BF),
+        pltpu.VMEM((TOK, 512), BF),
+        pltpu.VMEM((64, TOK), BF),
+        pltpu.VMEM((512, 384), BF),
+        pltpu.VMEM((32, TOK), F32),
         pltpu.VMEM((NZ, 2, TOK, 512), BF),
         pltpu.VMEM((NY, TOK, 384), BF),
         pltpu.VMEM((NZ, NY, 2, 64, FFD), BF),
@@ -528,17 +540,17 @@
         pltpu.VMEM((16, FFD), BF),
         pltpu.VMEM((16, FFD), BF),
         pltpu.VMEM((TOK, FFD), BF),
-        pltpu.VMEM((2, NX, 32, 1024), BF),
-        pltpu.VMEM((2, NX, 32, 1024), BF),
+        pltpu.VMEM((NZ, NX, 32, 256), BF),
+        pltpu.VMEM((NZ, NX, 32, 256), BF),
         dma, dma((2, 4, 2)), dma, dma((2, 2)), dma, dma((2, 4)), dma, dma((2, 2, 8)),
         dma, dma((2, 2)), dma, dma((2, 4, 4)),
         dma, dma((8,)), dma, dma, dma, dma, dma, dma((3,)), dma, dma((3,)), dma((2,)), dma((2,)),
-        dma, dma((2, 3)), dma((2,)),
+        dma, dma((NZ, 3)), dma((10,)),
     ]
     return pl.pallas_call(
         kernel,
-        out_shape=jax.ShapeDtypeStruct((32, D), BF),
-        in_specs=[vmem] * 10 + [hbm] * 2,
+        out_shape=pltpu.VMEM((32, D), BF),
+        in_specs=[vmem] * 2 + [hbm] * 10,
         out_specs=vmem,
         scratch_shapes=scratch,
         compiler_params=pltpu.CompilerParams(collective_id=0, has_side_effects=True),
@@ -549,10 +561,10 @@
     queries, latents, shared_key, expand_weight, residual, out_weight,
     norm_gain, gate_weight, value_weight, conv_weight, down_weight,
 ):
-    frequency = 10000.0 ** (-jnp.arange(ROPE // 2, dtype=F32) / (ROPE // 2))
+    frequency = (10000.0 ** (-np.arange(ROPE // 2) / (ROPE // 2))).astype(np.float32)
     return layer(
-        queries.T, latents, shared_key.T, expand_weight, gate_weight, value_weight, down_weight.T,
-        jnp.broadcast_to(frequency[:, None], (ROPE // 2, TOK)), norm_gain[None, :], conv_weight,
+        norm_gain, conv_weight, queries.T, latents, shared_key.T, expand_weight, gate_weight, value_weight,
+        down_weight.T, np.ascontiguousarray(np.broadcast_to(frequency[:, None], (ROPE // 2, TOK))),
         residual, out_weight,
     )
 

time: 70.7 us -> 64.6 us (0.914)
  Pallas kernels: 67 us -> 63.7 us
  local copies, waits for them, and re-layouts: 3.53 us -> 0.66 us
    pallas_call x1, Pallas kernels: 67 us -> 63.7 us  [layer(): pl.pallas_call(kernel, out_shape=pltpu.VMEM((32, D), BF), in_specs=[vmem]...]
    broadcast_in_dim x2 -> x0, local copies, waits for them, and re-layouts: 1.97 us -> none  [the longest x1 1.29 us: body(): norm_gain[None, :]]
    unnamed x1, local copies, waits for them, and re-layouts: 1.57 us -> 0.66 us
where the time goes in v3:
time: 64.6 us; the launch traced here: 64.4 us
  Pallas kernels  63.7 us (99%)
  local copies, waits for them, and re-layouts  0.66 us (1%)
    pallas_call x1, Pallas kernels, layer(): pl.pallas_call(kernel, out_shape=pltpu.VMEM((32, D), BF), in_specs=[vmem]...  63.7 us

profile of v3, /device:TPU:1, one launch (start us, length us, event | category | flops | bytes accessed | tf_op | source)
XLA Modules:
  0.0 64.4 jit_solution(11119220123317575980)
XLA Ops:
  0.0 63.7 %shard_map.118 = bf16[32,2048]{1,0:T(8,128)(2,1)S(1)} custom-call(bf16[2048]{0:T(1024)(128)(2,1)} %gain.1, bf16[3,768]{1,0:T(4,128)(2,1)} %conv_w.1, bf16[320,128]{1,0:T(8,128)(2,1)} %bitcast.3, bf16[128,512]{1,0:T(8,128)(2,1)} %lat_hbm.1, bf16[64,128]{1,0:T(8,128)(2,1)} %bitcast.5, bf16[512,384]{1,0:T(8,128)(2,1)} %ew_hbm.1, bf16[32,768]{1,0:T(8,128)(2,1)} %gate_hbm.1, ...), custom_call_target="tpu_custom_call" | custom-call | tf_op jit(solution)/shard_map/pallas_call | solution.py:550
  63.8 0.7 %copy.14 = bf16[32,2048]{1,0:T(8,128)(2,1)} copy(bf16[32,2048]{1,0:T(8,128)(2,1)S(1)} %shard_map.118) | data formatting | bytes 262144

commit v4 on v3

--- a/solution.py
+++ b/solution.py
@@ -18,6 +18,7 @@
 SP_TP = ("sp_0", "sp_1", "sp_2", "tp")
 NZ, NY, NX = 8, 4, 4
 TOK = 128
+ROWS = TOK + 32
 D = 2048
 FFD = 768
 MESH = pl.DeviceIdType.MESH
@@ -37,9 +38,9 @@
     gain, conv_w, q_hbm, lat_hbm, key_hbm, ew_hbm, gate_hbm, value_hbm, dn_hbm, freq_hbm, resid_hbm, ow_hbm,
     out_ref,
     q_t, lat, key_t, ew, freq, kvb, qb, gv, dn, ow, resid, s_ref, p_ref, macc, mrow, accw, accn,
-    part, ob, att, stream, normed, gate, value, hp, hn, act, fp, fr,
+    part, ob, att, stream, normed, gate, value, act, fp, fr,
     kvz_s, kvz_r, q_s, q_r, gvz_s, gvz_r, gvy_s, gvy_r, dny_s, dny_r, dnz_s, dnz_r,
-    pk_s, pk_r, pg_s, pg_r, pd_s, pd_r, o_s, o_r, x_s, x_r, h_s, h_r, f_s, f_r, loc,
+    pk_s, pk_r, pg_s, pg_r, pd_s, pd_r, o_s, o_r, x_s, x_r, e_s, e_r, h_s, h_r, f_s, f_r, loc,
 ):
     z = lax.axis_index("sp_0")
     y = lax.axis_index("sp_1")
@@ -84,8 +85,9 @@
     barrier = pltpu.get_barrier_semaphore()
     greeted = [
         partner, right_z, left_z, right_y, left_y, {"sp_1": yat(2)},
-        {"tp": xat(1)}, {"tp": xat(2)}, {"tp": xat(3)}, device_of(after), device_of(before),
+        {"tp": xat(1)}, {"tp": xat(2)}, {"tp": xat(3)},
     ]
+    greeted += [device_of(i) | {"tp": xat(o)} for i in (after, before) for o in range(NX)]
     for dev in greeted:
         pl.semaphore_signal(barrier, inc=1, device_id=dev, device_id_type=MESH)
 
@@ -102,7 +104,7 @@
         load(gate_hbm, gv.at[z, y, c, pl.ds(0, 32)], 5), load(value_hbm, gv.at[z, y, c, pl.ds(32, 32)], 6),
         load(dn_hbm, dn.at[z, y, c], 7),
     ]
-    load_res = load(resid_hbm, resid, 8)
+    load_res = load(resid_hbm, resid.at[pl.ds(0, TOK)], 8)
     load_ow = load(ow_hbm, ow, 9)
     pl.semaphore_wait(barrier, len(greeted))
     for copy in first_loads:
@@ -270,9 +272,9 @@
             wait_recv(dn.at[lo, yy, c, pl.ds(0, 16)], dnz_r.at[0, 3, r])
             wait_recv(dn.at[lo, yy, c, pl.ds(16, 16)], dnz_r.at[1, 3, r])
         if r == 3:
-            send(dn.at[lo, :, c], dn.at[lo, :, c], pd_s, pd_r, partner)
+            send(dn.at[lo, :, c], dn.at[lo, :, c], pd_s, pd_r.at[slot_of(s, 0)], partner)
             if 0 < s < 4:
-                send(dn.at[hi, :, c], dn.at[hi, :, c], pd_s, pd_r, partner)
+                send(dn.at[hi, :, c], dn.at[hi, :, c], pd_s, pd_r.at[slot_of(s, 1)], partner)
 
     heads = (
         (0, 256, 0, 256, 256, 512, (NOPE_A + ROPE) ** (-0.5) * LOG2E, accw),
@@ -341,7 +343,7 @@
                 share = jnp.exp2((ms[g] - top) * factor)
                 total = total + share * stat(g, 70 + 3 * head)
                 value_sum = value_sum + share * ob[g, :, lanes].astype(F32)
-            att[x, :, lanes] = (value_sum / total).astype(BF)
+            att[x, 0:TOK, lanes] = (value_sum / total).astype(BF)
 
     def part_out():
         send(part.at[3], ob.at[3], o_s, o_r.at[2], {"sp_1": yat(2)})
@@ -354,11 +356,19 @@
 
     def att_out():
         for o in (2, 1, 3):
-            send(att.at[x], att.at[x], x_s, x_r.at[o - 1], {"tp": xat(o)})
+            mine = att.at[x, pl.ds(0, TOK)]
+            send(mine, mine, x_s, x_r.at[o - 1], {"tp": xat(o)})
+        for o in range(NX):
+            peer = {"tp": xat(o)}
+            send(att.at[x, pl.ds(112, 16)], att.at[x, pl.ds(128, 16)], e_s, e_r.at[0, o], device_of(after) | peer)
+            send(att.at[x, pl.ds(0, 16)], att.at[x, pl.ds(144, 16)], e_s, e_r.at[1, o], device_of(before) | peer)
 
     gvz_own()
     dny_own()
     gvy_own()
+    load_res.wait()
+    send(resid.at[pl.ds(112, 16)], resid.at[pl.ds(128, 16)], h_s, h_r.at[0], device_of(after))
+    send(resid.at[pl.ds(0, 16)], resid.at[pl.ds(144, 16)], h_s, h_r.at[1], device_of(before))
     q_relay(1)
     kvz(1, 0)
     dny(1)
@@ -419,11 +429,15 @@
     gvy(2, 5)
     dnz(3, 0)
     load_ow.wait()
-    load_res.wait()
+    wait_recv(resid.at[pl.ds(128, 16)], h_r.at[0])
+    wait_recv(resid.at[pl.ds(144, 16)], h_r.at[1])
     for o in (2, 1, 3):
-        wait_recv(att.at[xat(-o)], x_r.at[o - 1])
-
-    ss = jnp.zeros((TOK, 1), F32)
+        wait_recv(att.at[xat(-o), pl.ds(0, TOK)], x_r.at[o - 1])
+    for o in range(NX):
+        wait_recv(att.at[xat(-o), pl.ds(128, 16)], e_r.at[0, o])
+        wait_recv(att.at[xat(-o), pl.ds(144, 16)], e_r.at[1, o])
+
+    ss = jnp.zeros((ROWS, 1), F32)
     for n in range(8):
         cols = slice(n * 256, n * 256 + 256)
         total = resid[:, cols].astype(F32)
@@ -441,31 +455,24 @@
     gvy(2, 6)
     dnz(3, 3)
     gvy(2, 7)
-    dnz(4, 1)
-    dnz(4, 2)
-    dnz(4, 0)
-    dnz(4, 3)
     wait_recv(gv.at[:, :, other], pg_r)
 
-    def up(lo, dst):
+    def up(lo, rows, dst):
         for n in range(3):
             cols = slice(n * 256, n * 256 + 256)
             w = gv[:, :, :, lo : lo + 32, cols].reshape(D, 256)
-            dst[:, cols] = jnp.dot(normed[...], w, preferred_element_type=F32).astype(BF)
-
-    up(0, gate)
-    send(gate.at[pl.ds(112, 16)], hp, h_s.at[0], h_r.at[0], device_of(after))
-    send(gate.at[pl.ds(0, 16)], hn, h_s.at[1], h_r.at[1], device_of(before))
-    up(32, value)
-    wait_recv(hp, h_r.at[0])
-    wait_recv(hn, h_r.at[1])
+            dst[:, cols] = jnp.dot(normed[0:rows], w, preferred_element_type=F32).astype(BF)
+
+    up(0, ROWS, gate)
+    up(32, TOK, value)
 
     row = lax.broadcasted_iota(jnp.int32, (TOK, 256), 0)
     for n in range(3):
         cols = slice(n * 256, n * 256 + 256)
-        g = gate[:, cols].astype(F32)
-        first = jnp.where(place > 0, hp[:, cols].astype(F32)[15:16], 0.0)
-        last = jnp.where(place < 63, hn[:, cols].astype(F32)[0:1], 0.0)
+        g = gate[0:TOK, cols].astype(F32)
+        edge = gate[TOK:ROWS, cols].astype(F32)
+        first = jnp.where(place > 0, edge[15:16], 0.0)
+        last = jnp.where(place < 63, edge[16:17], 0.0)
         low = jnp.where(row == 0, first, pltpu.roll(g, 1, 0))
         high = jnp.where(row == TOK - 1, last, pltpu.roll(g, TOK - 1, 0))
         cw = conv_w[:, cols].astype(F32)
@@ -473,23 +480,26 @@
         silu = mixed / (1.0 + jnp.exp(-mixed))
         act[:, cols] = (silu * value[:, cols].astype(F32)).astype(BF)
 
-    wait_recv(dn.at[:, :, other], pd_r)
-
-    for n in range(NZ):
-        w = dn[n].reshape(256, FFD)
+    for j in range(NZ):
+        zz = zat(offsets[j])
+        if j == 7:
+            for r in range(NY):
+                dnz(4, r)
+        wait_recv(dn.at[zz, :, other], pd_r.at[j])
+        w = dn[zz].reshape(256, FFD)
         d = lax.dot_general(act[...], w, (((1,), (1,)), ((), ())), preferred_element_type=F32)
-        fp[n] = d.astype(BF).reshape(NX, 32, 256)
+        fp[j] = d.astype(BF).reshape(NX, 32, 256)
         for o in (2, 1, 3):
             peer = xat(o)
-            send(fp.at[n, peer], fr.at[n, x], f_s, f_r.at[n, o - 1], {"tp": peer})
+            send(fp.at[j, peer], fr.at[j, x], f_s, f_r.at[j, o - 1], {"tp": peer})
 
     rows = pl.ds(pl.multiple_of(x * 32, 32), 32)
-    for n in range(NZ):
-        cols = slice(n * 256, n * 256 + 256)
-        total = stream[rows, cols].astype(F32) + fp[n, x].astype(F32)
+    for j in range(NZ):
+        cols = pl.ds(pl.multiple_of(zat(offsets[j]) * 256, 256), 256)
+        total = stream[rows, cols].astype(F32) + fp[j, x].astype(F32)
         for o in (1, 3, 2):
-            wait_recv(fr.at[n, xat(-o)], f_r.at[n, o - 1])
-            total = total + fr[n, xat(-o)].astype(F32)
+            wait_recv(fr.at[j, xat(-o)], f_r.at[j, o - 1])
+            total = total + fr[j, xat(-o)].astype(F32)
         out_ref[:, cols] = total.astype(BF)
 
     wait_send(kvb.at[pl.ds(0, 7), 0], kvz_s)
@@ -502,9 +512,9 @@
     wait_send(gv.at[:, :, 0], pg_s)
     wait_send(dn.at[:, :, 0], pd_s)
     wait_send(part.at[pl.ds(0, 3)], o_s)
-    wait_send(att.at[pl.ds(0, 3)], x_s)
-    wait_send(hp, h_s.at[0])
-    wait_send(hn, h_s.at[1])
+    wait_send(att.at[pl.ds(0, 3), pl.ds(0, TOK)], x_s)
+    wait_send(att.at[:, pl.ds(0, 32)], e_s)
+    wait_send(resid.at[pl.ds(0, 32)], h_s)
     wait_send(fp.at[:, pl.ds(0, 3)], f_s)
 
 
@@ -523,7 +533,7 @@
         pltpu.VMEM((NZ, NY, 2, 64, FFD), BF),
         pltpu.VMEM((NZ, NY, 2, 32, FFD), BF),
         pltpu.VMEM((768, D), BF),
-        pltpu.VMEM((TOK, D), BF),
+        pltpu.VMEM((ROWS, D), BF),
         pltpu.VMEM((2, NZ, 512, 256), F32),
         pltpu.VMEM((2, 512, 2048), BF),
         pltpu.VMEM((2, 512, 128), F32),
@@ -532,19 +542,17 @@
         pltpu.VMEM((512, 128), F32),
         pltpu.VMEM((NY, TOK, 256), BF),
         pltpu.VMEM((NY, TOK, 256), BF),
-        pltpu.VMEM((NX, TOK, 256), BF),
-        pltpu.VMEM((TOK, D), BF),
-        pltpu.VMEM((TOK, D), BF),
+        pltpu.VMEM((NX, ROWS, 256), BF),
+        pltpu.VMEM((ROWS, D), BF),
+        pltpu.VMEM((ROWS, D), BF),
+        pltpu.VMEM((ROWS, FFD), BF),
         pltpu.VMEM((TOK, FFD), BF),
-        pltpu.VMEM((TOK, FFD), BF),
-        pltpu.VMEM((16, FFD), BF),
-        pltpu.VMEM((16, FFD), BF),
         pltpu.VMEM((TOK, FFD), BF),
         pltpu.VMEM((NZ, NX, 32, 256), BF),
         pltpu.VMEM((NZ, NX, 32, 256), BF),
         dma, dma((2, 4, 2)), dma, dma((2, 2)), dma, dma((2, 4)), dma, dma((2, 2, 8)),
         dma, dma((2, 2)), dma, dma((2, 4, 4)),
-        dma, dma((8,)), dma, dma, dma, dma, dma, dma((3,)), dma, dma((3,)), dma((2,)), dma((2,)),
+        dma, dma((8,)), dma, dma, dma, dma((8,)), dma, dma((3,)), dma, dma((3,)), dma, dma((2, 4)), dma, dma((2,)),
         dma, dma((NZ, 3)), dma((10,)),
     ]
     return pl.pallas_call(

time: 64.6 us -> 63.2 us (0.978)
  Pallas kernels: 63.7 us -> 62.4 us
    pallas_call x1, Pallas kernels: 63.7 us -> 62.4 us  [layer(): pl.pallas_call(kernel, out_shape=pltpu.VMEM((32, D), BF), in_specs=[vmem]...]
where the time goes in v4:
time: 63.2 us; the launch traced here: 63 us
  Pallas kernels  62.4 us (99%)
  local copies, waits for them, and re-layouts  0.66 us (1%)
    pallas_call x1, Pallas kernels, layer(): pl.pallas_call(kernel, out_shape=pltpu.VMEM((32, D), BF), in_specs=[vmem]...  62.4 us

profile of v4, /device:TPU:1, one launch (start us, length us, event | category | flops | bytes accessed | tf_op | source)
XLA Modules:
  0.0 63.0 jit_solution(1964818965277036335)
XLA Ops:
  0.0 62.4 %shard_map.118 = bf16[32,2048]{1,0:T(8,128)(2,1)S(1)} custom-call(bf16[2048]{0:T(1024)(128)(2,1)} %gain.1, bf16[3,768]{1,0:T(4,128)(2,1)} %conv_w.1, bf16[320,128]{1,0:T(8,128)(2,1)} %bitcast.3, bf16[128,512]{1,0:T(8,128)(2,1)} %lat_hbm.1, bf16[64,128]{1,0:T(8,128)(2,1)} %bitcast.5, bf16[512,384]{1,0:T(8,128)(2,1)} %ew_hbm.1, bf16[32,768]{1,0:T(8,128)(2,1)} %gate_hbm.1, ...), custom_call_target="tpu_custom_call" | custom-call | tf_op jit(solution)/shard_map/pallas_call | solution.py:558
  62.4 0.7 %copy.14 = bf16[32,2048]{1,0:T(8,128)(2,1)} copy(bf16[32,2048]{1,0:T(8,128)(2,1)S(1)} %shard_map.118) | data formatting | bytes 262144

commit v5 on v4

--- a/solution.py
+++ b/solution.py
@@ -38,7 +38,7 @@
     gain, conv_w, q_hbm, lat_hbm, key_hbm, ew_hbm, gate_hbm, value_hbm, dn_hbm, freq_hbm, resid_hbm, ow_hbm,
     out_ref,
     q_t, lat, key_t, ew, freq, kvb, qb, gv, dn, ow, resid, s_ref, p_ref, macc, mrow, accw, accn,
-    part, ob, att, stream, normed, gate, value, act, fp, fr,
+    part, ob, att, stream, normed, gacc, vacc, gate, value, act, fp, fr,
     kvz_s, kvz_r, q_s, q_r, gvz_s, gvz_r, gvy_s, gvy_r, dny_s, dny_r, dnz_s, dnz_r,
     pk_s, pk_r, pg_s, pg_r, pd_s, pd_r, o_s, o_r, x_s, x_r, e_s, e_r, h_s, h_r, f_s, f_r, loc,
 ):
@@ -130,22 +130,22 @@
     kvb[0, 0, :, 128:256] = jnp.where(low_lane, key_rows, swapped).astype(BF)
     kvb[0, 0, :, 256:384] = expanded[:, 128:256].astype(BF)
     kvb[0, 0, :, 384:512] = jnp.where(low_lane, swapped, 1.0).astype(BF)
-    qb[0, :, 0:128] = upright([q_t[0:128, :].astype(F32)]).astype(BF)
-    qb[0, :, 128:256] = upright(turned(q_t[192:224, :], q_t[224:256, :]) + [nothing]).astype(BF)
-    qb[0, :, 256:384] = upright(
+    qb[3, :, 0:128] = upright([q_t[0:128, :].astype(F32)]).astype(BF)
+    qb[3, :, 128:256] = upright(turned(q_t[192:224, :], q_t[224:256, :]) + [nothing]).astype(BF)
+    qb[3, :, 256:384] = upright(
         turned(q_t[256:288, :], q_t[288:320, :]) + [q_t[128:192, :].astype(F32)]
     ).astype(BF)
 
     def rows_of(slot, h):
-        return kvb.at[slot, 0, pl.ds(64 * h, 64)]
+        return kvb.at[slot, 0, pl.ds(32 * h, 32)]
 
     def slot_of(s, ahead):
         return 0 if s == 0 else 7 if s == 4 else 2 * s - 1 + ahead
 
     def kv_out(s, h):
-        if s < 3 or h == 0:
+        if s < 3 or h < 2:
             send(rows_of(slot_of(s, 0), h), rows_of(slot_of(s + 1, 0), h), kvz_s, kvz_r.at[0, s, h], right_z)
-        if s < 3 or h == 1:
+        if s < 3 or h >= 2:
             send(rows_of(slot_of(s, 1), h), rows_of(slot_of(s + 1, 1), h), kvz_s, kvz_r.at[1, s, h], left_z)
 
     def kv_across(slot):
@@ -156,28 +156,28 @@
             wait_recv(rows_of(slot_of(s, 0), h), kvz_r.at[0, s - 1, h])
             wait_recv(rows_of(slot_of(s, 1), h), kvz_r.at[1, s - 1, h])
             kv_out(s, h)
-            if h == 1:
+            if h == 3:
                 kv_across(2 * s - 1)
                 kv_across(2 * s)
         else:
-            wait_recv(rows_of(7, 0), kvz_r.at[0, 3, 0])
-            wait_recv(rows_of(7, 1), kvz_r.at[1, 3, 1])
+            for q in range(4):
+                wait_recv(rows_of(7, q), kvz_r.at[q // 2, 3, q])
             kv_across(7)
 
     def q_relay(s):
         if s == 1:
             wait_recv(qb.at[1], q_r.at[0, 0])
-            send(qb.at[1, pl.ds(0, 64)], qb.at[3, pl.ds(0, 64)], q_s, q_r.at[0, 1], right_y)
+            send(qb.at[1, pl.ds(0, 64)], qb.at[0, pl.ds(0, 64)], q_s, q_r.at[0, 1], right_y)
             wait_recv(qb.at[2], q_r.at[1, 0])
-            send(qb.at[2, pl.ds(64, 64)], qb.at[3, pl.ds(64, 64)], q_s, q_r.at[1, 1], left_y)
+            send(qb.at[2, pl.ds(64, 64)], qb.at[0, pl.ds(64, 64)], q_s, q_r.at[1, 1], left_y)
         else:
-            wait_recv(qb.at[3, pl.ds(0, 64)], q_r.at[0, 1])
-            wait_recv(qb.at[3, pl.ds(64, 64)], q_r.at[1, 1])
-
-    kv_out(0, 0)
-    kv_out(0, 1)
-    send(qb.at[0], qb.at[1], q_s, q_r.at[0, 0], right_y)
-    send(qb.at[0], qb.at[2], q_s, q_r.at[1, 0], left_y)
+            wait_recv(qb.at[0, pl.ds(0, 64)], q_r.at[0, 1])
+            wait_recv(qb.at[0, pl.ds(64, 64)], q_r.at[1, 1])
+
+    for q in range(4):
+        kv_out(0, q)
+    send(qb.at[3], qb.at[1], q_s, q_r.at[0, 0], right_y)
+    send(qb.at[3], qb.at[2], q_s, q_r.at[1, 0], left_y)
     kv_across(0)
     macc[...] = jnp.full((2, 512, 128), -3e38, F32)
 
@@ -195,7 +195,7 @@
         own = gv.at[z, y, c]
         send(own, own, gvy_s, gvy_r.at[0, 0, 0], right_y)
         send(own, own, gvy_s, gvy_r.at[1, 0, 0], left_y)
-        send(own, own, pg_s, pg_r, partner)
+        send(own, own, pg_s, pg_r.at[0], partner)
 
     for copy in weight_loads:
         copy.wait()
@@ -206,7 +206,7 @@
         block = gv.at[zz, y, c]
         send(block, block, gvy_s, gvy_r.at[0, 0, j], right_y)
         send(block, block, gvy_s, gvy_r.at[1, 0, j], left_y)
-        send(block, block, pg_s, pg_r, partner)
+        send(block, block, pg_s, pg_r.at[j], partner)
 
     def gvz(s):
         lo, hi = zat(-s), zat(s)
@@ -234,12 +234,12 @@
             wait_recv(gv.at[zz, b, c], gvy_r.at[1, 0, j])
             src = gv.at[zz, b, c, pl.ds(32, 32)]
             send(src, src, gvy_s, gvy_r.at[1, 1, j], left_y)
-            send(gv.at[zz, a, c], gv.at[zz, a, c], pg_s, pg_r, partner)
-            send(gv.at[zz, b, c], gv.at[zz, b, c], pg_s, pg_r, partner)
+            send(gv.at[zz, a, c], gv.at[zz, a, c], pg_s, pg_r.at[j], partner)
+            send(gv.at[zz, b, c], gv.at[zz, b, c], pg_s, pg_r.at[j], partner)
         else:
             wait_recv(gv.at[zz, far, c, pl.ds(0, 32)], gvy_r.at[0, 1, j])
             wait_recv(gv.at[zz, far, c, pl.ds(32, 32)], gvy_r.at[1, 1, j])
-            send(gv.at[zz, far, c], gv.at[zz, far, c], pg_s, pg_r, partner)
+            send(gv.at[zz, far, c], gv.at[zz, far, c], pg_s, pg_r.at[j], partner)
 
     def dny(s):
         a, b, far = yat(-1), yat(1), yat(2)
@@ -271,10 +271,9 @@
         else:
             wait_recv(dn.at[lo, yy, c, pl.ds(0, 16)], dnz_r.at[0, 3, r])
             wait_recv(dn.at[lo, yy, c, pl.ds(16, 16)], dnz_r.at[1, 3, r])
-        if r == 3:
-            send(dn.at[lo, :, c], dn.at[lo, :, c], pd_s, pd_r.at[slot_of(s, 0)], partner)
-            if 0 < s < 4:
-                send(dn.at[hi, :, c], dn.at[hi, :, c], pd_s, pd_r.at[slot_of(s, 1)], partner)
+        send(dn.at[lo, yy, c], dn.at[lo, yy, c], pd_s, pd_r.at[slot_of(s, 0)], partner)
+        if 0 < s < 4:
+            send(dn.at[hi, yy, c], dn.at[hi, yy, c], pd_s, pd_r.at[slot_of(s, 1)], partner)
 
     heads = (
         (0, 256, 0, 256, 256, 512, (NOPE_A + ROPE) ** (-0.5) * LOG2E, accw),
@@ -291,23 +290,26 @@
             s_ref[head, j] = s
             macc[head] = jnp.maximum(macc[head], jnp.maximum(s[:, :128], s[:, 128:]))
 
-    def weigh(head):
-        v0, v1, factor, acc = heads[head][4:]
-        m = jnp.broadcast_to(jnp.max(macc[head], axis=1, keepdims=True), (512, 128))
-        mrow[head] = m
-        for j in range(NZ):
-            for half in range(2):
-                s = s_ref[head, j, :, half * 128 : half * 128 + 128]
-                at = j * 256 + half * 128
-                p_ref[head, :, at : at + 128] = jnp.exp2((s - m) * factor).astype(BF)
-        vs = kvb[:, :, :, v0:v1].reshape(2048, v1 - v0)
-        acc[...] = jnp.dot(p_ref[head], vs, preferred_element_type=F32)
-
-    def pack():
-        def step(b, carry):
-            rows = pl.ds(pl.multiple_of(b * TOK, TOK), TOK)
+    def weigh(half):
+        rows = slice(256 * half, 256 * half + 256)
+        for head in range(2):
+            v0, v1, factor, acc = heads[head][4:]
+            m = jnp.broadcast_to(jnp.max(macc[head, rows], axis=1, keepdims=True), (256, 128))
+            mrow[head, rows] = m
+            for j in range(NZ):
+                for side in range(2):
+                    s = s_ref[head, j, rows, side * 128 : side * 128 + 128]
+                    at = j * 256 + side * 128
+                    p_ref[head, :, at : at + 128] = jnp.exp2((s - m) * factor).astype(BF)
+            vs = kvb[:, :, :, v0:v1].reshape(2048, v1 - v0)
+            acc[rows] = jnp.dot(p_ref[head], vs, preferred_element_type=F32)
+
+    lane = lax.broadcasted_iota(jnp.int32, (TOK, 128), 1)
+
+    def pack(half):
+        for b in (2 * half, 2 * half + 1):
+            rows = slice(b * TOK, b * TOK + TOK)
             wide, narrow = accw[rows, :], accn[rows, :]
-            lane = lax.broadcasted_iota(jnp.int32, (TOK, 128), 1)
             tile = narrow
             stats = (
                 mrow[0, rows, :], mrow[1, rows, :],
@@ -321,38 +323,30 @@
             tile = jnp.where(lane >= at, 0.0, tile)
             part[b, :, 0:128] = wide[:, 0:128].astype(BF)
             part[b, :, 128:256] = tile.astype(BF)
-            return carry
-
-        lax.fori_loop(0, NY, step, 0)
+        if half == 0:
+            send(part.at[0], ob.at[0], o_s, o_r.at[0], {"sp_1": yat(2)})
+            send(part.at[1], ob.at[2], o_s, o_r.at[2], left_y)
+        else:
+            send(part.at[2], ob.at[1], o_s, o_r.at[1], right_y)
 
     def merge():
-        ob[0] = part[0]
-
-        def stat(g, at):
-            t = ob[g, :, 128:256].astype(F32)
-            return t[:, at : at + 1] + t[:, at + 1 : at + 2] + t[:, at + 2 : at + 3]
-
-        for head in range(2):
-            factor = heads[head][6]
-            ms = [stat(g, 64 + 3 * head) for g in range(NY)]
-            top = jnp.maximum(jnp.maximum(ms[0], ms[1]), jnp.maximum(ms[2], ms[3]))
-            lanes = slice(0, 128) if head == 0 else slice(128, 256)
-            total = jnp.zeros((TOK, 1), F32)
-            value_sum = jnp.zeros((TOK, 128), F32)
-            for g in range(NY):
-                share = jnp.exp2((ms[g] - top) * factor)
-                total = total + share * stat(g, 70 + 3 * head)
-                value_sum = value_sum + share * ob[g, :, lanes].astype(F32)
-            att[x, 0:TOK, lanes] = (value_sum / total).astype(BF)
-
-    def part_out():
-        send(part.at[3], ob.at[3], o_s, o_r.at[2], {"sp_1": yat(2)})
-        send(part.at[1], ob.at[2], o_s, o_r.at[1], left_y)
-        send(part.at[2], ob.at[1], o_s, o_r.at[0], right_y)
+        blocks = [part.at[3]] + [ob.at[g] for g in range(3)]
+        tiles = [block[:, 128:256].astype(F32) for block in blocks]
+        stats = [s + pltpu.roll(s, 127, 1) + pltpu.roll(s, 126, 1) for s in tiles]
+        top = jnp.maximum(jnp.maximum(stats[0], stats[1]), jnp.maximum(stats[2], stats[3]))
+        factor = jnp.where(lane == 64, heads[0][6], heads[1][6])
+        shares = [jnp.exp2((s - top) * factor) for s in stats]
+        total = sum(pltpu.roll(w, 6, 1) * s for w, s in zip(shares, stats))
+        inverse = pltpu.roll(1.0 / total, 122, 1)
+        shares = [w * inverse for w in shares]
+        wide = sum(w[:, 64:65] * block[:, 0:128].astype(F32) for w, block in zip(shares, blocks))
+        narrow = sum(w[:, 67:68] * s for w, s in zip(shares, tiles))
+        att[x, 0:TOK, 0:128] = wide.astype(BF)
+        att[x, 0:TOK, 128:256] = narrow.astype(BF)
 
     def part_in():
-        for o in (1, 2, 3):
-            wait_recv(ob.at[o], o_r.at[o - 1])
+        for o in range(3):
+            wait_recv(ob.at[o], o_r.at[o])
 
     def att_out():
         for o in (2, 1, 3):
@@ -363,71 +357,80 @@
             send(att.at[x, pl.ds(112, 16)], att.at[x, pl.ds(128, 16)], e_s, e_r.at[0, o], device_of(after) | peer)
             send(att.at[x, pl.ds(0, 16)], att.at[x, pl.ds(144, 16)], e_s, e_r.at[1, o], device_of(before) | peer)
 
+    def edges_out():
+        load_res.wait()
+        send(resid.at[pl.ds(112, 16)], resid.at[pl.ds(128, 16)], h_s, h_r.at[0], device_of(after))
+        send(resid.at[pl.ds(0, 16)], resid.at[pl.ds(144, 16)], h_s, h_r.at[1], device_of(before))
+
+    edges_out()
+    gvy_own()
     gvz_own()
+    kvz(1, 0)
+    q_relay(1)
+    kvz(1, 1)
     dny_own()
-    gvy_own()
-    load_res.wait()
-    send(resid.at[pl.ds(112, 16)], resid.at[pl.ds(128, 16)], h_s, h_r.at[0], device_of(after))
-    send(resid.at[pl.ds(0, 16)], resid.at[pl.ds(144, 16)], h_s, h_r.at[1], device_of(before))
-    q_relay(1)
-    kvz(1, 0)
-    dny(1)
-    kvz(1, 1)
+    kvz(1, 2)
+    kvz(1, 3)
     gvy(1, 0)
     gvz(1)
     q_relay(2)
     scores(0)
     scores(1)
+    kvz(2, 0)
+    scores(2)
+    dny(1)
+    kvz(2, 1)
+    kvz(2, 2)
+    gvy(2, 0)
+    kvz(2, 3)
+    scores(3)
+    gvz(2)
+    scores(4)
+    kvz(3, 0)
+    kvz(3, 1)
+    gvy(1, 2)
+    kvz(3, 2)
     dny(2)
-    scores(2)
-    kvz(2, 0)
-    gvy(2, 0)
-    kvz(2, 1)
     gvy(1, 1)
-    scores(3)
-    scores(4)
-    gvz(2)
-    kvz(3, 0)
-    gvy(2, 1)
-    kvz(3, 1)
+    kvz(3, 3)
+    dnz(0, 2)
+    dnz(0, 3)
+    dnz(0, 0)
+    scores(5)
+    gvz(3)
+    scores(6)
+    kvz(4, 0)
     dnz(0, 1)
-    dnz(0, 0)
-    gvy(1, 2)
-    dnz(0, 2)
-    scores(5)
-    scores(6)
-    gvz(3)
-    kvz(4, 0)
-    gvy(1, 3)
-    dnz(0, 3)
+    dnz(1, 2)
     gvy(2, 2)
-    dnz(1, 1)
     scores(7)
     weigh(0)
+    dnz(1, 0)
+    dnz(1, 3)
+    gvy(2, 1)
+    pack(0)
     weigh(1)
-    pack()
-    part_out()
-    dnz(1, 2)
-    dnz(1, 0)
+    pack(1)
     gvz(4)
+    gvy(1, 5)
+    dnz(1, 1)
+    gvy(1, 3)
     gvy(1, 4)
-    gvy(1, 5)
+    dnz(2, 2)
     gvy(1, 6)
-    dnz(1, 3)
-    gvy(2, 3)
-    dnz(2, 1)
-    dnz(2, 2)
+    dnz(2, 0)
+    dnz(2, 3)
     part_in()
     merge()
     att_out()
-    dnz(2, 0)
-    dnz(2, 3)
+    dnz(2, 1)
+    dnz(3, 2)
     gvy(1, 7)
+    dnz(3, 0)
+    gvy(2, 5)
+    dnz(3, 3)
+    gvy(2, 3)
     dnz(3, 1)
-    gvy(2, 4)
-    dnz(3, 2)
-    gvy(2, 5)
-    dnz(3, 0)
     load_ow.wait()
     wait_recv(resid.at[pl.ds(128, 16)], h_r.at[0])
     wait_recv(resid.at[pl.ds(144, 16)], h_r.at[1])
@@ -451,20 +454,38 @@
     for n in range(8):
         cols = slice(n * 256, n * 256 + 256)
         scaled = stream[:, cols].astype(F32) * scale
-        normed[:, cols] = (scaled * gain[cols].astype(F32).reshape(1, 256)).astype(BF)
+        normed[n] = (scaled * gain[cols].astype(F32).reshape(1, 256)).astype(BF)
+    gvy(2, 4)
     gvy(2, 6)
-    dnz(3, 3)
-    gvy(2, 7)
-    wait_recv(gv.at[:, :, other], pg_r)
-
-    def up(lo, rows, dst):
+
+    def up(lo, rows, js, acc, n):
+        cols = slice(n * 256, n * 256 + 256)
+        total = None
+        for j in js:
+            zz = zat(offsets[j])
+            w = gv[zz, :, :, lo : lo + 32, cols].reshape(256, 256)
+            term = jnp.dot(normed[zz, 0:rows], w, preferred_element_type=F32)
+            total = term if total is None else total + term
+        return total if acc is None else acc[:, cols] + total
+
+    def up_first():
+        for j in range(7):
+            wait_recv(gv.at[zat(offsets[j]), :, other], pg_r.at[j])
         for n in range(3):
             cols = slice(n * 256, n * 256 + 256)
-            w = gv[:, :, :, lo : lo + 32, cols].reshape(D, 256)
-            dst[:, cols] = jnp.dot(normed[0:rows], w, preferred_element_type=F32).astype(BF)
-
-    up(0, ROWS, gate)
-    up(32, TOK, value)
+            gacc[:, cols] = up(0, ROWS, range(7), None, n)
+            vacc[:, cols] = up(32, TOK, range(7), None, n)
+
+    def up_last():
+        wait_recv(gv.at[zat(offsets[7]), :, other], pg_r.at[7])
+        for n in range(3):
+            cols = slice(n * 256, n * 256 + 256)
+            gate[:, cols] = up(0, ROWS, (7,), gacc, n).astype(BF)
+            value[:, cols] = up(32, TOK, (7,), vacc, n).astype(BF)
+
+    up_first()
+    gvy(2, 7)
+    up_last()
 
     row = lax.broadcasted_iota(jnp.int32, (TOK, 256), 0)
     for n in range(3):
@@ -535,7 +556,7 @@
         pltpu.VMEM((768, D), BF),
         pltpu.VMEM((ROWS, D), BF),
         pltpu.VMEM((2, NZ, 512, 256), F32),
-        pltpu.VMEM((2, 512, 2048), BF),
+        pltpu.VMEM((2, 256, 2048), BF),
         pltpu.VMEM((2, 512, 128), F32),
         pltpu.VMEM((2, 512, 128), F32),
         pltpu.VMEM((512, 256), F32),
@@ -544,15 +565,17 @@
         pltpu.VMEM((NY, TOK, 256), BF),
         pltpu.VMEM((NX, ROWS, 256), BF),
         pltpu.VMEM((ROWS, D), BF),
-        pltpu.VMEM((ROWS, D), BF),
+        pltpu.VMEM((NZ, ROWS, 256), BF),
+        pltpu.VMEM((ROWS, FFD), F32),
+        pltpu.VMEM((TOK, FFD), F32),
         pltpu.VMEM((ROWS, FFD), BF),
         pltpu.VMEM((TOK, FFD), BF),
         pltpu.VMEM((TOK, FFD), BF),
         pltpu.VMEM((NZ, NX, 32, 256), BF),
         pltpu.VMEM((NZ, NX, 32, 256), BF),
-        dma, dma((2, 4, 2)), dma, dma((2, 2)), dma, dma((2, 4)), dma, dma((2, 2, 8)),
+        dma, dma((2, 4, 4)), dma, dma((2, 2)), dma, dma((2, 4)), dma, dma((2, 2, 8)),
         dma, dma((2, 2)), dma, dma((2, 4, 4)),
-        dma, dma((8,)), dma, dma, dma, dma((8,)), dma, dma((3,)), dma, dma((3,)), dma, dma((2, 4)), dma, dma((2,)),
+        dma, dma((8,)), dma, dma((8,)), dma, dma((8,)), dma, dma((3,)), dma, dma((3,)), dma, dma((2, 4)), dma, dma((2,)),
         dma, dma((NZ, 3)), dma((10,)),
     ]
     return pl.pallas_call(

time: 63.2 us -> 61.9 us (0.979)
  Pallas kernels: 62.4 us -> 61.1 us
    pallas_call x1, Pallas kernels: 62.4 us -> 61.1 us  [layer(): pl.pallas_call(kernel, out_shape=pltpu.VMEM((32, D), BF), in_specs=[vmem]...]
where the time goes in v5:
time: 61.9 us; the launch traced here: 61.8 us
  Pallas kernels  61.1 us (99%)
  local copies, waits for them, and re-layouts  0.66 us (1%)
    pallas_call x1, Pallas kernels, layer(): pl.pallas_call(kernel, out_shape=pltpu.VMEM((32, D), BF), in_specs=[vmem]...  61.1 us

profile of v5, /device:TPU:1, one launch (start us, length us, event | category | flops | bytes accessed | tf_op | source)
XLA Modules:
  0.0 61.8 jit_solution(9945040741403177380)
XLA Ops:
  0.0 61.1 %shard_map.118 = bf16[32,2048]{1,0:T(8,128)(2,1)S(1)} custom-call(bf16[2048]{0:T(1024)(128)(2,1)} %gain.1, bf16[3,768]{1,0:T(4,128)(2,1)} %conv_w.1, bf16[320,128]{1,0:T(8,128)(2,1)} %bitcast.3, bf16[128,512]{1,0:T(8,128)(2,1)} %lat_hbm.1, bf16[64,128]{1,0:T(8,128)(2,1)} %bitcast.5, bf16[512,384]{1,0:T(8,128)(2,1)} %ew_hbm.1, bf16[32,768]{1,0:T(8,128)(2,1)} %gate_hbm.1, ...), custom_call_target="tpu_custom_call" | custom-call | tf_op jit(solution)/shard_map/pallas_call | solution.py:581
  61.1 0.7 %copy.14 = bf16[32,2048]{1,0:T(8,128)(2,1)} copy(bf16[32,2048]{1,0:T(8,128)(2,1)S(1)} %shard_map.118) | data formatting | bytes 262144

commit v6 on v5

--- a/solution.py
+++ b/solution.py
@@ -35,9 +35,9 @@
 
 
 def kernel(
-    gain, conv_w, q_hbm, lat_hbm, key_hbm, ew_hbm, gate_hbm, value_hbm, dn_hbm, freq_hbm, resid_hbm, ow_hbm,
+    gain_hbm, conv_hbm, q_hbm, lat_hbm, key_hbm, ew_hbm, gate_hbm, value_hbm, dn_hbm, freq_hbm, resid_hbm, ow_hbm,
     out_ref,
-    q_t, lat, key_t, ew, freq, kvb, qb, gv, dn, ow, resid, s_ref, p_ref, macc, mrow, accw, accn,
+    gain, conv_w, q_t, lat, key_t, ew, freq, kvb, qb, gv, dn, ow, resid, s_ref, p_ref, macc, mrow, accw, accn,
     part, ob, att, stream, normed, gacc, vacc, gate, value, act, fp, fr,
     kvz_s, kvz_r, q_s, q_r, gvz_s, gvz_r, gvy_s, gvy_r, dny_s, dny_r, dnz_s, dnz_r,
     pk_s, pk_r, pg_s, pg_r, pd_s, pd_r, o_s, o_r, x_s, x_r, e_s, e_r, h_s, h_r, f_s, f_r, loc,
@@ -106,6 +106,8 @@
     ]
     load_res = load(resid_hbm, resid.at[pl.ds(0, TOK)], 8)
     load_ow = load(ow_hbm, ow, 9)
+    load_gain = load(gain_hbm, gain, 10)
+    load_conv = load(conv_hbm, conv_w, 11)
     pl.semaphore_wait(barrier, len(greeted))
     for copy in first_loads:
         copy.wait()
@@ -432,6 +434,8 @@
     gvy(2, 3)
     dnz(3, 1)
     load_ow.wait()
+    load_gain.wait()
+    load_conv.wait()
     wait_recv(resid.at[pl.ds(128, 16)], h_r.at[0])
     wait_recv(resid.at[pl.ds(144, 16)], h_r.at[1])
     for o in (2, 1, 3):
@@ -468,24 +472,18 @@
             total = term if total is None else total + term
         return total if acc is None else acc[:, cols] + total
 
-    def up_first():
-        for j in range(7):
-            wait_recv(gv.at[zat(offsets[j]), :, other], pg_r.at[j])
-        for n in range(3):
-            cols = slice(n * 256, n * 256 + 256)
-            gacc[:, cols] = up(0, ROWS, range(7), None, n)
-            vacc[:, cols] = up(32, TOK, range(7), None, n)
-
-    def up_last():
-        wait_recv(gv.at[zat(offsets[7]), :, other], pg_r.at[7])
-        for n in range(3):
-            cols = slice(n * 256, n * 256 + 256)
-            gate[:, cols] = up(0, ROWS, (7,), gacc, n).astype(BF)
-            value[:, cols] = up(32, TOK, (7,), vacc, n).astype(BF)
-
-    up_first()
+    for j in range(7):
+        wait_recv(gv.at[zat(offsets[j]), :, other], pg_r.at[j])
+    for n in range(3):
+        gacc[:, n * 256 : n * 256 + 256] = up(0, ROWS, range(7), None, n)
     gvy(2, 7)
-    up_last()
+    for n in range(3):
+        vacc[:, n * 256 : n * 256 + 256] = up(32, TOK, range(7), None, n)
+    wait_recv(gv.at[zat(offsets[7]), :, other], pg_r.at[7])
+    for n in range(3):
+        cols = slice(n * 256, n * 256 + 256)
+        gate[:, cols] = up(0, ROWS, (7,), gacc, n).astype(BF)
+        value[:, cols] = up(32, TOK, (7,), vacc, n).astype(BF)
 
     row = lax.broadcasted_iota(jnp.int32, (TOK, 256), 0)
     for n in range(3):
@@ -544,6 +542,8 @@
     hbm = pl.BlockSpec(memory_space=pltpu.HBM)
     dma = pltpu.SemaphoreType.DMA
     scratch = [
+        pltpu.VMEM((D,), BF),
+        pltpu.VMEM((3, FFD), BF),
         pltpu.VMEM((320, TOK), BF),
         pltpu.VMEM((TOK, 512), BF),
         pltpu.VMEM((64, TOK), BF),
@@ -576,12 +576,12 @@
         dma, dma((2, 4, 4)), dma, dma((2, 2)), dma, dma((2, 4)), dma, dma((2, 2, 8)),
         dma, dma((2, 2)), dma, dma((2, 4, 4)),
         dma, dma((8,)), dma, dma((8,)), dma, dma((8,)), dma, dma((3,)), dma, dma((3,)), dma, dma((2, 4)), dma, dma((2,)),
-        dma, dma((NZ, 3)), dma((10,)),
+        dma, dma((NZ, 3)), dma((12,)),
     ]
     return pl.pallas_call(
         kernel,
         out_shape=pltpu.VMEM((32, D), BF),
-        in_specs=[vmem] * 2 + [hbm] * 10,
+        in_specs=[hbm] * 12,
         out_specs=vmem,
         scratch_shapes=scratch,
         compiler_params=pltpu.CompilerParams(collective_id=0, has_side_effects=True),

time: 61.9 us -> 60.9 us (0.984)
  Pallas kernels: 61.1 us -> 60.1 us
    pallas_call x1, Pallas kernels: 61.1 us -> 60.1 us  [layer(): pl.pallas_call(kernel, out_shape=pltpu.VMEM((32, D), BF), in_specs=[hbm]...]
where the time goes in v6:
time: 60.9 us; the launch traced here: 60.8 us
  Pallas kernels  60.1 us (99%)
  local copies, waits for them, and re-layouts  0.66 us (1%)
    pallas_call x1, Pallas kernels, layer(): pl.pallas_call(kernel, out_shape=pltpu.VMEM((32, D), BF), in_specs=[hbm]...  60.1 us

profile of v6, /device:TPU:1, one launch (start us, length us, event | category | flops | bytes accessed | tf_op | source)
XLA Modules:
  0.0 60.8 jit_solution(12942712932253604550)
XLA Ops:
  0.0 60.1 %shard_map.118 = bf16[32,2048]{1,0:T(8,128)(2,1)S(1)} custom-call(bf16[2048]{0:T(1024)(128)(2,1)} %gain_hbm.1, bf16[3,768]{1,0:T(4,128)(2,1)} %conv_hbm.1, bf16[320,128]{1,0:T(8,128)(2,1)} %bitcast.3, bf16[128,512]{1,0:T(8,128)(2,1)} %lat_hbm.1, bf16[64,128]{1,0:T(8,128)(2,1)} %bitcast.5, bf16[512,384]{1,0:T(8,128)(2,1)} %ew_hbm.1, ...), custom_call_target="tpu_custom_call" | custom-call | tf_op jit(solution)/shard_map/pallas_call | solution.py:581
  60.1 0.7 %copy.14 = bf16[32,2048]{1,0:T(8,128)(2,1)} copy(bf16[32,2048]{1,0:T(8,128)(2,1)S(1)} %shard_map.118) | data formatting | bytes 262144

commit v7 on v6

--- a/solution.py
+++ b/solution.py
@@ -37,10 +37,9 @@
 def kernel(
     gain_hbm, conv_hbm, q_hbm, lat_hbm, key_hbm, ew_hbm, gate_hbm, value_hbm, dn_hbm, freq_hbm, resid_hbm, ow_hbm,
     out_ref,
-    gain, conv_w, q_t, lat, key_t, ew, freq, kvb, qb, gv, dn, ow, resid, s_ref, p_ref, macc, mrow, accw, accn,
+    gain, conv_w, q_t, lat, key_t, ew, freq, kvb, qb, gb, va, da, db, ow, resid, s_ref, p_ref, macc, mrow, accw, accn,
     part, ob, att, stream, normed, gacc, vacc, gate, value, act, fp, fr,
-    kvz_s, kvz_r, q_s, q_r, gvz_s, gvz_r, gvy_s, gvy_r, dny_s, dny_r, dnz_s, dnz_r,
-    pk_s, pk_r, pg_s, pg_r, pd_s, pd_r, o_s, o_r, x_s, x_r, e_s, e_r, h_s, h_r, f_s, f_r, loc,
+    kvz_s, kvz_r, q_s, q_r, pk_s, pk_r, o_s, o_r, x_s, x_r, e_s, e_r, h_s, h_r, f_s, f_r, loc, *ring_sems,
 ):
     z = lax.axis_index("sp_0")
     y = lax.axis_index("sp_1")
@@ -101,8 +100,10 @@
         load(q_hbm, q_t, 4),
     ]
     weight_loads = [
-        load(gate_hbm, gv.at[z, y, c, pl.ds(0, 32)], 5), load(value_hbm, gv.at[z, y, c, pl.ds(32, 32)], 6),
-        load(dn_hbm, dn.at[z, y, c], 7),
+        load(gate_hbm, gb.at[z, y, c, pl.ds(0, 32)], 5),
+        load(value_hbm.at[pl.ds(0, 16)], gb.at[z, y, c, pl.ds(32, 16)], 6),
+        load(value_hbm.at[pl.ds(16, 16)], va.at[z, y, c], 7),
+        load(dn_hbm.at[pl.ds(0, 16)], da.at[z, y, c], 12), load(dn_hbm.at[pl.ds(16, 16)], db.at[z, y, c], 13),
     ]
     load_res = load(resid_hbm, resid.at[pl.ds(0, TOK)], 8)
     load_ow = load(ow_hbm, ow, 9)
@@ -183,99 +184,97 @@
     kv_across(0)
     macc[...] = jnp.full((2, 512, 128), -3e38, F32)
 
-    def gvz_own():
-        own = gv.at[z, y, c]
-        send(own, own, gvz_s, gvz_r.at[0, 0], right_z)
-        send(own, own, gvz_s, gvz_r.at[1, 0], left_z)
-
-    def dny_own():
-        own = dn.at[z, y, c]
-        send(own, own, dny_s, dny_r.at[0, 0], right_y)
-        send(own, own, dny_s, dny_r.at[1, 0], left_y)
-
-    def gvy_own():
-        own = gv.at[z, y, c]
-        send(own, own, gvy_s, gvy_r.at[0, 0, 0], right_y)
-        send(own, own, gvy_s, gvy_r.at[1, 0, 0], left_y)
-        send(own, own, pg_s, pg_r.at[0], partner)
-
     for copy in weight_loads:
         copy.wait()
 
     offsets = [0, -1, 1, -2, 2, -3, 3, 4]
 
-    def gv_out(zz, j):
-        block = gv.at[zz, y, c]
-        send(block, block, gvy_s, gvy_r.at[0, 0, j], right_y)
-        send(block, block, gvy_s, gvy_r.at[1, 0, j], left_y)
-        send(block, block, pg_s, pg_r.at[j], partner)
-
-    def gvz(s):
-        lo, hi = zat(-s), zat(s)
-        if s < 4:
-            wait_recv(gv.at[lo, y, c], gvz_r.at[0, s - 1])
-            src = gv.at[lo, y, c] if s < 3 else gv.at[lo, y, c, pl.ds(0, 32)]
-            send(src, src, gvz_s, gvz_r.at[0, s], right_z)
-            wait_recv(gv.at[hi, y, c], gvz_r.at[1, s - 1])
-            src = gv.at[hi, y, c] if s < 3 else gv.at[hi, y, c, pl.ds(32, 32)]
-            send(src, src, gvz_s, gvz_r.at[1, s], left_z)
-            gv_out(lo, 2 * s - 1)
-            gv_out(hi, 2 * s)
-        else:
-            wait_recv(gv.at[lo, y, c, pl.ds(0, 32)], gvz_r.at[0, 3])
-            wait_recv(gv.at[lo, y, c, pl.ds(32, 32)], gvz_r.at[1, 3])
-            gv_out(lo, 7)
-
-    def gvy(s, j):
-        zz = zat(offsets[j])
-        a, b, far = yat(-1), yat(1), yat(2)
-        if s == 1:
-            wait_recv(gv.at[zz, a, c], gvy_r.at[0, 0, j])
-            src = gv.at[zz, a, c, pl.ds(0, 32)]
-            send(src, src, gvy_s, gvy_r.at[0, 1, j], right_y)
-            wait_recv(gv.at[zz, b, c], gvy_r.at[1, 0, j])
-            src = gv.at[zz, b, c, pl.ds(32, 32)]
-            send(src, src, gvy_s, gvy_r.at[1, 1, j], left_y)
-            send(gv.at[zz, a, c], gv.at[zz, a, c], pg_s, pg_r.at[j], partner)
-            send(gv.at[zz, b, c], gv.at[zz, b, c], pg_s, pg_r.at[j], partner)
-        else:
-            wait_recv(gv.at[zz, far, c, pl.ds(0, 32)], gvy_r.at[0, 1, j])
-            wait_recv(gv.at[zz, far, c, pl.ds(32, 32)], gvy_r.at[1, 1, j])
-            send(gv.at[zz, far, c], gv.at[zz, far, c], pg_s, pg_r.at[j], partner)
-
-    def dny(s):
-        a, b, far = yat(-1), yat(1), yat(2)
-        if s == 1:
-            wait_recv(dn.at[z, a, c], dny_r.at[0, 0])
-            src = dn.at[z, a, c, pl.ds(0, 16)]
-            send(src, src, dny_s, dny_r.at[0, 1], right_y)
-            wait_recv(dn.at[z, b, c], dny_r.at[1, 0])
-            src = dn.at[z, b, c, pl.ds(16, 16)]
-            send(src, src, dny_s, dny_r.at[1, 1], left_y)
-        else:
-            wait_recv(dn.at[z, far, c, pl.ds(0, 16)], dny_r.at[0, 1])
-            wait_recv(dn.at[z, far, c, pl.ds(16, 16)], dny_r.at[1, 1])
-
-    def dnz(s, r):
-        yy = yat((0, -1, 1, 2)[r])
-        lo, hi = zat(-s), zat(s)
-        if s == 0:
-            block = dn.at[z, yy, c]
-            send(block, block, dnz_s, dnz_r.at[0, 0, r], right_z)
-            send(block, block, dnz_s, dnz_r.at[1, 0, r], left_z)
-        elif s < 4:
-            wait_recv(dn.at[lo, yy, c], dnz_r.at[0, s - 1, r])
-            src = dn.at[lo, yy, c] if s < 3 else dn.at[lo, yy, c, pl.ds(0, 16)]
-            send(src, src, dnz_s, dnz_r.at[0, s, r], right_z)
-            wait_recv(dn.at[hi, yy, c], dnz_r.at[1, s - 1, r])
-            src = dn.at[hi, yy, c] if s < 3 else dn.at[hi, yy, c, pl.ds(16, 16)]
-            send(src, src, dnz_s, dnz_r.at[1, s, r], left_z)
-        else:
-            wait_recv(dn.at[lo, yy, c, pl.ds(0, 16)], dnz_r.at[0, 3, r])
-            wait_recv(dn.at[lo, yy, c, pl.ds(16, 16)], dnz_r.at[1, 3, r])
-        send(dn.at[lo, yy, c], dn.at[lo, yy, c], pd_s, pd_r.at[slot_of(s, 0)], partner)
-        if 0 < s < 4:
-            send(dn.at[hi, yy, c], dn.at[hi, yy, c], pd_s, pd_r.at[slot_of(s, 1)], partner)
+    def z_then_y(buf, z_s, z_r, y_s, y_r, p_s, p_r):
+        def half(zz, yy, h):
+            return buf.at[zz, yy, c, :, pl.ds(384 * h, 384)]
+
+        def out(zz, j):
+            block = buf.at[zz, y, c]
+            send(block, block, y_s, y_r.at[0, 0, j], right_y)
+            send(block, block, y_s, y_r.at[1, 0, j], left_y)
+            send(block, block, p_s, p_r.at[j], partner)
+
+        def on_z(s):
+            lo, hi = zat(-s), zat(s)
+            if s == 4:
+                wait_recv(half(lo, y, 0), z_r.at[0, 3])
+                wait_recv(half(lo, y, 1), z_r.at[1, 3])
+                out(lo, 7)
+                return
+            for way, (zz, dev) in enumerate(((lo, right_z), (hi, left_z))):
+                block = buf.at[zz, y, c]
+                if s > 0:
+                    wait_recv(block, z_r.at[way, s - 1])
+                src = block if s < 3 else half(zz, y, way)
+                send(src, src, z_s, z_r.at[way, s], dev)
+            if s > 0:
+                out(lo, 2 * s - 1)
+                out(hi, 2 * s)
+
+        def on_y(s, j):
+            zz = zat(offsets[j])
+            a, b, far = yat(-1), yat(1), yat(2)
+            if s == 0:
+                out(z, 0)
+            elif s == 1:
+                for way, (yy, dev) in enumerate(((a, right_y), (b, left_y))):
+                    wait_recv(buf.at[zz, yy, c], y_r.at[way, 0, j])
+                    src = half(zz, yy, way)
+                    send(src, src, y_s, y_r.at[way, 1, j], dev)
+                for yy in (a, b):
+                    send(buf.at[zz, yy, c], buf.at[zz, yy, c], p_s, p_r.at[j], partner)
+            else:
+                wait_recv(half(zz, far, 0), y_r.at[0, 1, j])
+                wait_recv(half(zz, far, 1), y_r.at[1, 1, j])
+                send(buf.at[zz, far, c], buf.at[zz, far, c], p_s, p_r.at[j], partner)
+
+        return on_z, on_y
+
+    def y_then_z(buf, z_s, z_r, y_s, y_r, p_s, p_r):
+        def half(zz, yy, h):
+            return buf.at[zz, yy, c, :, pl.ds(384 * h, 384)]
+
+        def on_y(s):
+            a, b, far = yat(-1), yat(1), yat(2)
+            if s == 2:
+                wait_recv(half(z, far, 0), y_r.at[0, 1])
+                wait_recv(half(z, far, 1), y_r.at[1, 1])
+                return
+            for way, (yy, dev) in enumerate(((a, right_y), (b, left_y))):
+                if s == 0:
+                    src = buf.at[z, y, c]
+                else:
+                    wait_recv(buf.at[z, yy, c], y_r.at[way, 0])
+                    src = half(z, yy, way)
+                send(src, src, y_s, y_r.at[way, s], dev)
+
+        def on_z(s, r):
+            yy = yat((0, -1, 1, 2)[r])
+            lo, hi = zat(-s), zat(s)
+            if s == 4:
+                wait_recv(half(lo, yy, 0), z_r.at[0, 3, r])
+                wait_recv(half(lo, yy, 1), z_r.at[1, 3, r])
+            else:
+                for way, (zz, dev) in enumerate(((lo, right_z), (hi, left_z))):
+                    block = buf.at[zz, yy, c]
+                    if s > 0:
+                        wait_recv(block, z_r.at[way, s - 1, r])
+                    src = block if s < 3 else half(zz, yy, way)
+                    send(src, src, z_s, z_r.at[way, s, r], dev)
+            for ahead, zz in enumerate((lo, hi) if 0 < s < 4 else (lo,)):
+                send(buf.at[zz, yy, c], buf.at[zz, yy, c], p_s, p_r.at[slot_of(s, ahead)], partner)
+
+        return on_y, on_z
+
+    gb_z, gb_y = z_then_y(gb, *ring_sems[0:6])
+    db_z, db_y = z_then_y(db, *ring_sems[6:12])
+    va_y, va_z = y_then_z(va, *ring_sems[12:18])
+    da_y, da_z = y_then_z(da, *ring_sems[18:24])
 
     heads = (
         (0, 256, 0, 256, 256, 512, (NOPE_A + ROPE) ** (-0.5) * LOG2E, accw),
@@ -365,74 +364,107 @@
         send(resid.at[pl.ds(0, 16)], resid.at[pl.ds(144, 16)], h_s, h_r.at[1], device_of(before))
 
     edges_out()
-    gvy_own()
-    gvz_own()
+    gb_z(0)
+    gb_y(0, 0)
+    db_y(0, 0)
     kvz(1, 0)
     q_relay(1)
     kvz(1, 1)
-    dny_own()
     kvz(1, 2)
     kvz(1, 3)
-    gvy(1, 0)
-    gvz(1)
+    da_y(0)
+    va_y(0)
+    gb_z(1)
+    kvz(2, 0)
     q_relay(2)
     scores(0)
     scores(1)
-    kvz(2, 0)
+    kvz(2, 1)
     scores(2)
-    dny(1)
-    kvz(2, 1)
     kvz(2, 2)
-    gvy(2, 0)
     kvz(2, 3)
+    gb_y(1, 0)
+    va_z(0, 0)
+    gb_y(1, 1)
+    gb_z(2)
     scores(3)
-    gvz(2)
     scores(4)
     kvz(3, 0)
+    va_y(1)
     kvz(3, 1)
-    gvy(1, 2)
     kvz(3, 2)
-    dny(2)
-    gvy(1, 1)
+    gb_y(2, 0)
+    gb_y(2, 1)
     kvz(3, 3)
-    dnz(0, 2)
-    dnz(0, 3)
-    dnz(0, 0)
+    va_z(0, 2)
+    va_z(0, 1)
+    db_z(0)
+    da_y(1)
+    da_z(0, 2)
+    da_z(0, 1)
+    va_z(1, 0)
+    gb_y(1, 3)
     scores(5)
-    gvz(3)
+    gb_z(3)
     scores(6)
+    gb_y(1, 4)
+    va_y(2)
+    va_z(0, 3)
+    da_y(2)
+    da_z(0, 3)
     kvz(4, 0)
-    dnz(0, 1)
-    dnz(1, 2)
-    gvy(2, 2)
+    db_y(1, 0)
+    va_z(1, 2)
+    gb_y(2, 3)
+    va_z(1, 1)
+    db_z(1)
     scores(7)
     weigh(0)
-    dnz(1, 0)
-    dnz(1, 3)
-    gvy(2, 1)
+    va_z(2, 0)
+    da_z(1, 1)
     pack(0)
     weigh(1)
+    va_z(1, 3)
     pack(1)
-    gvz(4)
-    gvy(1, 5)
-    dnz(1, 1)
-    gvy(1, 3)
-    gvy(1, 4)
-    dnz(2, 2)
-    gvy(1, 6)
-    dnz(2, 0)
-    dnz(2, 3)
+    da_z(0, 0)
+    gb_z(4)
+    db_y(1, 1)
+    va_z(2, 2)
+    db_y(2, 0)
+    gb_y(1, 2)
+    gb_y(2, 4)
+    gb_y(1, 6)
+    va_z(2, 1)
+    da_z(1, 3)
+    gb_y(1, 5)
+    db_y(1, 2)
+    db_z(2)
+    va_z(3, 0)
+    da_z(2, 1)
+    va_z(2, 3)
     part_in()
     merge()
     att_out()
-    dnz(2, 1)
-    dnz(3, 2)
-    gvy(1, 7)
-    dnz(3, 0)
-    gvy(2, 5)
-    dnz(3, 3)
-    gvy(2, 3)
-    dnz(3, 1)
+    da_z(1, 2)
+    da_z(1, 0)
+    va_z(3, 2)
+    va_z(3, 1)
+    gb_y(1, 7)
+    da_z(2, 3)
+    db_y(2, 1)
+    db_z(3)
+    va_z(4, 0)
+    gb_y(2, 2)
+    da_z(3, 1)
+    gb_y(2, 6)
+    va_z(3, 3)
+    da_z(2, 2)
+    gb_y(2, 5)
+    db_y(2, 2)
+    da_z(2, 0)
+    va_z(4, 2)
+    db_y(1, 3)
+    va_z(4, 1)
     load_ow.wait()
     load_gain.wait()
     load_conv.wait()
@@ -459,31 +491,53 @@
         cols = slice(n * 256, n * 256 + 256)
         scaled = stream[:, cols].astype(F32) * scale
         normed[n] = (scaled * gain[cols].astype(F32).reshape(1, 256)).astype(BF)
-    gvy(2, 4)
-    gvy(2, 6)
-
-    def up(lo, rows, js, acc, n):
-        cols = slice(n * 256, n * 256 + 256)
+    da_z(3, 3)
+    db_y(1, 4)
+    db_z(4)
+    da_z(4, 1)
+    db_y(1, 5)
+    va_z(4, 3)
+    gb_y(2, 7)
+
+    def gate_rows(zz, cols):
+        return gb[zz, :, :, 0:32, cols].reshape(256, 256)
+
+    def value_rows(zz, cols):
+        return jnp.concatenate([gb[zz, :, :, 32:48, cols], va[zz, :, :, :, cols]], axis=2).reshape(256, 256)
+
+    def up(weights, rows, js, n):
         total = None
         for j in js:
             zz = zat(offsets[j])
-            w = gv[zz, :, :, lo : lo + 32, cols].reshape(256, 256)
+            w = weights(zz, slice(n * 256, n * 256 + 256))
             term = jnp.dot(normed[zz, 0:rows], w, preferred_element_type=F32)
             total = term if total is None else total + term
-        return total if acc is None else acc[:, cols] + total
+        return total
+
+    def arrived(buf, sems, j):
+        wait_recv(buf.at[zat(offsets[j]), :, other], sems.at[j])
 
     for j in range(7):
-        wait_recv(gv.at[zat(offsets[j]), :, other], pg_r.at[j])
+        arrived(gb, ring_sems[5], j)
     for n in range(3):
-        gacc[:, n * 256 : n * 256 + 256] = up(0, ROWS, range(7), None, n)
-    gvy(2, 7)
+        gacc[:, n * 256 : n * 256 + 256] = up(gate_rows, ROWS, range(7), n)
+    db_y(1, 6)
+    da_z(3, 2)
+    db_y(2, 3)
+    for j in range(7):
+        arrived(va, ring_sems[17], j)
     for n in range(3):
-        vacc[:, n * 256 : n * 256 + 256] = up(32, TOK, range(7), None, n)
-    wait_recv(gv.at[zat(offsets[7]), :, other], pg_r.at[7])
+        vacc[:, n * 256 : n * 256 + 256] = up(value_rows, TOK, range(7), n)
+    da_z(3, 0)
+    db_y(2, 4)
+    arrived(gb, ring_sems[5], 7)
+    arrived(va, ring_sems[17], 7)
     for n in range(3):
         cols = slice(n * 256, n * 256 + 256)
-        gate[:, cols] = up(0, ROWS, (7,), gacc, n).astype(BF)
-        value[:, cols] = up(32, TOK, (7,), vacc, n).astype(BF)
+        gate[:, cols] = (gacc[:, cols] + up(gate_rows, ROWS, (7,), n)).astype(BF)
+        value[:, cols] = (vacc[:, cols] + up(value_rows, TOK, (7,), n)).astype(BF)
+    db_y(1, 7)
+    da_z(4, 3)
 
     row = lax.broadcasted_iota(jnp.int32, (TOK, 256), 0)
     for n in range(3):
@@ -501,16 +555,23 @@
 
     for j in range(NZ):
         zz = zat(offsets[j])
-        if j == 7:
-            for r in range(NY):
-                dnz(4, r)
-        wait_recv(dn.at[zz, :, other], pd_r.at[j])
-        w = dn[zz].reshape(256, FFD)
+        arrived(da, ring_sems[23], j)
+        arrived(db, ring_sems[11], j)
+        w = jnp.concatenate([da[zz], db[zz]], axis=2).reshape(256, FFD)
         d = lax.dot_general(act[...], w, (((1,), (1,)), ((), ())), preferred_element_type=F32)
         fp[j] = d.astype(BF).reshape(NX, 32, 256)
         for o in (2, 1, 3):
             peer = xat(o)
             send(fp.at[j, peer], fr.at[j, x], f_s, f_r.at[j, o - 1], {"tp": peer})
+        if j == 3:
+            db_y(2, 5)
+        if j == 4:
+            db_y(2, 6)
+        if j == 5:
+            da_z(4, 2)
+            da_z(4, 0)
+        if j == 6:
+            db_y(2, 7)
 
     rows = pl.ds(pl.multiple_of(x * 32, 32), 32)
     for j in range(NZ):
@@ -523,13 +584,15 @@
 
     wait_send(kvb.at[pl.ds(0, 7), 0], kvz_s)
     wait_send(qb.at[pl.ds(0, 3)], q_s)
-    wait_send(gv.at[pl.ds(0, 7), 0, 0], gvz_s)
-    wait_send(gv.at[:, pl.ds(0, 3), 0], gvy_s)
-    wait_send(dn.at[0, pl.ds(0, 3), 0], dny_s)
-    wait_send(dn.at[pl.ds(0, 7), :, 0], dnz_s)
     wait_send(kvb.at[:, 0], pk_s)
-    wait_send(gv.at[:, :, 0], pg_s)
-    wait_send(dn.at[:, :, 0], pd_s)
+    for buf, (z_s, _, y_s, _, p_s, _) in ((gb, ring_sems[0:6]), (db, ring_sems[6:12])):
+        wait_send(buf.at[pl.ds(0, 7), 0, 0], z_s)
+        wait_send(buf.at[:, pl.ds(0, 3), 0], y_s)
+        wait_send(buf.at[:, :, 0], p_s)
+    for buf, (z_s, _, y_s, _, p_s, _) in ((va, ring_sems[12:18]), (da, ring_sems[18:24])):
+        wait_send(buf.at[pl.ds(0, 7), :, 0], z_s)
+        wait_send(buf.at[0, pl.ds(0, 3), 0], y_s)
+        wait_send(buf.at[:, :, 0], p_s)
     wait_send(part.at[pl.ds(0, 3)], o_s)
     wait_send(att.at[pl.ds(0, 3), pl.ds(0, TOK)], x_s)
     wait_send(att.at[:, pl.ds(0, 32)], e_s)
@@ -551,8 +614,10 @@
         pltpu.VMEM((32, TOK), F32),
         pltpu.VMEM((NZ, 2, TOK, 512), BF),
         pltpu.VMEM((NY, TOK, 384), BF),
-        pltpu.VMEM((NZ, NY, 2, 64, FFD), BF),
-        pltpu.VMEM((NZ, NY, 2, 32, FFD), BF),
+        pltpu.VMEM((NZ, NY, 2, 48, FFD), BF),
+        pltpu.VMEM((NZ, NY, 2, 16, FFD), BF),
+        pltpu.VMEM((NZ, NY, 2, 16, FFD), BF),
+        pltpu.VMEM((NZ, NY, 2, 16, FFD), BF),
         pltpu.VMEM((768, D), BF),
         pltpu.VMEM((ROWS, D), BF),
         pltpu.VMEM((2, NZ, 512, 256), F32),
@@ -573,11 +638,11 @@
         pltpu.VMEM((TOK, FFD), BF),
         pltpu.VMEM((NZ, NX, 32, 256), BF),
         pltpu.VMEM((NZ, NX, 32, 256), BF),
-        dma, dma((2, 4, 4)), dma, dma((2, 2)), dma, dma((2, 4)), dma, dma((2, 2, 8)),
-        dma, dma((2, 2)), dma, dma((2, 4, 4)),
-        dma, dma((8,)), dma, dma((8,)), dma, dma((8,)), dma, dma((3,)), dma, dma((3,)), dma, dma((2, 4)), dma, dma((2,)),
-        dma, dma((NZ, 3)), dma((12,)),
+        dma, dma((2, 4, 4)), dma, dma((2, 2)), dma, dma((8,)), dma, dma((3,)), dma, dma((3,)),
+        dma, dma((2, 4)), dma, dma((2,)), dma, dma((NZ, 3)), dma((14,)),
     ]
+    scratch += 2 * [dma, dma((2, 4)), dma, dma((2, 2, 8)), dma, dma((8,))]
+    scratch += 2 * [dma, dma((2, 4, 4)), dma, dma((2, 2)), dma, dma((8,))]
     return pl.pallas_call(
         kernel,
         out_shape=pltpu.VMEM((32, D), BF),

time: 60.9 us -> 61.8 us (1.015)
  Pallas kernels: 60.1 us -> 61.1 us
    pallas_call x1, Pallas kernels: 60.1 us -> 61.1 us  [layer(): pl.pallas_call(kernel, out_shape=pltpu.VMEM((32, D), BF), in_specs=[hbm]...]
where the time goes in v7:
time: 61.8 us
  Pallas kernels  61.1 us (99%)
  local copies, waits for them, and re-layouts  0.66 us (1%)
    pallas_call x1, Pallas kernels, layer(): pl.pallas_call(kernel, out_shape=pltpu.VMEM((32, D), BF), in_specs=[hbm]...  61.1 us

profile of v7, /device:TPU:1, one launch (start us, length us, event | category | flops | bytes accessed | tf_op | source)
XLA Modules:
  0.0 61.8 jit_solution(9170312669970169993)
XLA Ops:
  0.0 61.1 %shard_map.118 = bf16[32,2048]{1,0:T(8,128)(2,1)S(1)} custom-call(bf16[2048]{0:T(1024)(128)(2,1)} %gain_hbm.1, bf16[3,768]{1,0:T(4,128)(2,1)} %conv_hbm.1, bf16[320,128]{1,0:T(8,128)(2,1)} %bitcast.3, bf16[128,512]{1,0:T(8,128)(2,1)} %lat_hbm.1, bf16[64,128]{1,0:T(8,128)(2,1)} %bitcast.5, bf16[512,384]{1,0:T(8,128)(2,1)} %ew_hbm.1, ...), custom_call_target="tpu_custom_call" | custom-call | tf_op jit(solution)/shard_map/pallas_call | solution.py:646
  61.1 0.7 %copy.14 = bf16[32,2048]{1,0:T(8,128)(2,1)} copy(bf16[32,2048]{1,0:T(8,128)(2,1)S(1)} %shard_map.118) | data formatting | bytes 262144

commit v8 on v7

--- a/solution.py
+++ b/solution.py
@@ -494,8 +494,6 @@
     da_z(3, 3)
     db_y(1, 4)
     db_z(4)
-    da_z(4, 1)
-    db_y(1, 5)
     va_z(4, 3)
     gb_y(2, 7)
 
@@ -521,15 +519,15 @@
         arrived(gb, ring_sems[5], j)
     for n in range(3):
         gacc[:, n * 256 : n * 256 + 256] = up(gate_rows, ROWS, range(7), n)
+    db_y(1, 5)
+    da_z(4, 1)
     db_y(1, 6)
     da_z(3, 2)
-    db_y(2, 3)
     for j in range(7):
         arrived(va, ring_sems[17], j)
     for n in range(3):
         vacc[:, n * 256 : n * 256 + 256] = up(value_rows, TOK, range(7), n)
     da_z(3, 0)
-    db_y(2, 4)
     arrived(gb, ring_sems[5], 7)
     arrived(va, ring_sems[17], 7)
     for n in range(3):
@@ -537,7 +535,6 @@
         gate[:, cols] = (gacc[:, cols] + up(gate_rows, ROWS, (7,), n)).astype(BF)
         value[:, cols] = (vacc[:, cols] + up(value_rows, TOK, (7,), n)).astype(BF)
     db_y(1, 7)
-    da_z(4, 3)
 
     row = lax.broadcasted_iota(jnp.int32, (TOK, 256), 0)
     for n in range(3):
@@ -563,12 +560,18 @@
         for o in (2, 1, 3):
             peer = xat(o)
             send(fp.at[j, peer], fr.at[j, x], f_s, f_r.at[j, o - 1], {"tp": peer})
+        if j == 0:
+            db_y(2, 3)
+            da_z(4, 3)
+        if j == 1:
+            db_y(2, 4)
+        if j == 2:
+            db_y(2, 5)
         if j == 3:
-            db_y(2, 5)
+            db_y(2, 6)
         if j == 4:
-            db_y(2, 6)
+            da_z(4, 2)
         if j == 5:
-            da_z(4, 2)
             da_z(4, 0)
         if j == 6:
             db_y(2, 7)

time: 61.8 us -> 61.4 us (level)
  no operation moved by 1% of the time
where the time goes in v8:
time: 61.4 us; the launch traced here: 61.3 us
  Pallas kernels  60.6 us (99%)
  local copies, waits for them, and re-layouts  0.66 us (1%)
    pallas_call x1, Pallas kernels, layer(): pl.pallas_call(kernel, out_shape=pltpu.VMEM((32, D), BF), in_specs=[hbm]...  60.6 us

profile of v8, /device:TPU:1, one launch (start us, length us, event | category | flops | bytes accessed | tf_op | source)
XLA Modules:
  0.0 61.3 jit_solution(5290332626567626977)
XLA Ops:
  0.0 60.6 %shard_map.118 = bf16[32,2048]{1,0:T(8,128)(2,1)S(1)} custom-call(bf16[2048]{0:T(1024)(128)(2,1)} %gain_hbm.1, bf16[3,768]{1,0:T(4,128)(2,1)} %conv_hbm.1, bf16[320,128]{1,0:T(8,128)(2,1)} %bitcast.3, bf16[128,512]{1,0:T(8,128)(2,1)} %lat_hbm.1, bf16[64,128]{1,0:T(8,128)(2,1)} %bitcast.5, bf16[512,384]{1,0:T(8,128)(2,1)} %ew_hbm.1, ...), custom_call_target="tpu_custom_call" | custom-call | tf_op jit(solution)/shard_map/pallas_call | solution.py:649
  60.6 0.7 %copy.14 = bf16[32,2048]{1,0:T(8,128)(2,1)} copy(bf16[32,2048]{1,0:T(8,128)(2,1)S(1)} %shard_map.118) | data formatting | bytes 262144

commit v9 on v8

--- a/solution.py
+++ b/solution.py
@@ -109,7 +109,6 @@
     load_ow = load(ow_hbm, ow, 9)
     load_gain = load(gain_hbm, gain, 10)
     load_conv = load(conv_hbm, conv_w, 11)
-    pl.semaphore_wait(barrier, len(greeted))
     for copy in first_loads:
         copy.wait()
 
@@ -139,6 +138,9 @@
         turned(q_t[256:288, :], q_t[288:320, :]) + [q_t[128:192, :].astype(F32)]
     ).astype(BF)
 
+    macc[...] = jnp.full((2, 512, 128), -3e38, F32)
+    pl.semaphore_wait(barrier, len(greeted))
+
     def rows_of(slot, h):
         return kvb.at[slot, 0, pl.ds(32 * h, 32)]
 
@@ -182,7 +184,6 @@
     send(qb.at[3], qb.at[1], q_s, q_r.at[0, 0], right_y)
     send(qb.at[3], qb.at[2], q_s, q_r.at[1, 0], left_y)
     kv_across(0)
-    macc[...] = jnp.full((2, 512, 128), -3e38, F32)
 
     for copy in weight_loads:
         copy.wait()
@@ -291,19 +292,34 @@
             s_ref[head, j] = s
             macc[head] = jnp.maximum(macc[head], jnp.maximum(s[:, :128], s[:, 128:]))
 
+    def weights(half, head, j0, j1):
+        rows = slice(256 * half, 256 * half + 256)
+        v0, v1, factor, acc = heads[head][4:]
+        m = jnp.broadcast_to(jnp.max(macc[head, rows], axis=1, keepdims=True), (256, 128))
+        for j in range(j0, j1):
+            for side in range(2):
+                s = s_ref[head, j, rows, side * 128 : side * 128 + 128]
+                at = j * 256 + side * 128
+                p_ref[head, :, at : at + 128] = jnp.exp2((s - m) * factor).astype(BF)
+        vs = kvb[j0:j1, :, :, v0:v1].reshape(256 * (j1 - j0), v1 - v0)
+        return m, jnp.dot(p_ref[head, :, j0 * 256 : j1 * 256], vs, preferred_element_type=F32)
+
+    def weigh_early(half):
+        rows = slice(256 * half, 256 * half + 256)
+        for head in range(2):
+            m, product = weights(half, head, 0, 5)
+            mrow[head, rows] = m
+            heads[head][7][rows] = product
+
     def weigh(half):
         rows = slice(256 * half, 256 * half + 256)
         for head in range(2):
-            v0, v1, factor, acc = heads[head][4:]
-            m = jnp.broadcast_to(jnp.max(macc[head, rows], axis=1, keepdims=True), (256, 128))
+            m, product = weights(half, head, 5, 8)
+            factor, acc = heads[head][6:]
+            shrink = jnp.exp2((mrow[head, rows] - m) * factor)
+            shrink = jnp.concatenate([shrink] * (acc.shape[1] // 128), axis=1)
             mrow[head, rows] = m
-            for j in range(NZ):
-                for side in range(2):
-                    s = s_ref[head, j, rows, side * 128 : side * 128 + 128]
-                    at = j * 256 + side * 128
-                    p_ref[head, :, at : at + 128] = jnp.exp2((s - m) * factor).astype(BF)
-            vs = kvb[:, :, :, v0:v1].reshape(2048, v1 - v0)
-            acc[rows] = jnp.dot(p_ref[head], vs, preferred_element_type=F32)
+            acc[rows] = acc[rows] * shrink + product
 
     lane = lax.broadcasted_iota(jnp.int32, (TOK, 128), 1)
 
@@ -366,105 +382,103 @@
     edges_out()
     gb_z(0)
     gb_y(0, 0)
-    db_y(0, 0)
+    va_y(0)
     kvz(1, 0)
     q_relay(1)
     kvz(1, 1)
+    db_y(0, 0)
     kvz(1, 2)
     kvz(1, 3)
     da_y(0)
-    va_y(0)
+    gb_y(1, 0)
+    va_y(1)
     gb_z(1)
     kvz(2, 0)
     q_relay(2)
     scores(0)
     scores(1)
     kvz(2, 1)
+    db_y(1, 0)
     scores(2)
     kvz(2, 2)
+    gb_y(2, 0)
     kvz(2, 3)
-    gb_y(1, 0)
-    va_z(0, 0)
-    gb_y(1, 1)
+    va_y(2)
     gb_z(2)
     scores(3)
     scores(4)
     kvz(3, 0)
-    va_y(1)
+    va_z(0, 2)
+    weigh_early(0)
     kvz(3, 1)
+    db_y(2, 0)
+    gb_y(1, 2)
     kvz(3, 2)
-    gb_y(2, 0)
-    gb_y(2, 1)
+    weigh_early(1)
     kvz(3, 3)
-    va_z(0, 2)
+    va_z(0, 3)
+    va_z(0, 0)
+    da_y(1)
+    db_z(0)
+    da_z(0, 2)
     va_z(0, 1)
-    db_z(0)
-    da_y(1)
-    da_z(0, 2)
-    da_z(0, 1)
-    va_z(1, 0)
-    gb_y(1, 3)
+    da_z(0, 0)
+    gb_z(3)
     scores(5)
-    gb_z(3)
+    gb_y(1, 4)
     scores(6)
-    gb_y(1, 4)
-    va_y(2)
-    va_z(0, 3)
+    va_z(1, 2)
+    gb_y(2, 2)
     da_y(2)
     da_z(0, 3)
     kvz(4, 0)
-    db_y(1, 0)
-    va_z(1, 2)
-    gb_y(2, 3)
-    va_z(1, 1)
+    va_z(1, 3)
+    va_z(1, 0)
     db_z(1)
     scores(7)
     weigh(0)
-    va_z(2, 0)
-    da_z(1, 1)
+    va_z(1, 1)
     pack(0)
     weigh(1)
-    va_z(1, 3)
     pack(1)
-    da_z(0, 0)
+    da_z(1, 0)
+    gb_y(2, 4)
     gb_z(4)
+    gb_y(1, 3)
+    da_z(0, 1)
+    gb_y(1, 6)
+    gb_y(1, 5)
     db_y(1, 1)
     va_z(2, 2)
-    db_y(2, 0)
-    gb_y(1, 2)
-    gb_y(2, 4)
-    gb_y(1, 6)
+    db_y(1, 2)
+    va_z(2, 3)
+    va_z(2, 0)
+    db_z(2)
     va_z(2, 1)
-    da_z(1, 3)
-    gb_y(1, 5)
-    db_y(1, 2)
-    db_z(2)
-    va_z(3, 0)
-    da_z(2, 1)
-    va_z(2, 3)
+    da_z(2, 0)
     part_in()
     merge()
     att_out()
+    da_z(1, 1)
+    gb_y(1, 1)
+    da_z(1, 3)
     da_z(1, 2)
-    da_z(1, 0)
     va_z(3, 2)
+    va_z(3, 3)
+    gb_y(1, 7)
+    va_z(3, 0)
+    gb_y(2, 3)
+    db_z(3)
     va_z(3, 1)
-    gb_y(1, 7)
+    gb_y(2, 6)
+    da_z(3, 0)
+    gb_y(2, 5)
+    da_z(2, 1)
+    db_y(2, 1)
+    db_y(2, 2)
     da_z(2, 3)
-    db_y(2, 1)
-    db_z(3)
-    va_z(4, 0)
-    gb_y(2, 2)
-    da_z(3, 1)
-    gb_y(2, 6)
-    va_z(3, 3)
+    db_y(1, 3)
     da_z(2, 2)
-    gb_y(2, 5)
-    db_y(2, 2)
-    da_z(2, 0)
-    va_z(4, 2)
-    db_y(1, 3)
-    va_z(4, 1)
     load_ow.wait()
     load_gain.wait()
     load_conv.wait()
@@ -491,10 +505,13 @@
         cols = slice(n * 256, n * 256 + 256)
         scaled = stream[:, cols].astype(F32) * scale
         normed[n] = (scaled * gain[cols].astype(F32).reshape(1, 256)).astype(BF)
-    da_z(3, 3)
     db_y(1, 4)
     db_z(4)
+    va_z(4, 2)
+    va_z(4, 0)
     va_z(4, 3)
+    va_z(4, 1)
+    gb_y(2, 1)
     gb_y(2, 7)
 
     def gate_rows(zz, cols):
@@ -519,22 +536,21 @@
         arrived(gb, ring_sems[5], j)
     for n in range(3):
         gacc[:, n * 256 : n * 256 + 256] = up(gate_rows, ROWS, range(7), n)
+    da_z(3, 1)
     db_y(1, 5)
-    da_z(4, 1)
-    db_y(1, 6)
-    da_z(3, 2)
     for j in range(7):
         arrived(va, ring_sems[17], j)
     for n in range(3):
         vacc[:, n * 256 : n * 256 + 256] = up(value_rows, TOK, range(7), n)
-    da_z(3, 0)
+    da_z(3, 3)
+    db_y(1, 6)
+    da_z(3, 2)
     arrived(gb, ring_sems[5], 7)
     arrived(va, ring_sems[17], 7)
     for n in range(3):
         cols = slice(n * 256, n * 256 + 256)
         gate[:, cols] = (gacc[:, cols] + up(gate_rows, ROWS, (7,), n)).astype(BF)
         value[:, cols] = (vacc[:, cols] + up(value_rows, TOK, (7,), n)).astype(BF)
-    db_y(1, 7)
 
     row = lax.broadcasted_iota(jnp.int32, (TOK, 256), 0)
     for n in range(3):
@@ -561,18 +577,19 @@
             peer = xat(o)
             send(fp.at[j, peer], fr.at[j, x], f_s, f_r.at[j, o - 1], {"tp": peer})
         if j == 0:
+            db_y(1, 7)
             db_y(2, 3)
-            da_z(4, 3)
         if j == 1:
+            da_z(4, 0)
             db_y(2, 4)
         if j == 2:
             db_y(2, 5)
+            da_z(4, 1)
         if j == 3:
             db_y(2, 6)
+            da_z(4, 3)
         if j == 4:
             da_z(4, 2)
-        if j == 5:
-            da_z(4, 0)
         if j == 6:
             db_y(2, 7)
 

time: 61.4 us -> 59.5 us (0.969)
  Pallas kernels: 60.6 us -> 58.7 us
    pallas_call x1, Pallas kernels: 60.6 us -> 58.7 us  [layer(): pl.pallas_call(kernel, out_shape=pltpu.VMEM((32, D), BF), in_specs=[hbm]...]
where the time goes in v9:
time: 59.5 us; the launch traced here: 59.4 us
  Pallas kernels  58.7 us (99%)
  local copies, waits for them, and re-layouts  0.66 us (1%)
    pallas_call x1, Pallas kernels, layer(): pl.pallas_call(kernel, out_shape=pltpu.VMEM((32, D), BF), in_specs=[hbm]...  58.7 us

profile of v9, /device:TPU:1, one launch (start us, length us, event | category | flops | bytes accessed | tf_op | source)
XLA Modules:
  0.0 59.4 jit_solution(11062201656806836542)
XLA Ops:
  0.0 58.7 %shard_map.118 = bf16[32,2048]{1,0:T(8,128)(2,1)S(1)} custom-call(bf16[2048]{0:T(1024)(128)(2,1)} %gain_hbm.1, bf16[3,768]{1,0:T(4,128)(2,1)} %conv_hbm.1, bf16[320,128]{1,0:T(8,128)(2,1)} %bitcast.3, bf16[128,512]{1,0:T(8,128)(2,1)} %lat_hbm.1, bf16[64,128]{1,0:T(8,128)(2,1)} %bitcast.5, bf16[512,384]{1,0:T(8,128)(2,1)} %ew_hbm.1, ...), custom_call_target="tpu_custom_call" | custom-call | tf_op jit(solution)/shard_map/pallas_call | solution.py:666
  58.7 0.7 %copy.14 = bf16[32,2048]{1,0:T(8,128)(2,1)} copy(bf16[32,2048]{1,0:T(8,128)(2,1)S(1)} %shard_map.118) | data formatting | bytes 262144

commit v10 on v9

--- a/solution.py
+++ b/solution.py
@@ -38,7 +38,7 @@
     gain_hbm, conv_hbm, q_hbm, lat_hbm, key_hbm, ew_hbm, gate_hbm, value_hbm, dn_hbm, freq_hbm, resid_hbm, ow_hbm,
     out_ref,
     gain, conv_w, q_t, lat, key_t, ew, freq, kvb, qb, gb, va, da, db, ow, resid, s_ref, p_ref, macc, mrow, accw, accn,
-    part, ob, att, stream, normed, gacc, vacc, gate, value, act, fp, fr,
+    part, ob, att, attp, stream, normed, gacc, vacc, gate, value, act, fp, fr,
     kvz_s, kvz_r, q_s, q_r, pk_s, pk_r, o_s, o_r, x_s, x_r, e_s, e_r, h_s, h_r, f_s, f_r, loc, *ring_sems,
 ):
     z = lax.axis_index("sp_0")
@@ -360,6 +360,8 @@
         narrow = sum(w[:, 67:68] * s for w, s in zip(shares, tiles))
         att[x, 0:TOK, 0:128] = wide.astype(BF)
         att[x, 0:TOK, 128:256] = narrow.astype(BF)
+        attp[x, 0:TOK] = wide.astype(BF)
+        attp[x, TOK:192] = jnp.where(lane[0:64] < 64, narrow[0:64], pltpu.roll(narrow[64:128], 64, 1)).astype(BF)
 
     def part_in():
         for o in range(3):
@@ -367,8 +369,7 @@
 
     def att_out():
         for o in (2, 1, 3):
-            mine = att.at[x, pl.ds(0, TOK)]
-            send(mine, mine, x_s, x_r.at[o - 1], {"tp": xat(o)})
+            send(attp.at[x], attp.at[x], x_s, x_r.at[o - 1], {"tp": xat(o)})
         for o in range(NX):
             peer = {"tp": xat(o)}
             send(att.at[x, pl.ds(112, 16)], att.at[x, pl.ds(128, 16)], e_s, e_r.at[0, o], device_of(after) | peer)
@@ -383,109 +384,114 @@
     gb_z(0)
     gb_y(0, 0)
     va_y(0)
+    db_y(0, 0)
     kvz(1, 0)
     q_relay(1)
     kvz(1, 1)
-    db_y(0, 0)
     kvz(1, 2)
     kvz(1, 3)
-    da_y(0)
     gb_y(1, 0)
-    va_y(1)
     gb_z(1)
+    db_y(1, 0)
     kvz(2, 0)
     q_relay(2)
     scores(0)
+    kvz(2, 1)
     scores(1)
-    kvz(2, 1)
-    db_y(1, 0)
+    kvz(2, 2)
+    da_y(0)
     scores(2)
-    kvz(2, 2)
-    gb_y(2, 0)
     kvz(2, 3)
-    va_y(2)
+    va_y(1)
+    va_z(0, 1)
     gb_z(2)
     scores(3)
     scores(4)
     kvz(3, 0)
-    va_z(0, 2)
     weigh_early(0)
     kvz(3, 1)
+    va_y(2)
+    va_z(0, 3)
+    weigh_early(1)
+    kvz(3, 2)
+    kvz(3, 3)
+    va_z(0, 0)
+    va_z(0, 2)
+    db_z(0)
     db_y(2, 0)
     gb_y(1, 2)
-    kvz(3, 2)
-    weigh_early(1)
-    kvz(3, 3)
-    va_z(0, 3)
-    va_z(0, 0)
+    va_z(1, 1)
     da_y(1)
-    db_z(0)
-    da_z(0, 2)
-    va_z(0, 1)
-    da_z(0, 0)
+    da_z(0, 1)
+    gb_y(1, 3)
+    scores(5)
     gb_z(3)
-    scores(5)
+    scores(6)
     gb_y(1, 4)
-    scores(6)
+    gb_y(2, 2)
+    va_z(1, 3)
+    kvz(4, 0)
+    va_z(1, 0)
     va_z(1, 2)
-    gb_y(2, 2)
-    da_y(2)
-    da_z(0, 3)
-    kvz(4, 0)
-    va_z(1, 3)
-    va_z(1, 0)
     db_z(1)
     scores(7)
     weigh(0)
-    va_z(1, 1)
+    va_z(2, 1)
+    da_y(2)
+    da_z(0, 0)
+    da_z(0, 2)
+    da_z(0, 3)
     pack(0)
     weigh(1)
     pack(1)
-    da_z(1, 0)
+    gb_z(4)
+    gb_y(1, 1)
+    gb_y(1, 5)
     gb_y(2, 4)
-    gb_z(4)
-    gb_y(1, 3)
-    da_z(0, 1)
-    gb_y(1, 6)
-    gb_y(1, 5)
+    gb_y(2, 3)
+    va_z(2, 3)
+    va_z(2, 0)
     db_y(1, 1)
     va_z(2, 2)
     db_y(1, 2)
-    va_z(2, 3)
-    va_z(2, 0)
     db_z(2)
-    va_z(2, 1)
-    da_z(2, 0)
+    va_z(3, 1)
+    da_z(1, 0)
+    da_z(1, 2)
+    da_z(1, 3)
     part_in()
     merge()
     att_out()
     da_z(1, 1)
-    gb_y(1, 1)
-    da_z(1, 3)
-    da_z(1, 2)
+    va_z(3, 3)
+    gb_y(2, 0)
+    va_z(3, 0)
+    gb_y(1, 6)
     va_z(3, 2)
-    va_z(3, 3)
     gb_y(1, 7)
-    va_z(3, 0)
-    gb_y(2, 3)
     db_z(3)
-    va_z(3, 1)
-    gb_y(2, 6)
-    da_z(3, 0)
+    va_z(4, 1)
+    gb_y(2, 1)
+    da_z(2, 0)
+    da_z(2, 2)
     gb_y(2, 5)
+    db_y(2, 1)
+    da_z(2, 3)
+    db_y(2, 2)
     da_z(2, 1)
-    db_y(2, 1)
-    db_y(2, 2)
-    da_z(2, 3)
     db_y(1, 3)
-    da_z(2, 2)
+    va_z(4, 3)
     load_ow.wait()
     load_gain.wait()
     load_conv.wait()
     wait_recv(resid.at[pl.ds(128, 16)], h_r.at[0])
     wait_recv(resid.at[pl.ds(144, 16)], h_r.at[1])
     for o in (2, 1, 3):
-        wait_recv(att.at[xat(-o), pl.ds(0, TOK)], x_r.at[o - 1])
+        wait_recv(attp.at[xat(-o)], x_r.at[o - 1])
+        packed = attp[xat(-o), TOK:192]
+        att[xat(-o), 0:TOK, 0:128] = attp[xat(-o), 0:TOK]
+        att[xat(-o), 0:64, 128:256] = packed
+        att[xat(-o), 64:128, 128:256] = pltpu.roll(packed.astype(F32), 64, 1).astype(BF)
     for o in range(NX):
         wait_recv(att.at[xat(-o), pl.ds(128, 16)], e_r.at[0, o])
         wait_recv(att.at[xat(-o), pl.ds(144, 16)], e_r.at[1, o])
@@ -505,13 +511,12 @@
         cols = slice(n * 256, n * 256 + 256)
         scaled = stream[:, cols].astype(F32) * scale
         normed[n] = (scaled * gain[cols].astype(F32).reshape(1, 256)).astype(BF)
+    db_z(4)
     db_y(1, 4)
-    db_z(4)
+    da_z(3, 0)
     va_z(4, 2)
     va_z(4, 0)
-    va_z(4, 3)
-    va_z(4, 1)
-    gb_y(2, 1)
+    gb_y(2, 6)
     gb_y(2, 7)
 
     def gate_rows(zz, cols):
@@ -534,17 +539,19 @@
 
     for j in range(7):
         arrived(gb, ring_sems[5], j)
-    for n in range(3):
-        gacc[:, n * 256 : n * 256 + 256] = up(gate_rows, ROWS, range(7), n)
-    da_z(3, 1)
+    gacc[:, 0:256] = up(gate_rows, ROWS, range(7), 0)
+    da_z(3, 2)
+    gacc[:, 256:512] = up(gate_rows, ROWS, range(7), 1)
+    gacc[:, 512:768] = up(gate_rows, ROWS, range(7), 2)
     db_y(1, 5)
+    da_z(3, 3)
     for j in range(7):
         arrived(va, ring_sems[17], j)
-    for n in range(3):
-        vacc[:, n * 256 : n * 256 + 256] = up(value_rows, TOK, range(7), n)
-    da_z(3, 3)
+    vacc[:, 0:256] = up(value_rows, TOK, range(7), 0)
+    vacc[:, 256:512] = up(value_rows, TOK, range(7), 1)
     db_y(1, 6)
-    da_z(3, 2)
+    da_z(3, 1)
+    vacc[:, 512:768] = up(value_rows, TOK, range(7), 2)
     arrived(gb, ring_sems[5], 7)
     arrived(va, ring_sems[17], 7)
     for n in range(3):
@@ -580,16 +587,16 @@
             db_y(1, 7)
             db_y(2, 3)
         if j == 1:
+            db_y(2, 4)
             da_z(4, 0)
-            db_y(2, 4)
         if j == 2:
             db_y(2, 5)
-            da_z(4, 1)
+            da_z(4, 2)
         if j == 3:
             db_y(2, 6)
             da_z(4, 3)
         if j == 4:
-            da_z(4, 2)
+            da_z(4, 1)
         if j == 6:
             db_y(2, 7)
 
@@ -614,7 +621,7 @@
         wait_send(buf.at[0, pl.ds(0, 3), 0], y_s)
         wait_send(buf.at[:, :, 0], p_s)
     wait_send(part.at[pl.ds(0, 3)], o_s)
-    wait_send(att.at[pl.ds(0, 3), pl.ds(0, TOK)], x_s)
+    wait_send(attp.at[pl.ds(0, 3)], x_s)
     wait_send(att.at[:, pl.ds(0, 32)], e_s)
     wait_send(resid.at[pl.ds(0, 32)], h_s)
     wait_send(fp.at[:, pl.ds(0, 3)], f_s)
@@ -649,6 +656,7 @@
         pltpu.VMEM((NY, TOK, 256), BF),
         pltpu.VMEM((NY, TOK, 256), BF),
         pltpu.VMEM((NX, ROWS, 256), BF),
+        pltpu.VMEM((NX, 192, 128), BF),
         pltpu.VMEM((ROWS, D), BF),
         pltpu.VMEM((NZ, ROWS, 256), BF),
         pltpu.VMEM((ROWS, FFD), F32),

time: 59.5 us -> 60.8 us (1.022)
  Pallas kernels: 58.7 us -> 60.1 us
    pallas_call x1, Pallas kernels: 58.7 us -> 60.1 us  [layer(): pl.pallas_call(kernel, out_shape=pltpu.VMEM((32, D), BF), in_specs=[hbm]...]
where the time goes in v10:
time: 60.8 us; the launch traced here: 60.7 us
  Pallas kernels  60.1 us (99%)
  local copies, waits for them, and re-layouts  0.66 us (1%)
    pallas_call x1, Pallas kernels, layer(): pl.pallas_call(kernel, out_shape=pltpu.VMEM((32, D), BF), in_specs=[hbm]...  60.1 us

profile of v10, /device:TPU:1, one launch (start us, length us, event | category | flops | bytes accessed | tf_op | source)
XLA Modules:
  0.0 60.7 jit_solution(15034525282555817134)
XLA Ops:
  0.0 60.1 %shard_map.118 = bf16[32,2048]{1,0:T(8,128)(2,1)S(1)} custom-call(bf16[2048]{0:T(1024)(128)(2,1)} %gain_hbm.1, bf16[3,768]{1,0:T(4,128)(2,1)} %conv_hbm.1, bf16[320,128]{1,0:T(8,128)(2,1)} %bitcast.3, bf16[128,512]{1,0:T(8,128)(2,1)} %lat_hbm.1, bf16[64,128]{1,0:T(8,128)(2,1)} %bitcast.5, bf16[512,384]{1,0:T(8,128)(2,1)} %ew_hbm.1, ...), custom_call_target="tpu_custom_call" | custom-call | tf_op jit(solution)/shard_map/pallas_call | solution.py:674
  60.1 0.7 %copy.14 = bf16[32,2048]{1,0:T(8,128)(2,1)} copy(bf16[32,2048]{1,0:T(8,128)(2,1)S(1)} %shard_map.118) | data formatting | bytes 262144

commit v11 on v9

--- a/solution.py
+++ b/solution.py
@@ -379,7 +379,6 @@
         send(resid.at[pl.ds(112, 16)], resid.at[pl.ds(128, 16)], h_s, h_r.at[0], device_of(after))
         send(resid.at[pl.ds(0, 16)], resid.at[pl.ds(144, 16)], h_s, h_r.at[1], device_of(before))
 
-    edges_out()
     gb_z(0)
     gb_y(0, 0)
     va_y(0)
@@ -390,6 +389,7 @@
     kvz(1, 2)
     kvz(1, 3)
     da_y(0)
+    edges_out()
     gb_y(1, 0)
     va_y(1)
     gb_z(1)

time: 59.5 us -> 60 us (level)
  no operation moved by 1% of the time
where the time goes in v11:
time: 60 us; the launch traced here: 59.9 us
  Pallas kernels  59.3 us (99%)
  local copies, waits for them, and re-layouts  0.66 us (1%)
    pallas_call x1, Pallas kernels, layer(): pl.pallas_call(kernel, out_shape=pltpu.VMEM((32, D), BF), in_specs=[hbm]...  59.3 us

profile of v11, /device:TPU:1, one launch (start us, length us, event | category | flops | bytes accessed | tf_op | source)
XLA Modules:
  0.0 59.9 jit_solution(6359611919580268255)
XLA Ops:
  0.0 59.3 %shard_map.118 = bf16[32,2048]{1,0:T(8,128)(2,1)S(1)} custom-call(bf16[2048]{0:T(1024)(128)(2,1)} %gain_hbm.1, bf16[3,768]{1,0:T(4,128)(2,1)} %conv_hbm.1, bf16[320,128]{1,0:T(8,128)(2,1)} %bitcast.3, bf16[128,512]{1,0:T(8,128)(2,1)} %lat_hbm.1, bf16[64,128]{1,0:T(8,128)(2,1)} %bitcast.5, bf16[512,384]{1,0:T(8,128)(2,1)} %ew_hbm.1, ...), custom_call_target="tpu_custom_call" | custom-call | tf_op jit(solution)/shard_map/pallas_call | solution.py:666
  59.3 0.7 %copy.14 = bf16[32,2048]{1,0:T(8,128)(2,1)} copy(bf16[32,2048]{1,0:T(8,128)(2,1)S(1)} %shard_map.118) | data formatting | bytes 262144
